TPU v7x, 32 devices: a whole 2x2x4 slice. The times are simulated.
32 devices in a mesh: row: 16 (over z, y, x), col: 2 (over core).
Axes of the slice: x: 2, y: 2, z: 4, core: 2. Of those that a mesh axis runs over, the one named last changes fastest.
Arguments:
- tokens: bfloat16 [2, 6144, 2048], P('col', 'row'), may hold values from -6 to 6
- norm_gain: bfloat16 [2048], replicated, may hold values from 0.099609375 to 1.8984375
- in_weight: bfloat16 [2048, 512], P('row', 'col'), may hold values from -0.125 to 0.125
- out_weight: bfloat16 [512, 2048], P('col', 'row'), may hold values from -0.25 to 0.25
Outputs:
- mixed: bfloat16 [2, 6144, 2048], P('col', 'row')
All inputs are finite; a program needn't handle non-finite values.
Results may differ from a plain program's by a relative error of at most 0.013.
Values may be sent and summed in bfloat16 or wider, within the bound.
No kernel may reach another device: no remote copies, remote signals or barrier semaphores. Data moves between devices by JAX's collectives and lax.ppermute only.
A program may use at most 64 MiB of HBM per device.

v0:
```python
import math

import jax
import jax.numpy as jnp
from jax import lax
from jax.sharding import PartitionSpec as P

GS = 64


EPS = 1e-06
PRECISE = lax.Precision.HIGHEST


def angle_pair(left_index, right_index, modulus):
    product = left_index[:, None] * right_index[None, :] % modulus
    radians = product.astype(jnp.float32) * (2.0 * math.pi / modulus)
    return (jnp.cos(radians), jnp.sin(radians))


def table_dot(matrix, values):
    return jnp.dot(matrix, values, precision=PRECISE, preferred_element_type=jnp.float32)


def right_dot(values, matrix):
    return jnp.dot(values, matrix, precision=PRECISE, preferred_element_type=jnp.float32)


def body(tokens, norm_gain, in_weight, out_weight):
    own_rows = tokens[0].astype(jnp.float32)
    inverse_rms = lax.rsqrt(jnp.mean(own_rows * own_rows, axis=-1, keepdims=True) + EPS)
    normed = (own_rows * inverse_rms * norm_gain.astype(jnp.float32)).astype(jnp.bfloat16)
    in_columns, out_rows = (
        lax.all_gather(in_weight, "col", axis=1, tiled=True),
        lax.all_gather(out_weight, "col", axis=0, tiled=True),
    )
    row_count = normed.shape[0]
    channels = in_columns.shape[1]
    peer_count = lax.axis_size("row")
    length = row_count * peer_count
    projected = jnp.dot(
        normed,
        lax.all_gather(in_columns, "row", axis=0, tiled=True),
        preferred_element_type=jnp.float32,
    ).astype(jnp.bfloat16)
    channel_index = jnp.arange(channels, dtype=jnp.int32)
    within = channel_index % GS
    same_group = channel_index[:, None] // GS == channel_index[None, :] // GS
    group_cos, group_sin = angle_pair(within, within, GS)
    group_cos = jnp.where(same_group, group_cos, 0.0)
    group_sin = jnp.where(same_group, group_sin, 0.0)
    peer_index = jnp.arange(peer_count, dtype=jnp.int32)
    small_cos, small_sin = angle_pair(peer_index, peer_index, peer_count)
    line_index = jnp.arange(row_count, dtype=jnp.int32)
    long_cos, long_sin = angle_pair(line_index, line_index, row_count)
    gathered = lax.all_to_all(projected, "row", split_axis=1, concat_axis=0, tiled=True).astype(
        jnp.float32
    )
    narrow = gathered.shape[1]
    flat = gathered.reshape(peer_count, row_count * narrow)
    first_real = table_dot(small_cos, flat).reshape(peer_count, row_count, narrow)
    first_imag = (-table_dot(small_sin, flat)).reshape(peer_count, row_count, narrow)
    turn_cos, turn_sin = angle_pair(peer_index, line_index, length)
    turn_cos = turn_cos[:, :, None]
    turn_sin = turn_sin[:, :, None]
    turned_real = first_real * turn_cos + first_imag * turn_sin
    turned_imag = first_imag * turn_cos - first_real * turn_sin
    lines_real = turned_real.transpose(1, 0, 2).reshape(row_count, peer_count * narrow)
    lines_imag = turned_imag.transpose(1, 0, 2).reshape(row_count, peer_count * narrow)
    whole_real = (table_dot(long_cos, lines_real) + table_dot(long_sin, lines_imag)).reshape(
        length, narrow
    )
    whole_imag = (table_dot(long_cos, lines_imag) - table_dot(long_sin, lines_real)).reshape(
        length, narrow
    )
    back_real, back_imag = (
        lax.all_to_all(
            whole_real.astype(jnp.bfloat16), "row", split_axis=0, concat_axis=1, tiled=True
        ).astype(whole_real.dtype),
        lax.all_to_all(
            whole_imag.astype(jnp.bfloat16), "row", split_axis=0, concat_axis=1, tiled=True
        ).astype(whole_imag.dtype),
    )
    mixed_real = right_dot(back_real, group_cos) + right_dot(back_imag, group_sin)
    arranged = (mixed_real * (1.0 / math.sqrt(length * GS))).astype(jnp.bfloat16)
    result = jnp.dot(
        arranged,
        lax.all_gather(out_rows, "row", axis=1, tiled=True),
        preferred_element_type=jnp.float32,
    )
    return result.astype(jnp.bfloat16)[None]


def solution(mesh):
    in_specs = (P("col", "row", None), P(), P("row", "col"), P("col", "row"))
    out_specs = P("col", "row", None)
    return jax.shard_map(body, mesh=mesh, in_specs=in_specs, out_specs=out_specs, check_vma=False)
```

profile of v0, /device:TPU:0, one launch (start us, length us, event | category | flops | bytes accessed | tf_op | source)
XLA Modules:
  0.0 173.7 jit_solution(4385895782396429230)
XLA Ops:
  6.5 3.8 %all_gather.12 = bf16[128,512]{1,0:T(8,128)(2,1)} all-gather(bf16[128,256]{1,0:T(8,128)(2,1)} %param.6), channel_id=1, replica_groups=mesh['row'=16,'col'=2] {'col'}, dimensions={1}, use_global_device_ids=true | all-gather | bytes 196608 | tf_op jit(solution)/shard_map/all_gather | solution.py:34
  10.4 3.4 %all_gather.14 = bf16[512,128]{1,0:T(8,128)(2,1)} all-gather(bf16[256,128]{1,0:T(8,128)(2,1)} %param.7), channel_id=1, replica_groups=mesh['row'=16,'col'=2] {'col'}, dimensions={0}, use_global_device_ids=true | all-gather | bytes 196608 | tf_op jit(solution)/shard_map/all_gather | solution.py:35
  13.8 0.7 convert_element_type.77
  14.5 1.8 %fusion = f32[384]{0:T(512)S(1)} fusion(bf16[1,384,2048]{2,1,0:T(8,128)(2,1)} %param.4), kind=kLoop, calls=%fused_computation.3 | loop fusion | flops 2358912 | bytes 1574400 | tf_op jit(solution)/shard_map/reduce_sum | solution.py:31
  16.3 57.0 %all-gather.3.cloned.1.call-done = bf16[2048,512]{1,0:T(8,128)(2,1)} async-done(((bf16[128,512]{1,0:T(8,128)(2,1)}), bf16[2048,512]{1,0:T(8,128)(2,1)}) %all-gather.3.cloned.1.call-update) | async-done | bytes 2097168 | tf_op jit(solution)/shard_map/all_gather | solution.py:43
  73.3 2.6 %fusion.13 = bf16[384,512]{1,0:T(8,128)(2,1)S(1)} fusion(bf16[2048,512]{1,0:T(8,128)(2,1)} %all-gather.3.cloned.1.call-done, bf16[1,384,2048]{2,1,0:T(8,128)(2,1)S(1)} %copy-done.1, f32[2048]{0:T(1024)S(1)} %convert_element_type.77, f32[384]{0:T(512)S(1)} %add_rsqrt_fusion), kind=kOutput, calls=%fused_computation.26 | convolution fusion | flops 808648704 | bytes 4072960 | tf_op jit(solution)/shard_map/dot_general | solution.py:41
  75.9 0.9 copy.14
  76.9 4.4 %all-to-all-start = ((bf16[384,16,32]{0,2,1:T(8,128)(2,1)}), bf16[384,16,32]{0,2,1:T(8,128)(2,1)S(1)}, u32[]{:S(2)}, u32[]{:S(2)}) async-start(bf16[384,16,32]{0,2,1:T(8,128)(2,1)} %bitcast.3), calls=%async_computation | async-start | bytes 786432 | tf_op jit(solution)/shard_map/all_to_all | solution.py:56
  81.3 0.7 fusion.59
  82.0 10.8 %all-to-all-done = bf16[384,16,32]{0,2,1:T(8,128)(2,1)S(1)} async-done(((bf16[384,16,32]{0,2,1:T(8,128)(2,1)}), bf16[384,16,32]{0,2,1:T(8,128)(2,1)S(1)}, u32[]{:S(2)}, u32[]{:S(2)}) %all-to-all-start) | async-done | bytes 393248 | tf_op jit(solution)/shard_map/all_to_all | solution.py:56
  92.9 0.8 copy.15
  93.7 1.6 reshape.164
  95.3 1.4 convolution_negate_fusion
  96.7 2.2 %reshape.165 = f32[16,384,32]{2,1,0:T(8,128)S(1)} reshape(f32[16,12288]{1,0:T(8,128)} %convolution_negate_fusion) | data formatting | bytes 1572864 | tf_op jit(solution)/shard_map/reshape | solution.py:62
  98.9 1.9 %copy.17 = f32[16,384,32]{1,0,2:T(8,128)} copy(f32[16,384,32]{2,1,0:T(8,128)S(1)} %reshape.165) | data formatting | bytes 1572864 | tf_op jit(solution)/shard_map/reshape | solution.py:62
  100.8 1.3 dot_general.36
  102.1 0.7 copy.16
  104.1 5.1 %fusion.30 = f32[384,512]{1,0:T(8,128)S(1)} fusion(f32[384,512]{0,1:T(8,128)S(1)} %bitcast.46), kind=kOutput, calls=%fused_computation.44 | convolution fusion | flops 907296768 | bytes 1572864 | tf_op jit(solution)/shard_map/dot_general | solution.py:22
  109.2 4.3 %fusion.10 = bf16[384,512]{1,0:T(8,128)(2,1)S(1)} fusion(f32[384,512]{1,0:T(8,128)S(1)} %fusion.30, f32[384,512]{0,1:T(8,128)S(1)} %bitcast.48), kind=kOutput, calls=%fused_computation.23 | convolution fusion | flops 907689984 | bytes 1966080 | tf_op jit(solution)/shard_map/dot_general | solution.py:22
  113.5 0.9 convert_element_type.82
  114.4 1.3 copy.21
  115.7 3.7 %all-to-all-start.1 = ((bf16[16,384,32]{1,2,0:T(8,128)(2,1)}), bf16[16,384,32]{1,2,0:T(8,128)(2,1)S(1)}, u32[]{:S(2)}, u32[]{:S(2)}) async-start(bf16[16,384,32]{1,2,0:T(8,128)(2,1)} %copy.21), calls=%async_computation.1 | async-start | bytes 786432 | tf_op jit(solution)/shard_map/all_to_all | solution.py:77
  119.4 5.1 %fusion.28 = f32[384,512]{1,0:T(8,128)S(1)} fusion(f32[384,512]{0,1:T(8,128)S(1)} %bitcast.49), kind=kOutput, calls=%fused_computation.43 | convolution fusion | flops 907296768 | bytes 1572864 | tf_op jit(solution)/shard_map/dot_general | solution.py:22
  124.5 4.3 %fusion.11 = bf16[384,512]{1,0:T(8,128)(2,1)S(1)} fusion(f32[384,512]{1,0:T(8,128)S(1)} %fusion.28, f32[384,512]{0,1:T(8,128)S(1)} %bitcast.47), kind=kOutput, calls=%fused_computation.24 | convolution fusion | flops 907689984 | bytes 1966080 | tf_op jit(solution)/shard_map/dot_general | solution.py:22
  128.9 0.9 convert_element_type.85
  129.7 1.3 copy.22
  131.0 6.3 %all-to-all-done.1 = bf16[16,384,32]{1,2,0:T(8,128)(2,1)S(1)} async-done(((bf16[16,384,32]{1,2,0:T(8,128)(2,1)}), bf16[16,384,32]{1,2,0:T(8,128)(2,1)S(1)}, u32[]{:S(2)}, u32[]{:S(2)}) %all-to-all-start.1) | async-done | bytes 393248 | tf_op jit(solution)/shard_map/all_to_all | solution.py:77
  137.3 8.8 %all-to-all-start.2 = ((bf16[16,384,32]{1,2,0:T(8,128)(2,1)}), bf16[16,384,32]{1,2,0:T(8,128)(2,1)S(1)}, u32[]{:S(2)}, u32[]{:S(2)}) async-start(bf16[16,384,32]{1,2,0:T(8,128)(2,1)} %copy.22), calls=%async_computation.2 | async-start | bytes 786432 | tf_op jit(solution)/shard_map/all_to_all | solution.py:80
  146.2 4.8 %fusion.16 = f32[384,512]{1,0:T(8,128)S(1)} fusion(bf16[384,512]{0,1:T(8,128)(2,1)S(1)} %bitcast.50, s32[512]{0:T(512)S(1)} %get-tuple-element.9, s32[512]{0:T(512)S(1)} %get-tuple-element.10), kind=kOutput, calls=%fused_computation.27 | convolution fusion | flops 1212153856 | bytes 1183744 | tf_op jit(solution)/shard_map/dot_general | solution.py:26
  151.0 7.2 %all-to-all-done.2 = bf16[16,384,32]{1,2,0:T(8,128)(2,1)S(1)} async-done(((bf16[16,384,32]{1,2,0:T(8,128)(2,1)}), bf16[16,384,32]{1,2,0:T(8,128)(2,1)S(1)}, u32[]{:S(2)}, u32[]{:S(2)}) %all-to-all-start.2) | async-done | bytes 393248 | tf_op jit(solution)/shard_map/all_to_all | solution.py:80
  158.2 4.9 %fusion.12 = bf16[384,512]{1,0:T(8,128)(2,1)S(1)} fusion(f32[384,512]{1,0:T(8,128)S(1)} %fusion.16, bf16[384,512]{0,1:T(8,128)(2,1)S(1)} %bitcast.51, s32[512]{0:T(512)S(1)} %get-tuple-element.9, s32[512]{0:T(512)S(1)} %get-tuple-element.10), kind=kOutput, calls=%fused_computation.25 | convolution fusion | flops 1212743680 | bytes 1576960 | tf_op jit(solution)/shard_map/dot_general | solution.py:26
  163.1 3.7 %fusion.3 = bf16[1,384,2048]{2,1,0:T(8,128)(2,1)} fusion(bf16[384,512]{1,0:T(8,128)(2,1)S(1)} %fusion.12, bf16[512,2048]{1,0:T(8,128)(2,1)} %all-gather.5.cloned.1.call-done), kind=kOutput, calls=%fused_computation.7 | convolution fusion | flops 806092800 | bytes 4063232 | tf_op jit(solution)/shard_map/dot_general | solution.py:86
  (18 shorter events, 1.3 us)
Async XLA Ops:
  6.5 66.8 %copy-start.1 = (bf16[1,384,2048]{2,1,0:T(8,128)(2,1)S(1)}, bf16[1,384,2048]{2,1,0:T(8,128)(2,1)}, u32[]{:S(2)}) copy-start(bf16[1,384,2048]{2,1,0:T(8,128)(2,1)} %param.4) | copy-start | bytes 4718596
  6.5 66.8 %all-gather.3.cloned.1.call-start = ((), (), s32[]{:S(2)}) async-start(), calls=%async_computation.3 | async-start | bytes 2228224 | tf_op jit(solution)/shard_map/all_gather | solution.py:43
  10.4 152.7 %all-gather.5.cloned.1.call-start = ((), (), s32[]{:S(2)}) async-start(), calls=%async_computation.4 | async-start | bytes 2228224 | tf_op jit(solution)/shard_map/all_gather | solution.py:88
  76.9 16.0 %all-to-all-start = ((bf16[384,16,32]{0,2,1:T(8,128)(2,1)}), bf16[384,16,32]{0,2,1:T(8,128)(2,1)S(1)}, u32[]{:S(2)}, u32[]{:S(2)}) async-start(bf16[384,16,32]{0,2,1:T(8,128)(2,1)} %bitcast.3), calls=%async_computation | async-start | bytes 786432 | tf_op jit(solution)/shard_map/all_to_all | solution.py:56
  100.8 2.0 %copy-start = (f32[16,384,32]{1,0,2:T(8,128)S(1)}, f32[16,384,32]{1,0,2:T(8,128)}, u32[]{:S(2)}) copy-start(f32[16,384,32]{1,0,2:T(8,128)} %copy.17) | copy-start | bytes 2359300
  100.8 2.0 %copy-start.2 = (f32[16,384]{1,0:T(8,128)S(1)}, f32[16,384]{1,0:T(8,128)}, u32[]{:S(2)}) copy-start(f32[16,384]{1,0:T(8,128)} %get-tuple-element.7) | copy-start | bytes 73732
  100.8 2.0 %copy-start.3 = (f32[16,384]{1,0:T(8,128)S(1)}, f32[16,384]{1,0:T(8,128)}, u32[]{:S(2)}) copy-start(f32[16,384]{1,0:T(8,128)} %get-tuple-element.8) | copy-start | bytes 73732
  115.7 21.7 %all-to-all-start.1 = ((bf16[16,384,32]{1,2,0:T(8,128)(2,1)}), bf16[16,384,32]{1,2,0:T(8,128)(2,1)S(1)}, u32[]{:S(2)}, u32[]{:S(2)}) async-start(bf16[16,384,32]{1,2,0:T(8,128)(2,1)} %copy.21), calls=%async_computation.1 | async-start | bytes 786432 | tf_op jit(solution)/shard_map/all_to_all | solution.py:77
  137.3 20.8 %all-to-all-start.2 = ((bf16[16,384,32]{1,2,0:T(8,128)(2,1)}), bf16[16,384,32]{1,2,0:T(8,128)(2,1)S(1)}, u32[]{:S(2)}, u32[]{:S(2)}) async-start(bf16[16,384,32]{1,2,0:T(8,128)(2,1)} %copy.22), calls=%async_computation.2 | async-start | bytes 786432 | tf_op jit(solution)/shard_map/all_to_all | solution.py:80
Sparse Core Ops, SparseCore 0:
  10.5 62.7 all-gather.2
  76.0 69.8 all-gather.4
where the time goes:
time: 174 us
  waiting for transfers between devices  81.4 us (47%)
  matrix products  36.9 us (21%)
  starting transfers between devices  17 us (10%)
  local copies, waits for them, and re-layouts  14.3 us (8%)
  between operations  13.6 us (8%)
  blocking collectives  7.18 us (4%)
  other arithmetic  3.24 us (2%)
    all_gather x1, waiting for transfers between devices, body(): lax.all_gather(in_columns, 'row', axis=0, tiled=True)  57 us
    dot_general x6, matrix products, table_dot(): jnp.dot(matrix, values, precision=PRECISE, preferred_element_type=jnp.flo...  20.9 us
    all_to_all x1, waiting for transfers between devices, body(): lax.all_to_all(projected, 'row', split_axis=1, concat_axis=0, tiled=True)  10.8 us
    dot_general x2, matrix products, right_dot(): jnp.dot(values, matrix, precision=PRECISE, preferred_element_type=jnp.flo...  9.71 us
    all_to_all x1, starting transfers between devices, body(): lax.all_to_all(whole_imag.astype(jnp.bfloat16), 'row', split_axis=0, conc...  8.8 us
    all_to_all x1, waiting for transfers between devices, body(): lax.all_to_all(whole_imag.astype(jnp.bfloat16), 'row', split_axis=0, conc...  7.2 us
    all_to_all x1, waiting for transfers between devices, body(): lax.all_to_all(whole_real.astype(jnp.bfloat16), 'row', split_axis=0, conc...  6.31 us
    all_to_all x1, starting transfers between devices, body(): lax.all_to_all(projected, 'row', split_axis=1, concat_axis=0, tiled=True)  4.42 us
  transfers between devices with their start and end apart: 5, of which 4 were waited for; matrix products, arithmetic and copies ran while one was open for 29% of the time, Pallas kernels for 0%

commit v1 on v0

v1 whole, which is shorter than its diff:
```python
import math

import jax
import jax.numpy as jnp
import numpy as np
from jax import lax
from jax.sharding import PartitionSpec as P

GS = 64
EPS = 1e-06
BF = jnp.bfloat16
F32 = jnp.float32


def angles(left, right, modulus):
    product = np.outer(np.asarray(left, np.int64), np.asarray(right, np.int64)) % modulus
    radians = product.astype(np.float64) * (2.0 * math.pi / modulus)
    return np.cos(radians), np.sin(radians)


def group_tables():
    cos, sin = angles(np.arange(GS), np.arange(GS), GS)
    half = GS // 2
    split = np.concatenate([cos[:, : half + 1], sin[:, 1:half]], axis=1)
    join = np.zeros((GS, GS))
    for j in range(half + 1):
        join[j, j] = 1.0
    for j in range(1, half):
        join[half + j, j] = -1.0
        join[j, GS - j] = 1.0
        join[half + j, GS - j] = 1.0
    return split, join


def spread_half(shard, peers):
    near = peers // 2
    other = lax.ppermute(shard, "row", [(i, i ^ near) for i in range(peers)])
    upper = lax.axis_index("row") >= near
    both = jnp.stack([jnp.where(upper, other, shard), jnp.where(upper, shard, other)])
    copies = jnp.broadcast_to(both[None], (near,) + both.shape)
    groups = [list(range(near)), list(range(near, peers))]
    got = lax.all_to_all(copies, "row", split_axis=0, concat_axis=0, tiled=True, axis_index_groups=groups)
    return got.transpose(1, 0, *range(2, got.ndim)).reshape((peers,) + shard.shape)


def column_parts(own, cols):
    if cols == 2:
        return [own, lax.ppermute(own, "col", [(0, 1), (1, 0)])]
    got = lax.all_gather(own, "col", axis=0, tiled=False)
    return [got[i] for i in range(cols)]


def dot(a, b, dims=((1,), (0,))):
    return lax.dot_general(a, b, (dims, ((), ())), preferred_element_type=F32)


def body(tokens, norm_gain, in_weight, out_weight):
    peers = lax.axis_size("row")
    cols = lax.axis_size("col")
    rows = tokens.shape[1]
    length = rows * peers
    channels = in_weight.shape[1] * cols
    narrow = channels // peers
    inner = rows // peers

    in_own = spread_half(in_weight, peers)
    in_own = in_own.reshape(-1, in_weight.shape[1])
    in_parts = column_parts(in_own, cols)
    out_own = spread_half(out_weight, peers)
    out_own = out_own.transpose(1, 0, 2).reshape(out_weight.shape[0], -1)
    out_parts = column_parts(out_own, cols)

    own_rows = tokens[0].astype(F32)
    inverse_rms = lax.rsqrt(jnp.mean(own_rows * own_rows, axis=-1, keepdims=True) + EPS)
    normed = (own_rows * inverse_rms * norm_gain.astype(F32)).astype(BF)
    projected = jnp.concatenate([dot(normed, part).astype(BF) for part in in_parts], axis=1)

    split, join = group_tables()
    groups = channels // GS
    split_all = jnp.asarray(np.kron(np.eye(groups), split.T), BF)
    join_all = jnp.asarray(np.kron(np.eye(groups), join), BF)
    sums = dot(split_all, projected, ((1,), (1,))).astype(BF)

    got = lax.all_to_all(sums.reshape(peers, narrow, rows), "row", split_axis=0, concat_axis=0, tiled=True)
    small_cos, small_sin = angles(np.arange(peers), np.arange(peers), peers)
    first = jnp.asarray(np.kron(np.concatenate([small_cos, -small_sin]), np.eye(narrow)), BF)
    stage = dot(first, got.reshape(channels, rows)).reshape(2, peers, narrow, rows)
    turn_cos, turn_sin = angles(np.arange(peers), np.arange(rows), length)
    turn_cos = jnp.asarray(turn_cos[:, None, :], F32)
    turn_sin = jnp.asarray(turn_sin[:, None, :], F32)
    real = stage[0] * turn_cos + stage[1] * turn_sin
    imag = stage[1] * turn_cos - stage[0] * turn_sin
    which = (lax.axis_index("row") * narrow + jnp.arange(narrow, dtype=jnp.int32)) % GS
    sine = (which > GS // 2)[None, :, None]
    lead = jnp.where(sine, -imag, real)
    tail = jnp.where(sine, real, imag)
    turned = jnp.concatenate([lead, tail], axis=-1).astype(BF).reshape(channels, 2 * rows)
    long_cos, long_sin = angles(np.arange(rows), np.arange(rows), rows)
    second = jnp.asarray(np.concatenate([long_cos, long_sin], axis=1), BF)
    whole = dot(second, turned, ((1,), (1,))).astype(BF)

    back = lax.all_to_all(whole.reshape(peers, inner, channels), "row", split_axis=0, concat_axis=0, tiled=True)
    back = back.reshape(peers, inner, peers, narrow).transpose(1, 2, 0, 3).reshape(rows, channels)
    mixed_real = (dot(back, join_all) * (1.0 / math.sqrt(length * GS))).astype(BF)
    width = channels // len(out_parts)
    result = sum(
        dot(mixed_real[:, i * width : (i + 1) * width], part) for i, part in enumerate(out_parts)
    )
    return result.astype(BF)[None]


def solution(mesh):
    in_specs = (P("col", "row", None), P(), P("row", "col"), P("col", "row"))
    out_specs = P("col", "row", None)
    return jax.shard_map(body, mesh=mesh, in_specs=in_specs, out_specs=out_specs, check_vma=False)
```

time: 174 us -> 98.4 us (0.57)
  waiting for transfers between devices: 81.4 us -> 36 us
  matrix products: 36.9 us -> 11.9 us
  between operations: 13.6 us -> 0.26 us
  blocking collectives: 7.18 us -> 18.4 us
  local copies, waits for them, and re-layouts: 14.3 us -> 9.74 us
  starting transfers between devices: 17 us -> 20.1 us
    all_gather x2 -> x0, waiting for transfers between devices: 57 us -> none  [the longest x1 57 us: body(): lax.all_gather(in_columns, 'row', axis=0, tiled=True)]
    dot_general x10 -> x8, matrix products: 36.9 us -> 11.9 us  [dot(): return lax.dot_general(a, b, (dims, ((), ())), preferred_element_type=F32)]
    all_to_all x0 -> x1, blocking collectives: none -> 18.4 us  [spread_half(): lax.all_to_all(copies, 'row', split_axis=0, concat_axis=0, tiled=True, ax...]
    ppermute x0 -> x4, waiting for transfers between devices: none -> 15 us  [the longest x2 15 us: spread_half(): other = lax.ppermute(shard, 'row', [(i, i ^ near) for i in range(peers)])]
    all_gather x2 -> x0, blocking collectives: 7.18 us -> none  [the longest x1 3.82 us: body(): lax.all_gather(in_weight, 'col', axis=1, tiled=True)]
    ppermute x0 -> x4, starting transfers between devices: none -> 7.03 us  [the longest x2 6.95 us: spread_half(): other = lax.ppermute(shard, 'row', [(i, i ^ near) for i in range(peers)])]
    convert_element_type x5 -> x1, local copies, waits for them, and re-layouts: 5.25 us -> 0.92 us  [body(): sums = dot(split_all, projected, ((1,), (1,))).astype(BF)]
    all_to_all x3, starting transfers between devices: 17 us -> 13 us  [the longest x1 5.2 us: body(): lax.all_to_all(sums.reshape(peers, narrow, rows), 'row', split_axis=0, co...]
  transfers between devices with their start and end apart: 5 -> 7, of which waited for: 4 -> 4; matrix products, arithmetic and copies ran while one was open for 29% -> 12% of each run, Pallas kernels for 0% -> 0%
where the time goes in v1:
time: 98.4 us; the launch traced here: 97.8 us
  waiting for transfers between devices  36 us (37%)
  starting transfers between devices  20.1 us (20%)
  blocking collectives  18.4 us (19%)
  matrix products  11.9 us (12%)
  local copies, waits for them, and re-layouts  9.74 us (10%)
  other arithmetic  1.54 us (2%)
    all_to_all x1, blocking collectives, spread_half(): lax.all_to_all(copies, 'row', split_axis=0, concat_axis=0, tiled=True, ax...  18.4 us
    ppermute x2, waiting for transfers between devices, spread_half(): other = lax.ppermute(shard, 'row', [(i, i ^ near) for i in range(peers)])  15 us
    dot_general x8, matrix products, dot(): return lax.dot_general(a, b, (dims, ((), ())), preferred_element_type=F32)  11.9 us
    all_to_all x1, waiting for transfers between devices, body(): lax.all_to_all(whole.reshape(peers, inner, channels), 'row', split_axis=0...  11 us
    all_to_all x1, waiting for transfers between devices, spread_half(): lax.all_to_all(copies, 'row', split_axis=0, concat_axis=0, tiled=True, ax...  9.98 us
    ppermute x2, starting transfers between devices, spread_half(): other = lax.ppermute(shard, 'row', [(i, i ^ near) for i in range(peers)])  6.95 us
    all_to_all x1, starting transfers between devices, body(): lax.all_to_all(sums.reshape(peers, narrow, rows), 'row', split_axis=0, co...  5.2 us
    all_to_all x1, starting transfers between devices, body(): lax.all_to_all(whole.reshape(peers, inner, channels), 'row', split_axis=0...  4.23 us
  transfers between devices with their start and end apart: 7, of which 4 were waited for; matrix products, arithmetic and copies ran while one was open for 12% of the time, Pallas kernels for 0%

profile of v1, /device:TPU:0, one launch (start us, length us, event | category | flops | bytes accessed | tf_op | source)
XLA Modules:
  0.0 97.8 jit_solution(14246640285468499379)
XLA Ops:
  0.0 4.1 %collective-permute-start = (bf16[128,256]{1,0:T(8,128)(2,1)}, bf16[128,256]{1,0:T(8,128)(2,1)S(1)}, u32[]{:S(2)}, u32[]{:S(2)}) collective-permute-start(bf16[128,256]{1,0:T(8,128)(2,1)} %param.12), channel_id=1, source_target_pairs={{0,16},{2,18},{4,20},{6,22},{8,24},{10,26},{12,28},{14,30},{16,0},... | collective-permute-start | bytes 196616 | tf_op jit(solution)/shard_map/ppermute | solution.py:37
  4.1 3.9 %collective-permute-done = bf16[128,256]{1,0:T(8,128)(2,1)S(1)} collective-permute-done((bf16[128,256]{1,0:T(8,128)(2,1)}, bf16[128,256]{1,0:T(8,128)(2,1)S(1)}, u32[]{:S(2)}, u32[]{:S(2)}) %collective-permute-start) | collective-permute-done | bytes 65568 | tf_op jit(solution)/shard_map/ppermute | solution.py:37
  7.9 0.9 select_bitcast_fusion.3
  8.9 18.4 %all_to_all.20 = bf16[8,2,128,256]{3,2,1,0:T(8,128)(2,1)S(1)} all-to-all(bf16[8,2,128,256]{3,2,1,0:T(8,128)(2,1)S(1)} %broadcast_in_dim.36), channel_id=1, replica_groups={{0,2,4,6,8,10,12,14},{16,18,20,22,24,26,28,30},{1,3,5,7,9,11,13,15},{17..., dimensions={0} | all-to-all | bytes 2097152 | tf_op jit(solution)/shard_map/all_to_all | solution.py:42
  27.5 0.5 copy-done.7
  28.0 0.7 copy-done
  28.7 0.4 fusion.2
  29.1 1.8 %fusion.30 = f32[384,512]{1,0:T(8,128)} fusion(bf16[512,256]{1,0:T(8,128)(2,1)S(1)} %copy-done.10, bf16[2048,256]{1,0:T(8,128)(2,1)S(1)} %bitcast.83, bf16[1,384,2048]{2,1,0:T(8,128)(2,1)S(1)} %copy-done, f32[2048]{0:T(1024)S(1)} %convert_element_type.49, f32[384]{0:T(512)S(1)} %add_rsqrt_fusion), kind=kOutput, calls=%fused_computation.31 | convolution fusion | flops 506560512 | bytes 3679744 | tf_op jit(solution)/shard_map/dot_general | solution.py:54
  31.0 2.4 %fusion.20 = bf16[512,384]{0,1:T(8,128)(2,1)S(1)} fusion(f32[384,512]{1,0:T(8,128)} %fusion.30, bf16[512,256]{1,0:T(8,128)(2,1)S(1)} %copy-done.9, bf16[2048,256]{1,0:T(8,128)(2,1)} %collective-permute-done.1, bf16[1,384,2048]{2,1,0:T(8,128)(2,1)S(1)} %copy-done, f32[2048]{0:T(1024)S(1)} %convert_element_type.49, f32[384]{0:T(512)S(1)} %add_rsqrt_fusion), kind=kOutput, calls=%fused_computation.24 | convolution fusion | flops 506953728 | bytes 4072960 | tf_op jit(solution)/shard_map/dot_general | solution.py:54
  33.4 0.9 copy.17
  34.3 5.2 %all-to-all-start.1 = ((bf16[16,32,384]{2,1,0:T(8,128)(2,1)}), bf16[16,32,384]{2,1,0:T(8,128)(2,1)S(1)}, u32[]{:S(2)}, u32[]{:S(2)}) async-start(bf16[16,32,384]{2,1,0:T(8,128)(2,1)} %bitcast.8), calls=%async_computation.1 | async-start | bytes 786432 | tf_op jit(solution)/shard_map/all_to_all | solution.py:84
  39.5 2.9 %collective-permute-start.2 = (bf16[256,128]{1,0:T(8,128)(2,1)S(1)}, bf16[256,128]{1,0:T(8,128)(2,1)S(1)}, u32[]{:S(2)}, u32[]{:S(2)}) collective-permute-start(bf16[256,128]{1,0:T(8,128)(2,1)S(1)} %copy-done.6), channel_id=1, source_target_pairs={{0,16},{2,18},{4,20},{6,22},{8,24},{10,26},{12,28},{14,30},{16,0},... | collective-permute-start | bytes 196616 | tf_op jit(solution)/shard_map/ppermute | solution.py:37
  42.4 11.1 %collective-permute-done.2 = bf16[256,128]{1,0:T(8,128)(2,1)S(1)} collective-permute-done((bf16[256,128]{1,0:T(8,128)(2,1)S(1)}, bf16[256,128]{1,0:T(8,128)(2,1)S(1)}, u32[]{:S(2)}, u32[]{:S(2)}) %collective-permute-start.2) | collective-permute-done | bytes 65568 | tf_op jit(solution)/shard_map/ppermute | solution.py:37
  53.6 1.2 %broadcast_in_dim.37 = bf16[8,2,256,128]{3,2,1,0:T(8,128)(2,1)} broadcast(bf16[2,256,128]{2,1,0:T(8,128)(2,1)S(1)} %pad_maximum_fusion.1), dimensions={1,2,3} | broadcast | bytes 1179648 | tf_op jit(solution)/shard_map/broadcast_in_dim | solution.py:40
  54.7 3.6 %all-to-all-start.3 = ((bf16[8,2,256,128]{3,2,1,0:T(8,128)(2,1)}), bf16[8,2,256,128]{3,2,1,0:T(8,128)(2,1)S(1)}, u32[]{:S(2)}, u32[]{:S(2)}) async-start(bf16[8,2,256,128]{3,2,1,0:T(8,128)(2,1)} %broadcast_in_dim.37), calls=%async_computation.3 | async-start | bytes 2097152 | tf_op jit(solution)/shard_map/all_to_all | solution.py:42
  58.5 0.7 fusion.42
  59.2 0.1 fusion.33
  59.3 0.1 fusion.32
  59.5 0.8 copy-done.2
  60.3 0.5 fusion.34
  60.8 0.5 copy-done.3
  61.3 1.2 %fusion.19 = bf16[512,384]{0,1:T(8,128)(2,1)} fusion(f32[512,384]{0,1:T(8,128)S(1)} %fusion.34, bf16[384,384]{1,0:T(8,128)(2,1)S(1)} %copy-done.3, bf16[512,384]{1,0:T(8,128)(2,1)S(1)} %fusion.33, f32[512,384]{1,0:T(8,128)S(1)} %fusion.32, pred[512]{0:T(512)(128)(4,1)S(1)} %broadcast_in_dim.34), kind=kOutput, calls=%fused_computation.23 | convolution fusion | flops 151584768 | bytes 2654720 | tf_op jit(solution)/shard_map/dot_general | solution.py:54
  62.5 10.0 %all-to-all-done.3 = bf16[8,2,256,128]{3,2,1,0:T(8,128)(2,1)S(1)} async-done(((bf16[8,2,256,128]{3,2,1,0:T(8,128)(2,1)}), bf16[8,2,256,128]{3,2,1,0:T(8,128)(2,1)S(1)}, u32[]{:S(2)}, u32[]{:S(2)}) %all-to-all-start.3) | async-done | bytes 1048608 | tf_op jit(solution)/shard_map/all_to_all | solution.py:42
  72.5 4.2 %all-to-all-start.2 = ((bf16[16,24,512]{2,1,0:T(8,128)(2,1)}), bf16[16,24,512]{2,1,0:T(8,128)(2,1)S(1)}, u32[]{:S(2)}, u32[]{:S(2)}) async-start(bf16[16,24,512]{2,1,0:T(8,128)(2,1)} %bitcast.13), calls=%async_computation.2 | async-start | bytes 786432 | tf_op jit(solution)/shard_map/all_to_all | solution.py:102
  76.8 1.3 %copy.20 = bf16[256,16,128]{0,2,1:T(8,128)(2,1)} copy(bf16[256,16,128]{2,0,1:T(8,128)(2,1)S(1)} %bitcast.80) | data formatting | bytes 2097152 | tf_op jit(solution)/shard_map/transpose | solution.py:70
  78.1 11.0 %all-to-all-done.2 = bf16[16,24,512]{2,1,0:T(8,128)(2,1)S(1)} async-done(((bf16[16,24,512]{2,1,0:T(8,128)(2,1)}), bf16[16,24,512]{2,1,0:T(8,128)(2,1)S(1)}, u32[]{:S(2)}, u32[]{:S(2)}) %all-to-all-start.2) | async-done | bytes 393248 | tf_op jit(solution)/shard_map/all_to_all | solution.py:102
  89.2 0.9 reshape.85
  90.0 1.0 %copy.18 = bf16[24,16,16,32]{3,2,1,0:T(8,128)(2,1)S(1)} copy(bf16[24,16,16,32]{3,1,0,2:T(8,128)(2,1)S(1)} %bitcast.79) | data formatting | bytes 786432 | tf_op jit(solution)/shard_map/transpose | solution.py:103
  91.1 1.5 %reshape.86 = bf16[384,512]{1,0:T(8,128)(2,1)S(1)} reshape(bf16[24,16,16,32]{3,2,1,0:T(8,128)(2,1)S(1)} %copy.18) | data formatting | bytes 786432 | tf_op jit(solution)/shard_map/reshape | solution.py:103
  92.6 0.4 fusion.17
  92.9 1.8 %fusion.38 = f32[384,2048]{1,0:T(8,128)S(1)} fusion(bf16[256,2048]{0,1:T(8,128)(2,1)} %bitcast.20, bf16[384,512]{1,0:T(8,128)(2,1)S(1)} %fusion.17), kind=kOutput, calls=%fused_computation.40 | convolution fusion | flops 402653184 | bytes 4390912 | tf_op jit(solution)/shard_map/dot_general | solution.py:54
  94.8 3.0 %fusion.7 = bf16[1,384,2048]{2,1,0:T(8,128)(2,1)} fusion(f32[384,2048]{1,0:T(8,128)S(1)} %fusion.38, bf16[256,2048]{0,1:T(8,128)(2,1)} %collective-permute-done.3, bf16[384,512]{1,0:T(8,128)(2,1)S(1)} %fusion.17), kind=kOutput, calls=%fused_computation.10 | convolution fusion | flops 404226048 | bytes 5963776 | tf_op jit(solution)/shard_map/dot_general | solution.py:54
  (34 shorter events, 0.6 us)
Async XLA Ops:
  0.0 7.9 %collective-permute-start = (bf16[128,256]{1,0:T(8,128)(2,1)}, bf16[128,256]{1,0:T(8,128)(2,1)S(1)}, u32[]{:S(2)}, u32[]{:S(2)}) collective-permute-start(bf16[128,256]{1,0:T(8,128)(2,1)} %param.12), channel_id=1, source_target_pairs={{0,16},{2,18},{4,20},{6,22},{8,24},{10,26},{12,28},{14,30},{16,0},... | collective-permute-start | bytes 196616 | tf_op jit(solution)/shard_map/ppermute | solution.py:37
  27.3 0.7 copy-start.7
  27.3 1.4 %copy-start = (bf16[1,384,2048]{2,1,0:T(8,128)(2,1)S(1)}, bf16[1,384,2048]{2,1,0:T(8,128)(2,1)}, u32[]{:S(2)}) copy-start(bf16[1,384,2048]{2,1,0:T(8,128)(2,1)} %param.10) | copy-start | bytes 4718596
  27.3 1.8 %copy-start.10 = (bf16[512,256]{1,0:T(8,128)(2,1)S(1)}, bf16[512,256]{1,0:T(8,128)(2,1)}, u32[]{:S(2)}) copy-start(bf16[512,256]{1,0:T(8,128)(2,1)} %constant.54) | copy-start | bytes 786436
  27.4 3.6 %collective-permute-start.1 = (bf16[2048,256]{1,0:T(8,128)(2,1)S(1)}, bf16[2048,256]{1,0:T(8,128)(2,1)}, u32[]{:S(2)}, u32[]{:S(2)}) collective-permute-start(bf16[2048,256]{1,0:T(8,128)(2,1)S(1)} %bitcast.82), channel_id=1, source_target_pairs={{0,1},{1,0},{2,3},{3,2},{4,5},{5,4},{6,7},{7,6},{8,9},{9,8},{10,11... | collective-permute-start | bytes 3145736 | tf_op jit(solution)/shard_map/ppermute | solution.py:48
  29.1 1.9 %copy-start.9 = (bf16[512,256]{1,0:T(8,128)(2,1)S(1)}, bf16[512,256]{1,0:T(8,128)(2,1)}, u32[]{:S(2)}) copy-start(bf16[512,256]{1,0:T(8,128)(2,1)} %constant.55) | copy-start | bytes 786436
  33.4 6.1 %copy-start.6 = (bf16[256,128]{1,0:T(8,128)(2,1)S(1)}, bf16[256,128]{1,0:T(8,128)(2,1)}, u32[]{:S(2)}) copy-start(bf16[256,128]{1,0:T(8,128)(2,1)} %param.13) | copy-start | bytes 196612
  34.3 19.3 %all-to-all-start.1 = ((bf16[16,32,384]{2,1,0:T(8,128)(2,1)}), bf16[16,32,384]{2,1,0:T(8,128)(2,1)S(1)}, u32[]{:S(2)}, u32[]{:S(2)}) async-start(bf16[16,32,384]{2,1,0:T(8,128)(2,1)} %bitcast.8), calls=%async_computation.1 | async-start | bytes 786432 | tf_op jit(solution)/shard_map/all_to_all | solution.py:84
  39.5 14.0 %collective-permute-start.2 = (bf16[256,128]{1,0:T(8,128)(2,1)S(1)}, bf16[256,128]{1,0:T(8,128)(2,1)S(1)}, u32[]{:S(2)}, u32[]{:S(2)}) collective-permute-start(bf16[256,128]{1,0:T(8,128)(2,1)S(1)} %copy-done.6), channel_id=1, source_target_pairs={{0,16},{2,18},{4,20},{6,22},{8,24},{10,26},{12,28},{14,30},{16,0},... | collective-permute-start | bytes 196616 | tf_op jit(solution)/shard_map/ppermute | solution.py:37
  53.6 4.9 %copy-start.1 = (bf16[1024,512]{1,0:T(8,128)(2,1)S(1)}, bf16[1024,512]{1,0:T(8,128)(2,1)}, u32[]{:S(2)}) copy-start(bf16[1024,512]{1,0:T(8,128)(2,1)} %constant.49.clone) | copy-start | bytes 3145732
  54.7 17.7 %all-to-all-start.3 = ((bf16[8,2,256,128]{3,2,1,0:T(8,128)(2,1)}), bf16[8,2,256,128]{3,2,1,0:T(8,128)(2,1)S(1)}, u32[]{:S(2)}, u32[]{:S(2)}) async-start(bf16[8,2,256,128]{3,2,1,0:T(8,128)(2,1)} %broadcast_in_dim.37), calls=%async_computation.3 | async-start | bytes 2097152 | tf_op jit(solution)/shard_map/all_to_all | solution.py:42
  58.3 0.9 copy-start.4
  58.3 0.9 copy-start.5
  59.3 1.0 copy-start.2
  60.3 1.0 copy-start.3
  72.5 16.7 %all-to-all-start.2 = ((bf16[16,24,512]{2,1,0:T(8,128)(2,1)}), bf16[16,24,512]{2,1,0:T(8,128)(2,1)S(1)}, u32[]{:S(2)}, u32[]{:S(2)}) async-start(bf16[16,24,512]{2,1,0:T(8,128)(2,1)} %bitcast.13), calls=%async_computation.2 | async-start | bytes 786432 | tf_op jit(solution)/shard_map/all_to_all | solution.py:102
  78.1 16.6 %collective-permute-start.3 = (bf16[256,2048]{0,1:T(8,128)(2,1)}, bf16[256,2048]{0,1:T(8,128)(2,1)}, u32[]{:S(2)}, u32[]{:S(2)}) collective-permute-start(bf16[256,2048]{0,1:T(8,128)(2,1)} %bitcast.20), channel_id=1, source_target_pairs={{0,1},{1,0},{2,3},{3,2},{4,5},{5,4},{6,7},{7,6},{8,9},{9,8},{10,11... | collective-permute-start | bytes 3145736 | tf_op jit(solution)/shard_map/ppermute | solution.py:48
  91.0 1.5 %copy-start.8 = (bf16[512,512]{1,0:T(8,128)(2,1)S(1)}, bf16[512,512]{1,0:T(8,128)(2,1)}, u32[]{:S(2)}) copy-start(bf16[512,512]{1,0:T(8,128)(2,1)} %constant.48.clone) | copy-start | bytes 1572868

commit v2 on v1

--- a/solution.py
+++ b/solution.py
@@ -4,6 +4,8 @@
 import jax.numpy as jnp
 import numpy as np
 from jax import lax
+from jax.experimental import pallas as pl
+from jax.experimental.pallas import tpu as pltpu
 from jax.sharding import PartitionSpec as P
 
 GS = 64
@@ -54,7 +56,7 @@
     return lax.dot_general(a, b, (dims, ((), ())), preferred_element_type=F32)
 
 
-def body(tokens, norm_gain, in_weight, out_weight):
+def body_general(tokens, norm_gain, in_weight, out_weight):
     peers = lax.axis_size("row")
     cols = lax.axis_size("col")
     rows = tokens.shape[1]
@@ -109,6 +111,254 @@
     return result.astype(BF)[None]
 
 
+def swap(value, axis, count, bit):
+    return lax.ppermute(value, axis, [(i, i ^ bit) for i in range(count)])
+
+
+def vmem_params():
+    return pltpu.CompilerParams(vmem_limit_bytes=24 * 2**20)
+
+
+def whole_specs(count):
+    return [pl.BlockSpec(memory_space=pltpu.VMEM)] * count
+
+
+def cost(flops, moved):
+    return pl.CostEstimate(flops=int(flops), bytes_accessed=int(moved), transcendentals=0)
+
+
+def norm_kernel(tokens_ref, gain_ref, out_ref):
+    rows = tokens_ref[0].astype(F32)
+    inverse_rms = lax.rsqrt(jnp.mean(rows * rows, axis=-1, keepdims=True) + EPS)
+    out_ref[...] = (rows * inverse_rms * gain_ref[...].astype(F32)).astype(BF)
+
+
+def norm_rows(tokens, gain):
+    rows, width = tokens.shape[1:]
+    step = rows // 6
+    return pl.pallas_call(
+        norm_kernel,
+        out_shape=jax.ShapeDtypeStruct((rows, width), BF),
+        grid=(rows // step,),
+        in_specs=[
+            pl.BlockSpec((1, step, width), lambda i: (0, i, 0)),
+            pl.BlockSpec((1, width), lambda i: (0, 0)),
+        ],
+        out_specs=pl.BlockSpec((step, width), lambda i: (i, 0)),
+        compiler_params=vmem_params(),
+        cost_estimate=cost(rows * width * 2000, rows * width * 4),
+        name="norm_rows",
+    )(tokens, gain.reshape(1, width))
+
+
+def project(me, normed, weight, split, half, into=None):
+    near, depth, columns = weight.shape
+    depth //= 2
+    rows = normed.shape[0]
+
+    def kernel(me_ref, normed_ref, weight_ref, split_ref, *rest):
+        out_ref = rest[-1]
+        upper = me_ref[0] // near
+        total = jnp.zeros((rows, columns), F32)
+        for s in range(near):
+            own = pl.multiple_of((upper * near + s) * depth, depth)
+            far = pl.multiple_of(((1 - upper) * near + s) * depth, depth)
+            piece = jnp.concatenate([normed_ref[:, pl.ds(own, depth)], normed_ref[:, pl.ds(far, depth)]], axis=1)
+            total = total + jnp.dot(piece, weight_ref[s], preferred_element_type=F32)
+        sums = dot(split_ref[...], total.astype(BF), ((1,), (1,)))
+        out_ref[...] = sums.astype(BF)
+
+    args = [me, normed, weight, split] + ([] if into is None else [into])
+    smem = pl.BlockSpec(memory_space=pltpu.SMEM)
+    extra = [] if into is None else [pl.BlockSpec(memory_space=pl.ANY)]
+    zero = lambda i: (0, 0)
+    return pl.pallas_call(
+        kernel,
+        out_shape=jax.ShapeDtypeStruct((2 * columns, rows), BF),
+        grid=(1,),
+        in_specs=[
+            smem,
+            pl.BlockSpec(normed.shape, zero),
+            pl.BlockSpec(weight.shape, lambda i: (0, 0, 0)),
+            pl.BlockSpec(split.shape, zero),
+        ]
+        + extra,
+        out_specs=pl.BlockSpec((columns, rows), lambda i: (half, 0)),
+        input_output_aliases={} if into is None else {4: 0},
+        compiler_params=vmem_params(),
+        cost_estimate=cost(2 * rows * near * 2 * depth * columns, weight.size * 2),
+        name="project",
+    )(*args)
+
+
+def transform_kernel(narrow, me_ref, got_ref, first_ref, cos_ref, sin_ref, second_ref, out_ref):
+    peers, _, rows = cos_ref.shape
+    stage = jnp.dot(first_ref[...], got_ref[...], preferred_element_type=F32)
+    stage = stage.reshape(2, peers, narrow, rows)
+    cos, sin = cos_ref[...], sin_ref[...]
+    real = stage[0] * cos + stage[1] * sin
+    imag = stage[1] * cos - stage[0] * sin
+    which = lax.broadcasted_iota(jnp.int32, (1, narrow, rows), 1) + me_ref[0] * narrow
+    sine = lax.rem(which, GS) > GS // 2
+    lead = jnp.where(sine, -imag, real).reshape(peers * narrow, rows).astype(BF)
+    tail = jnp.where(sine, real, imag).reshape(peers * narrow, rows).astype(BF)
+    lanes = ((1,), (1,))
+    out = dot(second_ref[:, :rows], lead, lanes) + dot(second_ref[:, rows:], tail, lanes)
+    out_ref[...] = out.astype(BF)
+
+
+def transform(me, got, peers, rows):
+    channels = got.shape[0]
+    narrow = channels // peers
+    small_cos, small_sin = angles(np.arange(peers), np.arange(peers), peers)
+    first = jnp.asarray(np.kron(np.concatenate([small_cos, -small_sin]), np.eye(narrow)), BF)
+    turn_cos, turn_sin = angles(np.arange(peers), np.arange(rows), rows * peers)
+    long_cos, long_sin = angles(np.arange(rows), np.arange(rows), rows)
+    second = jnp.asarray(np.concatenate([long_cos, long_sin], axis=1), BF)
+    turns = [jnp.asarray(t[:, None, :], F32) for t in (turn_cos, turn_sin)]
+
+    def kernel(*refs):
+        transform_kernel(narrow, *refs)
+
+    return pl.pallas_call(
+        kernel,
+        out_shape=jax.ShapeDtypeStruct((rows, channels), BF),
+        in_specs=[pl.BlockSpec(memory_space=pltpu.SMEM)] + whole_specs(5),
+        out_specs=pl.BlockSpec(memory_space=pltpu.VMEM),
+        compiler_params=vmem_params(),
+        cost_estimate=cost(4 * rows * channels * channels, 6 * channels * channels),
+        name="transform",
+    )(me, got, first, *turns, second)
+
+
+def regroup(quads, lane):
+    low, high = [], []
+    for j in range(2):
+        a, b = quads[j], quads[j + 2]
+        low.append(jnp.where(lane < 64, a, pltpu.roll(b, 64, 1)))
+        high.append(jnp.where(lane < 64, pltpu.roll(a, 64, 1), b))
+    out = []
+    even = lax.rem(lane, 64) < 32
+    for e, o in (low, high):
+        out.append(jnp.where(even, e, pltpu.roll(o, 32, 1)))
+        out.append(jnp.where(even, pltpu.roll(e, 96, 1), o))
+    return out
+
+
+def output_kernel(scale, depth, me_ref, back_ref, join_ref, *refs):
+    own, other, (out_ref, sheet) = refs[:8], refs[8:16], refs[16:]
+    peers, inner, channels = back_ref.shape
+    lane = lax.broadcasted_iota(jnp.int32, (inner, 128), 1)
+    quads = channels // 128
+    for a in range(quads):
+        made = []
+        for b in range(quads):
+            tiles = [back_ref[4 * b + j, :, 128 * a : 128 * a + 128].astype(F32) for j in range(4)]
+            made.append(regroup(tiles, lane))
+        for i in range(4):
+            for b in range(quads):
+                sheet[b, pl.ds(4 * a + i, inner, stride=peers), :] = made[b][i]
+    lines = jnp.concatenate([sheet[b].astype(BF) for b in range(quads)], axis=1)
+    mixed_real = jnp.dot(lines, join_ref[...], preferred_element_type=F32) * scale
+    mixed_real = mixed_real.astype(BF)
+    near = len(own)
+    upper = me_ref[0] // near
+    place = lax.rem(me_ref[0], near)
+    width = own[0].shape[2]
+    for m in range(near):
+        left = jnp.concatenate([own[m][0], own[m][1]], axis=1)
+        right = jnp.concatenate([other[m][0], other[m][1]], axis=1)
+        part = jnp.dot(mixed_real[:, :depth], left, preferred_element_type=F32)
+        part = part + jnp.dot(mixed_real[:, depth:], right, preferred_element_type=F32)
+        part = part.astype(BF)
+        at = lax.bitwise_xor(place, m)
+        here = pl.multiple_of((upper * near + at) * width, width)
+        there = pl.multiple_of(((1 - upper) * near + at) * width, width)
+        out_ref[:, pl.ds(here, width)] = part[:, :width]
+        out_ref[:, pl.ds(there, width)] = part[:, width:]
+
+
+def output(me, back, join, own, other, scale):
+    peers, inner, channels = back.shape
+    depth, width = own[0].shape[1:]
+    rows = peers * inner
+
+    def kernel(*refs):
+        output_kernel(scale, depth, *refs)
+
+    return pl.pallas_call(
+        kernel,
+        out_shape=jax.ShapeDtypeStruct((rows, width * peers), BF),
+        in_specs=[pl.BlockSpec(memory_space=pltpu.SMEM)] + whole_specs(2 + len(own) + len(other)),
+        out_specs=pl.BlockSpec(memory_space=pltpu.VMEM),
+        scratch_shapes=[pltpu.VMEM((channels // 128, rows, 128), F32)],
+        compiler_params=vmem_params(),
+        cost_estimate=cost(2 * rows * channels * width * peers, rows * width * peers * 2),
+        name="output",
+    )(me, back, join, *own, *other)
+
+
+def body_cube(tokens, norm_gain, in_weight, out_weight):
+    peers = lax.axis_size("row")
+    cols = lax.axis_size("col")
+    near = peers // 2
+    rows = tokens.shape[1]
+    channels = in_weight.shape[1] * cols
+    narrow = channels // peers
+    inner = rows // peers
+    me = lax.axis_index("row").astype(jnp.int32).reshape(1)
+    split, join = group_tables()
+    split_half = jnp.asarray(np.kron(np.eye(channels // cols // GS), split.T), BF)
+    join_all = jnp.asarray(np.kron(np.eye(channels // GS), join), BF)
+
+    def row_swap(value, bit):
+        return swap(value, "row", peers, bit)
+
+    def core_swap(value):
+        return swap(value, "col", cols, 1)
+
+    in_both = jnp.stack([in_weight, row_swap(in_weight, near)])
+    in_both = in_both.reshape(1, 2 * in_weight.shape[0], in_weight.shape[1])
+    groups = [list(range(near)), list(range(near, peers))]
+    in_own = lax.all_to_all(
+        jnp.broadcast_to(in_both, (near,) + in_both.shape[1:]),
+        "row",
+        split_axis=0,
+        concat_axis=0,
+        tiled=True,
+        axis_index_groups=groups,
+    )
+    normed = norm_rows(tokens, norm_gain)
+    in_other = core_swap(in_own)
+
+    pairs = {0: jnp.stack([out_weight, row_swap(out_weight, near)])}
+    for bit in (1, 2, 4):
+        pairs[bit] = row_swap(pairs[0], bit)
+    pairs[3] = row_swap(pairs[2], 1)
+    pairs[6] = row_swap(pairs[4], 2)
+    pairs[5] = row_swap(pairs[1], 4)
+    pairs[7] = row_swap(pairs[6], 1)
+    others = [core_swap(pairs[m]) for m in range(near)]
+
+    sums = project(me, normed, in_own, split_half, 0)
+    sums = project(me, normed, in_other, split_half, 1, sums)
+    got = lax.all_to_all(sums.reshape(peers, narrow, rows), "row", split_axis=0, concat_axis=0, tiled=True)
+    whole = transform(me, got.reshape(channels, rows), peers, rows)
+    back = lax.all_to_all(whole.reshape(peers, inner, channels), "row", split_axis=0, concat_axis=0, tiled=True)
+    scale = 1.0 / math.sqrt(rows * peers * GS)
+    result = output(me, back, join_all, [pairs[m] for m in range(near)], others, scale)
+    return result[None]
+
+
+def body(tokens, norm_gain, in_weight, out_weight):
+    peers, cols = lax.axis_size("row"), lax.axis_size("col")
+    channels = in_weight.shape[1] * cols
+    fits = tokens.shape[1] % (8 * peers) == 0 and in_weight.shape[0] % 128 == 0 and out_weight.shape[1] % 128 == 0
+    if peers == 16 and cols == 2 and channels == 32 * peers and fits:
+        return body_cube(tokens, norm_gain, in_weight, out_weight)
+    return body_general(tokens, norm_gain, in_weight, out_weight)
+
+
 def solution(mesh):
     in_specs = (P("col", "row", None), P(), P("row", "col"), P("col", "row"))
     out_specs = P("col", "row", None)

time: 98.4 us -> 89.4 us (0.909)
  blocking collectives: 18.4 us -> 36.6 us
  waiting for transfers between devices: 36 us -> 22.1 us
  matrix products: 11.9 us -> 0 us
  local copies, waits for them, and re-layouts: 9.74 us -> 1.53 us
  Pallas kernels: 0 us -> 8 us
    all_to_all x3 -> x1, waiting for transfers between devices: 21 us -> 0.01 us  [body_cube(): lax.all_to_all(whole.reshape(peers, inner, channels), 'row', split_axis=0...]
    all_to_all x1 -> x2, blocking collectives: 18.4 us -> 36.6 us  [the longest x1 18.4 us: body_cube(): lax.all_to_all(jnp.broadcast_to(in_both, (near,) + in_both.shape[1:]), 'r...]
    dot_general x8 -> x0, matrix products: 11.9 us -> none  [dot(): return lax.dot_general(a, b, (dims, ((), ())), preferred_element_type=F32)]
    all_to_all x3 -> x1, starting transfers between devices: 13 us -> 3.68 us  [body_cube(): lax.all_to_all(whole.reshape(peers, inner, channels), 'row', split_axis=0...]
    ppermute x4 -> x18, starting transfers between devices: 7.03 us -> 16 us  [swap(): return lax.ppermute(value, axis, [(i, i ^ bit) for i in range(count)])]
    pallas_call x0 -> x5, Pallas kernels: none -> 8 us  [the longest x1 3 us: output(): pl.pallas_call(kernel, out_shape=jax.ShapeDtypeStruct((rows, width * peer...]
    ppermute x4 -> x18, waiting for transfers between devices: 15 us -> 22.1 us  [swap(): return lax.ppermute(value, axis, [(i, i ^ bit) for i in range(count)])]
    reshape x2 -> x1, local copies, waits for them, and re-layouts: 2.36 us -> 0.01 us  [norm_rows(): gain.reshape(1, width)]
  transfers between devices with their start and end apart: 7 -> 19, of which waited for: 4 -> 7; matrix products, arithmetic and copies ran while one was open for 12% -> 0% of each run, Pallas kernels for 0% -> 2%
where the time goes in v2:
time: 89.4 us; the launch traced here: 89 us
  blocking collectives  36.6 us (41%)
  waiting for transfers between devices  22.1 us (25%)
  starting transfers between devices  19.7 us (22%)
  Pallas kernels  8 us (9%)
  local copies, waits for them, and re-layouts  1.53 us (2%)
    ppermute x18, waiting for transfers between devices, swap(): return lax.ppermute(value, axis, [(i, i ^ bit) for i in range(count)])  22.1 us
    all_to_all x1, blocking collectives, body_cube(): lax.all_to_all(jnp.broadcast_to(in_both, (near,) + in_both.shape[1:]), 'r...  18.4 us
    all_to_all x1, blocking collectives, body_cube(): lax.all_to_all(sums.reshape(peers, narrow, rows), 'row', split_axis=0, co...  18.2 us
    ppermute x18, starting transfers between devices, swap(): return lax.ppermute(value, axis, [(i, i ^ bit) for i in range(count)])  16 us
    all_to_all x1, starting transfers between devices, body_cube(): lax.all_to_all(whole.reshape(peers, inner, channels), 'row', split_axis=0...  3.68 us
    pallas_call x1, Pallas kernels, output(): pl.pallas_call(kernel, out_shape=jax.ShapeDtypeStruct((rows, width * peer...  3 us
    pallas_call x1, Pallas kernels, transform(): pl.pallas_call(kernel, out_shape=jax.ShapeDtypeStruct((rows, channels), B...  2.14 us
    pallas_call x2, Pallas kernels, project(): pl.pallas_call(kernel, out_shape=jax.ShapeDtypeStruct((2 * columns, rows)...  1.84 us
  transfers between devices with their start and end apart: 19, of which 7 were waited for; matrix products, arithmetic and copies ran while one was open for 0% of the time, Pallas kernels for 2%

profile of v2, /device:TPU:0, one launch (start us, length us, event | category | flops | bytes accessed | tf_op | source)
XLA Modules:
  0.0 89.0 jit_solution(7111854016327935141)
XLA Ops:
  0.0 4.1 %collective-permute-start = (bf16[128,256]{1,0:T(8,128)(2,1)}, bf16[128,256]{1,0:T(8,128)(2,1)S(1)}, u32[]{:S(2)}, u32[]{:S(2)}) collective-permute-start(bf16[128,256]{1,0:T(8,128)(2,1)} %param.12), channel_id=1, source_target_pairs={{0,16},{2,18},{4,20},{6,22},{8,24},{10,26},{12,28},{14,30},{16,0},... | collective-permute-start | bytes 196616 | tf_op jit(solution)/shard_map/ppermute | solution.py:115
  4.1 3.9 %collective-permute-done = bf16[128,256]{1,0:T(8,128)(2,1)S(1)} collective-permute-done((bf16[128,256]{1,0:T(8,128)(2,1)}, bf16[128,256]{1,0:T(8,128)(2,1)S(1)}, u32[]{:S(2)}, u32[]{:S(2)}) %collective-permute-start) | collective-permute-done | bytes 65568 | tf_op jit(solution)/shard_map/ppermute | solution.py:115
  7.9 0.9 pad_maximum_fusion
  8.8 0.1 broadcast_in_dim.11
  8.9 18.4 %all_to_all.15.weight_ref = bf16[8,256,256]{2,1,0:T(8,128)(2,1)S(1)} all-to-all(bf16[8,256,256]{2,1,0:T(8,128)(2,1)S(1)} %broadcast_in_dim.11), channel_id=1, replica_groups={{0,2,4,6,8,10,12,14},{16,18,20,22,24,26,28,30},{1,3,5,7,9,11,13,15},{17..., dimensions={0} | all-to-all | bytes 2097152 | tf_op jit(solution)/shard_map/all_to_all | solution.py:323
  27.3 1.4 %copy-done.6 = bf16[1,384,2048]{2,1,0:T(8,128)(2,1)S(1)} copy-done((bf16[1,384,2048]{2,1,0:T(8,128)(2,1)S(1)}, bf16[1,384,2048]{2,1,0:T(8,128)(2,1)}, u32[]{:S(2)}) %copy-start.6) | copy-done | bytes 1572888
  28.7 1.0 %norm_rows.1.normed_ref = bf16[384,2048]{1,0:T(8,128)(2,1)S(1)} custom-call(bf16[1,384,2048]{2,1,0:T(8,128)(2,1)S(1)} %copy-done.6, bf16[1,2048]{1,0:T(2,128)(2,1)S(1)} %reshape.18.gain_ref), custom_call_target="tpu_custom_call" | custom-call | flops 1572864000 | bytes 3145728 | tf_op jit(solution)/shard_map/norm_rows/pallas_call | solution.py:139
  29.7 0.9 %project.2.rest_0_ = bf16[512,384]{1,0:T(8,128)(2,1)S(1)} custom-call(s32[1]{0:T(128)} %bitcast.me_ref.refs_0_, bf16[384,2048]{1,0:T(8,128)(2,1)S(1)} %norm_rows.1.normed_ref, bf16[8,256,256]{2,1,0:T(8,128)(2,1)S(1)} %all_to_all.15.weight_ref, bf16[256,256]{1,0:T(8,128)(2,1)S(1)} %copy-done.3), custom_call_target="tpu_custom_call" | custom-call | flops 402653184 | bytes 1048576 | tf_op jit(solution)/shard_map/project/pallas_call | solution.py:175
  30.6 0.0 copy-start
  30.7 0.0 copy-start.1
  30.7 0.9 %project.3 = bf16[512,384]{1,0:T(8,128)(2,1)S(1)} custom-call(s32[1]{0:T(128)} %bitcast.me_ref.refs_0_, bf16[384,2048]{1,0:T(8,128)(2,1)S(1)} %norm_rows.1.normed_ref, bf16[8,256,256]{2,1,0:T(8,128)(2,1)S(1)} %collective-permute-done.1.weight_ref, bf16[256,256]{1,0:T(8,128)(2,1)S(1)} %copy-done.3, ...), custom_call_target="tpu_custom_call", output_to_operand_aliasing={{}: (4, {})} | custom-call | flops 402653184 | bytes 1048576 | tf_op jit(solution)/shard_map/project/pallas_call | solution.py:175
  31.6 18.2 %all_to_all.16 = bf16[16,32,384]{2,1,0:T(8,128)(2,1)S(1)} all-to-all(bf16[16,32,384]{2,1,0:T(8,128)(2,1)S(1)} %bitcast.10), channel_id=1, replica_groups=mesh['row'=16,'col'=2] {'row'}, dimensions={0} | all-to-all | bytes 786432 | tf_op jit(solution)/shard_map/all_to_all | solution.py:345
  49.9 2.1 %transform.1 = bf16[384,512]{1,0:T(8,128)(2,1)} custom-call(s32[1]{0:T(128)} %bitcast.me_ref.refs_0_, bf16[512,384]{1,0:T(8,128)(2,1)S(1)} %bitcast.11, bf16[1024,512]{1,0:T(8,128)(2,1)S(1)} %copy-done, f32[16,1,384]{2,1,0:T(1,128)S(1)} %copy-done.4, f32[16,1,384]{2,1,0:T(1,128)S(1)} %copy-done.5, bf16[384,768]{1,0:T(8,128)(2,1)S(1)} %copy-done.1), custom_call_target="tpu_custom_call" | custom-call | flops 402653184 | bytes 1572864 | tf_op jit(solution)/shard_map/transform/pallas_call | solution.py:223
  52.0 3.7 %all-to-all-start.2 = ((bf16[16,24,512]{2,1,0:T(8,128)(2,1)}), bf16[16,24,512]{2,1,0:T(8,128)(2,1)S(1)}, u32[]{:S(2)}, u32[]{:S(2)}) async-start(bf16[16,24,512]{2,1,0:T(8,128)(2,1)} %bitcast.6), calls=%async_computation.2 | async-start | bytes 786432 | tf_op jit(solution)/shard_map/all_to_all | solution.py:347
  55.7 2.9 %collective-permute-start.2 = (bf16[256,128]{1,0:T(8,128)(2,1)S(1)}, bf16[256,128]{1,0:T(8,128)(2,1)S(1)}, u32[]{:S(2)}, u32[]{:S(2)}) collective-permute-start(bf16[256,128]{1,0:T(8,128)(2,1)S(1)} %copy-done.7), channel_id=1, source_target_pairs={{0,16},{2,18},{4,20},{6,22},{8,24},{10,26},{12,28},{14,30},{16,0},... | collective-permute-start | bytes 196616 | tf_op jit(solution)/shard_map/ppermute | solution.py:115
  58.6 11.0 %collective-permute-done.2 = bf16[256,128]{1,0:T(8,128)(2,1)S(1)} collective-permute-done((bf16[256,128]{1,0:T(8,128)(2,1)S(1)}, bf16[256,128]{1,0:T(8,128)(2,1)S(1)}, u32[]{:S(2)}, u32[]{:S(2)}) %collective-permute-start.2) | collective-permute-done | bytes 65568 | tf_op jit(solution)/shard_map/ppermute | solution.py:115
  69.6 0.1 collective-permute-start.6
  69.7 1.5 %collective-permute-start.4 = (bf16[2,256,128]{2,1,0:T(8,128)(2,1)S(1)}, bf16[2,256,128]{2,1,0:T(8,128)(2,1)S(1)}, u32[]{:S(2)}, u32[]{:S(2)}) collective-permute-start(bf16[2,256,128]{2,1,0:T(8,128)(2,1)S(1)} %pad_maximum_fusion.1.refs_3_), channel_id=1, source_target_pairs={{0,4},{2,6},{4,0},{6,2},{8,12},{10,14},{12,8},{14,10},{16,20},{18,... | collective-permute-start | bytes 393224 | tf_op jit(solution)/shard_map/ppermute | solution.py:115
  71.2 1.5 %collective-permute-start.3 = (bf16[2,256,128]{2,1,0:T(8,128)(2,1)S(1)}, bf16[2,256,128]{2,1,0:T(8,128)(2,1)S(1)}, u32[]{:S(2)}, u32[]{:S(2)}) collective-permute-start(bf16[2,256,128]{2,1,0:T(8,128)(2,1)S(1)} %pad_maximum_fusion.1.refs_3_), channel_id=1, source_target_pairs={{0,2},{2,0},{4,6},{6,4},{8,10},{10,8},{12,14},{14,12},{16,18},{18,... | collective-permute-start | bytes 393224 | tf_op jit(solution)/shard_map/ppermute | solution.py:115
  72.7 2.0 %collective-permute-done.6.refs_7_ = bf16[2,256,128]{2,1,0:T(8,128)(2,1)S(1)} collective-permute-done((bf16[2,256,128]{2,1,0:T(8,128)(2,1)S(1)}, bf16[2,256,128]{2,1,0:T(8,128)(2,1)S(1)}, u32[]{:S(2)}, u32[]{:S(2)}) %collective-permute-start.6) | collective-permute-done | bytes 131104 | tf_op jit(solution)/shard_map/ppermute | solution.py:115
  74.7 1.4 %collective-permute-start.8 = (bf16[2,256,128]{2,1,0:T(8,128)(2,1)S(1)}, bf16[2,256,128]{2,1,0:T(8,128)(2,1)S(1)}, u32[]{:S(2)}, u32[]{:S(2)}) collective-permute-start(bf16[2,256,128]{2,1,0:T(8,128)(2,1)S(1)} %collective-permute-done.6.refs_7_), channel_id=1, source_target_pairs={{0,4},{2,6},{4,0},{6,2},{8,12},{10,14},{12,8},{14,10},{16,20},{18,... | collective-permute-start | bytes 393224 | tf_op jit(solution)/shard_map/ppermute | solution.py:115
  76.1 1.5 %collective-permute-start.5 = (bf16[2,256,128]{2,1,0:T(8,128)(2,1)S(1)}, bf16[2,256,128]{2,1,0:T(8,128)(2,1)S(1)}, u32[]{:S(2)}, u32[]{:S(2)}) collective-permute-start(bf16[2,256,128]{2,1,0:T(8,128)(2,1)S(1)} %collective-permute-done.4.refs_5_), channel_id=1, source_target_pairs={{0,2},{2,0},{4,6},{6,4},{8,10},{10,8},{12,14},{14,12},{16,18},{18,... | collective-permute-start | bytes 393224 | tf_op jit(solution)/shard_map/ppermute | solution.py:115
  77.5 0.6 collective-permute-start.7
  78.2 0.5 collective-permute-start.12
  78.7 0.9 %collective-permute-done.8.refs_9_ = bf16[2,256,128]{2,1,0:T(8,128)(2,1)S(1)} collective-permute-done((bf16[2,256,128]{2,1,0:T(8,128)(2,1)S(1)}, bf16[2,256,128]{2,1,0:T(8,128)(2,1)S(1)}, u32[]{:S(2)}, u32[]{:S(2)}) %collective-permute-start.8) | collective-permute-done | bytes 131104 | tf_op jit(solution)/shard_map/ppermute | solution.py:115
  79.6 1.5 %collective-permute-start.9 = (bf16[2,256,128]{2,1,0:T(8,128)(2,1)S(1)}, bf16[2,256,128]{2,1,0:T(8,128)(2,1)S(1)}, u32[]{:S(2)}, u32[]{:S(2)}) collective-permute-start(bf16[2,256,128]{2,1,0:T(8,128)(2,1)S(1)} %collective-permute-done.8.refs_9_), channel_id=1, source_target_pairs={{0,2},{2,0},{4,6},{6,4},{8,10},{10,8},{12,14},{14,12},{16,18},{18,... | collective-permute-start | bytes 393224 | tf_op jit(solution)/shard_map/ppermute | solution.py:115
  81.1 1.4 %collective-permute-done.7.refs_8_ = bf16[2,256,128]{2,1,0:T(8,128)(2,1)S(1)} collective-permute-done((bf16[2,256,128]{2,1,0:T(8,128)(2,1)S(1)}, bf16[2,256,128]{2,1,0:T(8,128)(2,1)S(1)}, u32[]{:S(2)}, u32[]{:S(2)}) %collective-permute-start.7) | collective-permute-done | bytes 131104 | tf_op jit(solution)/shard_map/ppermute | solution.py:115
  82.5 0.5 collective-permute-start.13
  83.0 0.1 collective-permute-start.15
  83.1 1.6 %collective-permute-done.9.refs_10_ = bf16[2,256,128]{2,1,0:T(8,128)(2,1)S(1)} collective-permute-done((bf16[2,256,128]{2,1,0:T(8,128)(2,1)S(1)}, bf16[2,256,128]{2,1,0:T(8,128)(2,1)S(1)}, u32[]{:S(2)}, u32[]{:S(2)}) %collective-permute-start.9) | collective-permute-done | bytes 131104 | tf_op jit(solution)/shard_map/ppermute | solution.py:115
  84.7 1.3 %collective-permute-done.17.refs_18_ = bf16[2,256,128]{2,1,0:T(8,128)(2,1)S(1)} collective-permute-done((bf16[2,256,128]{2,1,0:T(8,128)(2,1)S(1)}, bf16[2,256,128]{2,1,0:T(8,128)(2,1)S(1)}, u32[]{:S(2)}, u32[]{:S(2)}) %collective-permute-start.17) | collective-permute-done | bytes 131104 | tf_op jit(solution)/shard_map/ppermute | solution.py:115
  86.0 3.0 %output.1 = bf16[384,2048]{1,0:T(8,128)(2,1)} custom-call(s32[1]{0:T(128)} %bitcast.me_ref.refs_0_, bf16[16,24,512]{2,1,0:T(8,128)(2,1)S(1)} %all-to-all-done.2.refs_1_, bf16[512,512]{1,0:T(8,128)(2,1)S(1)} %copy-done.2, bf16[2,256,128]{2,1,0:T(8,128)(2,1)S(1)} %pad_maximum_fusion.1.refs_3_, bf16[2,256,128]{2,1,0:T(8,128)(2,1)S(1)} %collective-permute-done.3.refs_4_, ...), custom_call_target="tpu_custom_call" | custom-call | flops 805306368 | bytes 1572864 | tf_op jit(solution)/shard_map/output/pallas_call | solution.py:289
  (35 shorter events, 0.1 us)
Async XLA Ops:
  0.0 7.9 %collective-permute-start = (bf16[128,256]{1,0:T(8,128)(2,1)}, bf16[128,256]{1,0:T(8,128)(2,1)S(1)}, u32[]{:S(2)}, u32[]{:S(2)}) collective-permute-start(bf16[128,256]{1,0:T(8,128)(2,1)} %param.12), channel_id=1, source_target_pairs={{0,16},{2,18},{4,20},{6,22},{8,24},{10,26},{12,28},{14,30},{16,0},... | collective-permute-start | bytes 196616 | tf_op jit(solution)/shard_map/ppermute | solution.py:115
  8.8 18.5 %copy-start.8 = (bf16[2048]{0:T(1024)(128)(2,1)S(1)}, bf16[2048]{0:T(1024)(128)(2,1)}, u32[]{:S(2)}) copy-start(bf16[2048]{0:T(1024)(128)(2,1)} %param.11) | copy-start | bytes 12292
  27.2 3.5 %collective-permute-start.1 = (bf16[8,256,256]{2,1,0:T(8,128)(2,1)S(1)}, bf16[8,256,256]{2,1,0:T(8,128)(2,1)S(1)}, u32[]{:S(2)}, u32[]{:S(2)}) collective-permute-start(bf16[8,256,256]{2,1,0:T(8,128)(2,1)S(1)} %all_to_all.15.weight_ref), channel_id=1, source_target_pairs={{0,1},{1,0},{2,3},{3,2},{4,5},{5,4},{6,7},{7,6},{8,9},{9,8},{10,11... | collective-permute-start | bytes 3145736 | tf_op jit(solution)/shard_map/ppermute | solution.py:115
  27.3 1.4 %copy-start.6 = (bf16[1,384,2048]{2,1,0:T(8,128)(2,1)S(1)}, bf16[1,384,2048]{2,1,0:T(8,128)(2,1)}, u32[]{:S(2)}) copy-start(bf16[1,384,2048]{2,1,0:T(8,128)(2,1)} %tokens_ref.1) | copy-start | bytes 4718596
  28.7 1.0 %copy-start.3 = (bf16[256,256]{1,0:T(8,128)(2,1)S(1)}, bf16[256,256]{1,0:T(8,128)(2,1)}, u32[]{:S(2)}) copy-start(bf16[256,256]{1,0:T(8,128)(2,1)} %constant.18.clone.split_ref) | copy-start | bytes 393220
  30.6 19.2 %copy-start = (bf16[1024,512]{1,0:T(8,128)(2,1)S(1)}, bf16[1024,512]{1,0:T(8,128)(2,1)}, u32[]{:S(2)}) copy-start(bf16[1024,512]{1,0:T(8,128)(2,1)} %constant.20.clone.refs_2_) | copy-start | bytes 3145732
  30.7 19.2 %copy-start.1 = (bf16[384,768]{1,0:T(8,128)(2,1)S(1)}, bf16[384,768]{1,0:T(8,128)(2,1)}, u32[]{:S(2)}) copy-start(bf16[384,768]{1,0:T(8,128)(2,1)} %constant.21.clone.refs_5_) | copy-start | bytes 1769476
  30.7 19.2 %copy-start.4 = (f32[16,1,384]{2,1,0:T(1,128)S(1)}, f32[16,1,384]{2,1,0:T(1,128)}, u32[]{:S(2)}) copy-start(f32[16,1,384]{2,1,0:T(1,128)} %constant.22.clone.refs_3_) | copy-start | bytes 73732
  30.7 19.2 %copy-start.5 = (f32[16,1,384]{2,1,0:T(1,128)S(1)}, f32[16,1,384]{2,1,0:T(1,128)}, u32[]{:S(2)}) copy-start(f32[16,1,384]{2,1,0:T(1,128)} %constant.23.clone.refs_4_) | copy-start | bytes 73732
  49.9 5.8 %copy-start.7 = (bf16[256,128]{1,0:T(8,128)(2,1)S(1)}, bf16[256,128]{1,0:T(8,128)(2,1)}, u32[]{:S(2)}) copy-start(bf16[256,128]{1,0:T(8,128)(2,1)} %param.13) | copy-start | bytes 196612
  49.9 36.1 %copy-start.2 = (bf16[512,512]{1,0:T(8,128)(2,1)S(1)}, bf16[512,512]{1,0:T(8,128)(2,1)}, u32[]{:S(2)}) copy-start(bf16[512,512]{1,0:T(8,128)(2,1)} %constant.19.clone.refs_2_) | copy-start | bytes 1572868
  52.0 34.0 %all-to-all-start.2 = ((bf16[16,24,512]{2,1,0:T(8,128)(2,1)}), bf16[16,24,512]{2,1,0:T(8,128)(2,1)S(1)}, u32[]{:S(2)}, u32[]{:S(2)}) async-start(bf16[16,24,512]{2,1,0:T(8,128)(2,1)} %bitcast.6), calls=%async_computation.2 | async-start | bytes 786432 | tf_op jit(solution)/shard_map/all_to_all | solution.py:347
  55.7 13.9 %collective-permute-start.2 = (bf16[256,128]{1,0:T(8,128)(2,1)S(1)}, bf16[256,128]{1,0:T(8,128)(2,1)S(1)}, u32[]{:S(2)}, u32[]{:S(2)}) collective-permute-start(bf16[256,128]{1,0:T(8,128)(2,1)S(1)} %copy-done.7), channel_id=1, source_target_pairs={{0,16},{2,18},{4,20},{6,22},{8,24},{10,26},{12,28},{14,30},{16,0},... | collective-permute-start | bytes 196616 | tf_op jit(solution)/shard_map/ppermute | solution.py:115
  69.6 5.0 %collective-permute-start.6 = (bf16[2,256,128]{2,1,0:T(8,128)(2,1)S(1)}, bf16[2,256,128]{2,1,0:T(8,128)(2,1)S(1)}, u32[]{:S(2)}, u32[]{:S(2)}) collective-permute-start(bf16[2,256,128]{2,1,0:T(8,128)(2,1)S(1)} %pad_maximum_fusion.1.refs_3_), channel_id=1, source_target_pairs={{0,8},{2,10},{4,12},{6,14},{8,0},{10,2},{12,4},{14,6},{16,24},{18,... | collective-permute-start | bytes 393224 | tf_op jit(solution)/shard_map/ppermute | solution.py:115
  69.7 6.4 %collective-permute-start.4 = (bf16[2,256,128]{2,1,0:T(8,128)(2,1)S(1)}, bf16[2,256,128]{2,1,0:T(8,128)(2,1)S(1)}, u32[]{:S(2)}, u32[]{:S(2)}) collective-permute-start(bf16[2,256,128]{2,1,0:T(8,128)(2,1)S(1)} %pad_maximum_fusion.1.refs_3_), channel_id=1, source_target_pairs={{0,4},{2,6},{4,0},{6,2},{8,12},{10,14},{12,8},{14,10},{16,20},{18,... | collective-permute-start | bytes 393224 | tf_op jit(solution)/shard_map/ppermute | solution.py:115
  71.2 6.4 %collective-permute-start.3 = (bf16[2,256,128]{2,1,0:T(8,128)(2,1)S(1)}, bf16[2,256,128]{2,1,0:T(8,128)(2,1)S(1)}, u32[]{:S(2)}, u32[]{:S(2)}) collective-permute-start(bf16[2,256,128]{2,1,0:T(8,128)(2,1)S(1)} %pad_maximum_fusion.1.refs_3_), channel_id=1, source_target_pairs={{0,2},{2,0},{4,6},{6,4},{8,10},{10,8},{12,14},{14,12},{16,18},{18,... | collective-permute-start | bytes 393224 | tf_op jit(solution)/shard_map/ppermute | solution.py:115
  72.6 5.5 %collective-permute-start.10 = (bf16[2,256,128]{2,1,0:T(8,128)(2,1)S(1)}, bf16[2,256,128]{2,1,0:T(8,128)(2,1)S(1)}, u32[]{:S(2)}, u32[]{:S(2)}) collective-permute-start(bf16[2,256,128]{2,1,0:T(8,128)(2,1)S(1)} %pad_maximum_fusion.1.refs_3_), channel_id=1, source_target_pairs={{0,1},{1,0},{2,3},{3,2},{4,5},{5,4},{6,7},{7,6},{8,9},{9,8},{10,11... | collective-permute-start | bytes 393224 | tf_op jit(solution)/shard_map/ppermute | solution.py:115
  74.7 5.0 %collective-permute-start.8 = (bf16[2,256,128]{2,1,0:T(8,128)(2,1)S(1)}, bf16[2,256,128]{2,1,0:T(8,128)(2,1)S(1)}, u32[]{:S(2)}, u32[]{:S(2)}) collective-permute-start(bf16[2,256,128]{2,1,0:T(8,128)(2,1)S(1)} %collective-permute-done.6.refs_7_), channel_id=1, source_target_pairs={{0,4},{2,6},{4,0},{6,2},{8,12},{10,14},{12,8},{14,10},{16,20},{18,... | collective-permute-start | bytes 393224 | tf_op jit(solution)/shard_map/ppermute | solution.py:115
  76.1 5.0 %collective-permute-start.5 = (bf16[2,256,128]{2,1,0:T(8,128)(2,1)S(1)}, bf16[2,256,128]{2,1,0:T(8,128)(2,1)S(1)}, u32[]{:S(2)}, u32[]{:S(2)}) collective-permute-start(bf16[2,256,128]{2,1,0:T(8,128)(2,1)S(1)} %collective-permute-done.4.refs_5_), channel_id=1, source_target_pairs={{0,2},{2,0},{4,6},{6,4},{8,10},{10,8},{12,14},{14,12},{16,18},{18,... | collective-permute-start | bytes 393224 | tf_op jit(solution)/shard_map/ppermute | solution.py:115
  77.5 5.0 %collective-permute-start.7 = (bf16[2,256,128]{2,1,0:T(8,128)(2,1)S(1)}, bf16[2,256,128]{2,1,0:T(8,128)(2,1)S(1)}, u32[]{:S(2)}, u32[]{:S(2)}) collective-permute-start(bf16[2,256,128]{2,1,0:T(8,128)(2,1)S(1)} %collective-permute-done.3.refs_4_), channel_id=1, source_target_pairs={{0,8},{2,10},{4,12},{6,14},{8,0},{10,2},{12,4},{14,6},{16,24},{18,... | collective-permute-start | bytes 393224 | tf_op jit(solution)/shard_map/ppermute | solution.py:115
  78.2 4.4 %collective-permute-start.11 = (bf16[2,256,128]{2,1,0:T(8,128)(2,1)S(1)}, bf16[2,256,128]{2,1,0:T(8,128)(2,1)S(1)}, u32[]{:S(2)}, u32[]{:S(2)}) collective-permute-start(bf16[2,256,128]{2,1,0:T(8,128)(2,1)S(1)} %collective-permute-done.3.refs_4_), channel_id=1, source_target_pairs={{0,1},{1,0},{2,3},{3,2},{4,5},{5,4},{6,7},{7,6},{8,9},{9,8},{10,11... | collective-permute-start | bytes 393224 | tf_op jit(solution)/shard_map/ppermute | solution.py:115
  78.2 4.9 %collective-permute-start.12 = (bf16[2,256,128]{2,1,0:T(8,128)(2,1)S(1)}, bf16[2,256,128]{2,1,0:T(8,128)(2,1)S(1)}, u32[]{:S(2)}, u32[]{:S(2)}) collective-permute-start(bf16[2,256,128]{2,1,0:T(8,128)(2,1)S(1)} %collective-permute-done.4.refs_5_), channel_id=1, source_target_pairs={{0,1},{1,0},{2,3},{3,2},{4,5},{5,4},{6,7},{7,6},{8,9},{9,8},{10,11... | collective-permute-start | bytes 393224 | tf_op jit(solution)/shard_map/ppermute | solution.py:115
  79.6 5.0 %collective-permute-start.9 = (bf16[2,256,128]{2,1,0:T(8,128)(2,1)S(1)}, bf16[2,256,128]{2,1,0:T(8,128)(2,1)S(1)}, u32[]{:S(2)}, u32[]{:S(2)}) collective-permute-start(bf16[2,256,128]{2,1,0:T(8,128)(2,1)S(1)} %collective-permute-done.8.refs_9_), channel_id=1, source_target_pairs={{0,2},{2,0},{4,6},{6,4},{8,10},{10,8},{12,14},{14,12},{16,18},{18,... | collective-permute-start | bytes 393224 | tf_op jit(solution)/shard_map/ppermute | solution.py:115
  81.1 3.6 %collective-permute-start.14 = (bf16[2,256,128]{2,1,0:T(8,128)(2,1)S(1)}, bf16[2,256,128]{2,1,0:T(8,128)(2,1)S(1)}, u32[]{:S(2)}, u32[]{:S(2)}) collective-permute-start(bf16[2,256,128]{2,1,0:T(8,128)(2,1)S(1)} %collective-permute-done.6.refs_7_), channel_id=1, source_target_pairs={{0,1},{1,0},{2,3},{3,2},{4,5},{5,4},{6,7},{7,6},{8,9},{9,8},{10,11... | collective-permute-start | bytes 393224 | tf_op jit(solution)/shard_map/ppermute | solution.py:115
  82.5 2.2 %collective-permute-start.16 = (bf16[2,256,128]{2,1,0:T(8,128)(2,1)S(1)}, bf16[2,256,128]{2,1,0:T(8,128)(2,1)S(1)}, u32[]{:S(2)}, u32[]{:S(2)}) collective-permute-start(bf16[2,256,128]{2,1,0:T(8,128)(2,1)S(1)} %collective-permute-done.8.refs_9_), channel_id=1, source_target_pairs={{0,1},{1,0},{2,3},{3,2},{4,5},{5,4},{6,7},{7,6},{8,9},{9,8},{10,11... | collective-permute-start | bytes 393224 | tf_op jit(solution)/shard_map/ppermute | solution.py:115
  82.5 2.1 %collective-permute-start.13 = (bf16[2,256,128]{2,1,0:T(8,128)(2,1)S(1)}, bf16[2,256,128]{2,1,0:T(8,128)(2,1)S(1)}, u32[]{:S(2)}, u32[]{:S(2)}) collective-permute-start(bf16[2,256,128]{2,1,0:T(8,128)(2,1)S(1)} %collective-permute-done.5.refs_6_), channel_id=1, source_target_pairs={{0,1},{1,0},{2,3},{3,2},{4,5},{5,4},{6,7},{7,6},{8,9},{9,8},{10,11... | collective-permute-start | bytes 393224 | tf_op jit(solution)/shard_map/ppermute | solution.py:115
  83.0 1.6 %collective-permute-start.15 = (bf16[2,256,128]{2,1,0:T(8,128)(2,1)S(1)}, bf16[2,256,128]{2,1,0:T(8,128)(2,1)S(1)}, u32[]{:S(2)}, u32[]{:S(2)}) collective-permute-start(bf16[2,256,128]{2,1,0:T(8,128)(2,1)S(1)} %collective-permute-done.7.refs_8_), channel_id=1, source_target_pairs={{0,1},{1,0},{2,3},{3,2},{4,5},{5,4},{6,7},{7,6},{8,9},{9,8},{10,11... | collective-permute-start | bytes 393224 | tf_op jit(solution)/shard_map/ppermute | solution.py:115
  84.7 1.3 %collective-permute-start.17 = (bf16[2,256,128]{2,1,0:T(8,128)(2,1)S(1)}, bf16[2,256,128]{2,1,0:T(8,128)(2,1)S(1)}, u32[]{:S(2)}, u32[]{:S(2)}) collective-permute-start(bf16[2,256,128]{2,1,0:T(8,128)(2,1)S(1)} %collective-permute-done.9.refs_10_), channel_id=1, source_target_pairs={{0,1},{1,0},{2,3},{3,2},{4,5},{5,4},{6,7},{7,6},{8,9},{9,8},{10,11... | collective-permute-start | bytes 393224 | tf_op jit(solution)/shard_map/ppermute | solution.py:115

commit v3 on v2

--- a/solution.py
+++ b/solution.py
@@ -7,6 +7,7 @@
 from jax.experimental import pallas as pl
 from jax.experimental.pallas import tpu as pltpu
 from jax.sharding import PartitionSpec as P
+
 
 GS = 64
 EPS = 1e-06
@@ -246,7 +247,12 @@
 
 
 def output_kernel(scale, depth, me_ref, back_ref, join_ref, *refs):
-    own, other, (out_ref, sheet) = refs[:8], refs[8:16], refs[16:]
+    own, (other_a, other_b, other_c), (out_ref, sheet) = refs[:8], refs[8:11], refs[11:]
+    other = {7: other_c}
+    for i, m in enumerate((0, 1, 2, 4)):
+        other[m] = other_a.at[2 * i : 2 * i + 2]
+    for i, m in enumerate((3, 5, 6)):
+        other[m] = other_b.at[2 * i : 2 * i + 2]
     peers, inner, channels = back_ref.shape
     lane = lax.broadcasted_iota(jnp.int32, (inner, 128), 1)
     quads = channels // 128
@@ -331,14 +337,17 @@
     normed = norm_rows(tokens, norm_gain)
     in_other = core_swap(in_own)
 
-    pairs = {0: jnp.stack([out_weight, row_swap(out_weight, near)])}
+    out_far = row_swap(out_weight, near)
+    pairs = {0: jnp.stack([out_weight, out_far])}
     for bit in (1, 2, 4):
         pairs[bit] = row_swap(pairs[0], bit)
     pairs[3] = row_swap(pairs[2], 1)
     pairs[6] = row_swap(pairs[4], 2)
     pairs[5] = row_swap(pairs[1], 4)
     pairs[7] = row_swap(pairs[6], 1)
-    others = [core_swap(pairs[m]) for m in range(near)]
+    first = jnp.concatenate([pairs[m] for m in (0, 1, 2, 4)])
+    second = jnp.concatenate([pairs[m] for m in (3, 5, 6)])
+    others = [core_swap(value) for value in (first, second, pairs[7])]
 
     sums = project(me, normed, in_own, split_half, 0)
     sums = project(me, normed, in_other, split_half, 1, sums)

time: 89.4 us -> 83.1 us (0.930)
  blocking collectives: 36.6 us -> 18.4 us
  waiting for transfers between devices: 22.1 us -> 26.1 us
  starting transfers between devices: 19.7 us -> 23 us
  local copies, waits for them, and re-layouts: 1.53 us -> 4.77 us
  Pallas kernels: 8 us -> 9.32 us
    all_to_all x1 -> x0, blocking collectives: 18.2 us -> none  [body_cube(): lax.all_to_all(sums.reshape(peers, narrow, rows), 'row', split_axis=0, co...]
    all_to_all x0 -> x1, starting transfers between devices: none -> 5.34 us  [body_cube(): lax.all_to_all(sums.reshape(peers, narrow, rows), 'row', split_axis=0, co...]
    ppermute x18 -> x13, waiting for transfers between devices: 22.1 us -> 26.1 us  [swap(): return lax.ppermute(value, axis, [(i, i ^ bit) for i in range(count)])]
    ppermute x18 -> x13, starting transfers between devices: 16 us -> 13.3 us  [swap(): return lax.ppermute(value, axis, [(i, i ^ bit) for i in range(count)])]
    unnamed x18 -> x22, local copies, waits for them, and re-layouts: 1.45 us -> 4.03 us
    pallas_call x2, Pallas kernels: 1.84 us -> 3.19 us  [project(): pl.pallas_call(kernel, out_shape=jax.ShapeDtypeStruct((2 * columns, rows)...]
  transfers between devices with their start and end apart: 19 -> 15, of which waited for: 7 -> 6; matrix products, arithmetic and copies ran while one was open for 0% -> 4% of each run, Pallas kernels for 2% -> 6%
where the time goes in v3:
time: 83.1 us; the launch traced here: 82.6 us
  waiting for transfers between devices  26.1 us (31%)
  starting transfers between devices  23 us (28%)
  blocking collectives  18.4 us (22%)
  Pallas kernels  9.32 us (11%)
  local copies, waits for them, and re-layouts  4.77 us (6%)
  other arithmetic  0.91 us (1%)
    ppermute x13, waiting for transfers between devices, swap(): return lax.ppermute(value, axis, [(i, i ^ bit) for i in range(count)])  26.1 us
    all_to_all x1, blocking collectives, body_cube(): lax.all_to_all(jnp.broadcast_to(in_both, (near,) + in_both.shape[1:]), 'r...  18.4 us
    ppermute x13, starting transfers between devices, swap(): return lax.ppermute(value, axis, [(i, i ^ bit) for i in range(count)])  13.3 us
    all_to_all x1, starting transfers between devices, body_cube(): lax.all_to_all(sums.reshape(peers, narrow, rows), 'row', split_axis=0, co...  5.34 us
    all_to_all x1, starting transfers between devices, body_cube(): lax.all_to_all(whole.reshape(peers, inner, channels), 'row', split_axis=0...  4.37 us
    unnamed x22, local copies, waits for them, and re-layouts  4.03 us
    pallas_call x2, Pallas kernels, project(): pl.pallas_call(kernel, out_shape=jax.ShapeDtypeStruct((2 * columns, rows)...  3.19 us
    pallas_call x1, Pallas kernels, output(): pl.pallas_call(kernel, out_shape=jax.ShapeDtypeStruct((rows, width * peer...  3 us
  transfers between devices with their start and end apart: 15, of which 6 were waited for; matrix products, arithmetic and copies ran while one was open for 4% of the time, Pallas kernels for 6%

profile of v3, /device:TPU:0, one launch (start us, length us, event | category | flops | bytes accessed | tf_op | source)
XLA Modules:
  0.0 82.6 jit_solution(4471772997102931718)
XLA Ops:
  0.0 4.1 %collective-permute-start = (bf16[128,256]{1,0:T(8,128)(2,1)}, bf16[128,256]{1,0:T(8,128)(2,1)S(1)}, u32[]{:S(2)}, u32[]{:S(2)}) collective-permute-start(bf16[128,256]{1,0:T(8,128)(2,1)} %param.12), channel_id=1, source_target_pairs={{0,16},{2,18},{4,20},{6,22},{8,24},{10,26},{12,28},{14,30},{16,0},... | collective-permute-start | bytes 196616 | tf_op jit(solution)/shard_map/ppermute | solution.py:116
  4.1 3.9 %collective-permute-done = bf16[128,256]{1,0:T(8,128)(2,1)S(1)} collective-permute-done((bf16[128,256]{1,0:T(8,128)(2,1)}, bf16[128,256]{1,0:T(8,128)(2,1)S(1)}, u32[]{:S(2)}, u32[]{:S(2)}) %collective-permute-start) | collective-permute-done | bytes 65568 | tf_op jit(solution)/shard_map/ppermute | solution.py:116
  7.9 0.9 %pad_maximum_fusion.1 = bf16[2,128,256]{2,1,0:T(8,128)(2,1)S(1)} fusion(bf16[1,128,256]{2,1,0:T(8,128)(2,1)S(1)} %bitcast.17, bf16[1,128,256]{2,1,0:T(8,128)(2,1)} %bitcast.16), kind=kLoop, calls=%fused_computation.1 | loop fusion | flops 65536 | bytes 262144 | tf_op jit(solution)/shard_map/stack | solution.py:326
  8.8 0.0 copy-start.8
  8.8 0.1 broadcast_in_dim.11
  8.9 18.4 %all_to_all.15.weight_ref = bf16[8,256,256]{2,1,0:T(8,128)(2,1)S(1)} all-to-all(bf16[8,256,256]{2,1,0:T(8,128)(2,1)S(1)} %broadcast_in_dim.11), channel_id=1, replica_groups={{0,2,4,6,8,10,12,14},{16,18,20,22,24,26,28,30},{1,3,5,7,9,11,13,15},{17..., dimensions={0} | all-to-all | bytes 2097152 | tf_op jit(solution)/shard_map/all_to_all | solution.py:329
  27.3 0.0 copy-start.6
  27.3 1.4 %copy-done.6 = bf16[1,384,2048]{2,1,0:T(8,128)(2,1)S(1)} copy-done((bf16[1,384,2048]{2,1,0:T(8,128)(2,1)S(1)}, bf16[1,384,2048]{2,1,0:T(8,128)(2,1)}, u32[]{:S(2)}) %copy-start.6) | copy-done | bytes 1572888
  28.7 1.0 %norm_rows.1.normed_ref = bf16[384,2048]{1,0:T(8,128)(2,1)S(1)} custom-call(bf16[1,384,2048]{2,1,0:T(8,128)(2,1)S(1)} %copy-done.6, bf16[1,2048]{1,0:T(2,128)(2,1)S(1)} %reshape.18.gain_ref), custom_call_target="tpu_custom_call" | custom-call | flops 1572864000 | bytes 3145728 | tf_op jit(solution)/shard_map/norm_rows/pallas_call | solution.py:140
  29.7 1.6 %project.2.rest_0_ = bf16[512,384]{1,0:T(8,128)(2,1)} custom-call(s32[1]{0:T(128)} %bitcast.me_ref.refs_0_, bf16[384,2048]{1,0:T(8,128)(2,1)S(1)} %norm_rows.1.normed_ref, bf16[8,256,256]{2,1,0:T(8,128)(2,1)S(1)} %all_to_all.15.weight_ref, bf16[256,256]{1,0:T(8,128)(2,1)S(1)} %copy-done.3), custom_call_target="tpu_custom_call" | custom-call | flops 402653184 | bytes 1048576 | tf_op jit(solution)/shard_map/project/pallas_call | solution.py:176
  31.3 1.6 %project.3 = bf16[512,384]{1,0:T(8,128)(2,1)} custom-call(s32[1]{0:T(128)} %bitcast.me_ref.refs_0_, bf16[384,2048]{1,0:T(8,128)(2,1)S(1)} %norm_rows.1.normed_ref, bf16[8,256,256]{2,1,0:T(8,128)(2,1)S(1)} %collective-permute-done.1.weight_ref, bf16[256,256]{1,0:T(8,128)(2,1)S(1)} %copy-done.3, ...), custom_call_target="tpu_custom_call", output_to_operand_aliasing={{}: (4, {})} | custom-call | flops 402653184 | bytes 1048576 | tf_op jit(solution)/shard_map/project/pallas_call | solution.py:176
  32.9 5.3 %all-to-all-start.1 = ((bf16[16,32,384]{2,1,0:T(8,128)(2,1)}), bf16[16,32,384]{2,1,0:T(8,128)(2,1)S(1)}, u32[]{:S(2)}, u32[]{:S(2)}) async-start(bf16[16,32,384]{2,1,0:T(8,128)(2,1)} %bitcast.4), calls=%async_computation.1 | async-start | bytes 786432 | tf_op jit(solution)/shard_map/all_to_all | solution.py:354
  38.3 2.9 %collective-permute-start.2 = (bf16[256,128]{1,0:T(8,128)(2,1)S(1)}, bf16[256,128]{1,0:T(8,128)(2,1)S(1)}, u32[]{:S(2)}, u32[]{:S(2)}) collective-permute-start(bf16[256,128]{1,0:T(8,128)(2,1)S(1)} %copy-done.7), channel_id=1, source_target_pairs={{0,16},{2,18},{4,20},{6,22},{8,24},{10,26},{12,28},{14,30},{16,0},... | collective-permute-start | bytes 196616 | tf_op jit(solution)/shard_map/ppermute | solution.py:116
  41.2 0.6 constant_dynamic-update-slice_fusion.4
  41.8 11.5 %collective-permute-done.2 = bf16[256,128]{1,0:T(8,128)(2,1)S(1)} collective-permute-done((bf16[256,128]{1,0:T(8,128)(2,1)S(1)}, bf16[256,128]{1,0:T(8,128)(2,1)S(1)}, u32[]{:S(2)}, u32[]{:S(2)}) %collective-permute-start.2) | collective-permute-done | bytes 65568 | tf_op jit(solution)/shard_map/ppermute | solution.py:116
  53.3 1.5 %collective-permute-start.3 = (bf16[2,256,128]{2,1,0:T(8,128)(2,1)S(1)}, bf16[2,256,128]{2,1,0:T(8,128)(2,1)S(1)}, u32[]{:S(2)}, u32[]{:S(2)}) collective-permute-start(bf16[2,256,128]{2,1,0:T(8,128)(2,1)S(1)} %pad_maximum_fusion.2.refs_3_), channel_id=1, source_target_pairs={{0,2},{2,0},{4,6},{6,4},{8,10},{10,8},{12,14},{14,12},{16,18},{18,... | collective-permute-start | bytes 393224 | tf_op jit(solution)/shard_map/ppermute | solution.py:116
  54.9 1.5 %collective-permute-start.4 = (bf16[2,256,128]{2,1,0:T(8,128)(2,1)S(1)}, bf16[2,256,128]{2,1,0:T(8,128)(2,1)S(1)}, u32[]{:S(2)}, u32[]{:S(2)}) collective-permute-start(bf16[2,256,128]{2,1,0:T(8,128)(2,1)S(1)} %pad_maximum_fusion.2.refs_3_), channel_id=1, source_target_pairs={{0,4},{2,6},{4,0},{6,2},{8,12},{10,14},{12,8},{14,10},{16,20},{18,... | collective-permute-start | bytes 393224 | tf_op jit(solution)/shard_map/ppermute | solution.py:116
  56.3 0.6 constant_dynamic-update-slice_fusion.3
  57.0 2.9 %collective-permute-done.4.refs_5_ = bf16[2,256,128]{2,1,0:T(8,128)(2,1)S(1)} collective-permute-done((bf16[2,256,128]{2,1,0:T(8,128)(2,1)S(1)}, bf16[2,256,128]{2,1,0:T(8,128)(2,1)S(1)}, u32[]{:S(2)}, u32[]{:S(2)}) %collective-permute-start.4) | collective-permute-done | bytes 131104 | tf_op jit(solution)/shard_map/ppermute | solution.py:116
  59.8 0.6 collective-permute-start.5
  60.4 1.2 %collective-permute-done.6.refs_7_ = bf16[2,256,128]{2,1,0:T(8,128)(2,1)S(1)} collective-permute-done((bf16[2,256,128]{2,1,0:T(8,128)(2,1)S(1)}, bf16[2,256,128]{2,1,0:T(8,128)(2,1)S(1)}, u32[]{:S(2)}, u32[]{:S(2)}) %collective-permute-start.6) | collective-permute-done | bytes 131104 | tf_op jit(solution)/shard_map/ppermute | solution.py:116
  61.7 0.3 collective-permute-start.8
  61.9 0.7 constant_dynamic-update-slice_fusion.2
  62.6 2.1 %transform.1 = bf16[384,512]{1,0:T(8,128)(2,1)} custom-call(s32[1]{0:T(128)} %bitcast.me_ref.refs_0_, bf16[512,384]{1,0:T(8,128)(2,1)S(1)} %bitcast.12, bf16[1024,512]{1,0:T(8,128)(2,1)S(1)} %copy-done, f32[16,1,384]{2,1,0:T(1,128)S(1)} %copy-done.4, f32[16,1,384]{2,1,0:T(1,128)S(1)} %copy-done.5, bf16[384,768]{1,0:T(8,128)(2,1)S(1)} %copy-done.1), custom_call_target="tpu_custom_call" | custom-call | flops 402653184 | bytes 1572864 | tf_op jit(solution)/shard_map/transform/pallas_call | solution.py:224
  64.7 4.4 %all-to-all-start.2 = ((bf16[16,24,512]{2,1,0:T(8,128)(2,1)}), bf16[16,24,512]{2,1,0:T(8,128)(2,1)S(1)}, u32[]{:S(2)}, u32[]{:S(2)}) async-start(bf16[16,24,512]{2,1,0:T(8,128)(2,1)} %bitcast.6), calls=%async_computation.2 | async-start | bytes 786432 | tf_op jit(solution)/shard_map/all_to_all | solution.py:356
  69.1 0.7 constant_dynamic-update-slice_fusion.1
  69.8 0.7 constant_dynamic-update-slice_fusion
  70.5 0.6 collective-permute-start.11
  71.1 1.9 %collective-permute-start.9 = (bf16[2,256,128]{2,1,0:T(8,128)(2,1)S(1)}, bf16[2,256,128]{2,1,0:T(8,128)(2,1)S(1)}, u32[]{:S(2)}, u32[]{:S(2)}) collective-permute-start(bf16[2,256,128]{2,1,0:T(8,128)(2,1)S(1)} %collective-permute-done.8.refs_9_), channel_id=1, source_target_pairs={{0,2},{2,0},{4,6},{6,4},{8,10},{10,8},{12,14},{14,12},{16,18},{18,... | collective-permute-start | bytes 393224 | tf_op jit(solution)/shard_map/ppermute | solution.py:116
  73.0 5.2 %collective-permute-done.9.refs_10_ = bf16[2,256,128]{2,1,0:T(8,128)(2,1)S(1)} collective-permute-done((bf16[2,256,128]{2,1,0:T(8,128)(2,1)S(1)}, bf16[2,256,128]{2,1,0:T(8,128)(2,1)S(1)}, u32[]{:S(2)}, u32[]{:S(2)}) %collective-permute-start.9) | collective-permute-done | bytes 131104 | tf_op jit(solution)/shard_map/ppermute | solution.py:116
  78.2 1.3 %collective-permute-done.12.refs_13_ = bf16[2,256,128]{2,1,0:T(8,128)(2,1)S(1)} collective-permute-done((bf16[2,256,128]{2,1,0:T(8,128)(2,1)S(1)}, bf16[2,256,128]{2,1,0:T(8,128)(2,1)S(1)}, u32[]{:S(2)}, u32[]{:S(2)}) %collective-permute-start.12) | collective-permute-done | bytes 131104 | tf_op jit(solution)/shard_map/ppermute | solution.py:116
  79.6 3.0 %output.1 = bf16[384,2048]{1,0:T(8,128)(2,1)} custom-call(s32[1]{0:T(128)} %bitcast.me_ref.refs_0_, bf16[16,24,512]{2,1,0:T(8,128)(2,1)S(1)} %all-to-all-done.2.refs_1_, bf16[512,512]{1,0:T(8,128)(2,1)S(1)} %copy-done.2, bf16[2,256,128]{2,1,0:T(8,128)(2,1)S(1)} %pad_maximum_fusion.2.refs_3_, bf16[2,256,128]{2,1,0:T(8,128)(2,1)S(1)} %collective-permute-done.3.refs_4_, ...), custom_call_target="tpu_custom_call" | custom-call | flops 805306368 | bytes 1572864 | tf_op jit(solution)/shard_map/output/pallas_call | solution.py:295
  (32 shorter events, 0.1 us)
Async XLA Ops:
  0.0 7.9 %collective-permute-start = (bf16[128,256]{1,0:T(8,128)(2,1)}, bf16[128,256]{1,0:T(8,128)(2,1)S(1)}, u32[]{:S(2)}, u32[]{:S(2)}) collective-permute-start(bf16[128,256]{1,0:T(8,128)(2,1)} %param.12), channel_id=1, source_target_pairs={{0,16},{2,18},{4,20},{6,22},{8,24},{10,26},{12,28},{14,30},{16,0},... | collective-permute-start | bytes 196616 | tf_op jit(solution)/shard_map/ppermute | solution.py:116
  8.8 18.5 %copy-start.8 = (bf16[2048]{0:T(1024)(128)(2,1)S(1)}, bf16[2048]{0:T(1024)(128)(2,1)}, u32[]{:S(2)}) copy-start(bf16[2048]{0:T(1024)(128)(2,1)} %param.11) | copy-start | bytes 12292
  27.2 4.1 %collective-permute-start.1 = (bf16[8,256,256]{2,1,0:T(8,128)(2,1)S(1)}, bf16[8,256,256]{2,1,0:T(8,128)(2,1)S(1)}, u32[]{:S(2)}, u32[]{:S(2)}) collective-permute-start(bf16[8,256,256]{2,1,0:T(8,128)(2,1)S(1)} %all_to_all.15.weight_ref), channel_id=1, source_target_pairs={{0,1},{1,0},{2,3},{3,2},{4,5},{5,4},{6,7},{7,6},{8,9},{9,8},{10,11... | collective-permute-start | bytes 3145736 | tf_op jit(solution)/shard_map/ppermute | solution.py:116
  27.3 1.4 %copy-start.6 = (bf16[1,384,2048]{2,1,0:T(8,128)(2,1)S(1)}, bf16[1,384,2048]{2,1,0:T(8,128)(2,1)}, u32[]{:S(2)}) copy-start(bf16[1,384,2048]{2,1,0:T(8,128)(2,1)} %tokens_ref.1) | copy-start | bytes 4718596
  28.7 1.0 %copy-start.3 = (bf16[256,256]{1,0:T(8,128)(2,1)S(1)}, bf16[256,256]{1,0:T(8,128)(2,1)}, u32[]{:S(2)}) copy-start(bf16[256,256]{1,0:T(8,128)(2,1)} %constant.18.clone.split_ref) | copy-start | bytes 393220
  31.3 6.9 %copy-start.7 = (bf16[256,128]{1,0:T(8,128)(2,1)S(1)}, bf16[256,128]{1,0:T(8,128)(2,1)}, u32[]{:S(2)}) copy-start(bf16[256,128]{1,0:T(8,128)(2,1)} %param.13) | copy-start | bytes 196612
  31.3 31.3 %copy-start.1 = (bf16[384,768]{1,0:T(8,128)(2,1)S(1)}, bf16[384,768]{1,0:T(8,128)(2,1)}, u32[]{:S(2)}) copy-start(bf16[384,768]{1,0:T(8,128)(2,1)} %constant.21.clone.refs_5_) | copy-start | bytes 1769476
  32.9 29.7 %copy-start = (bf16[1024,512]{1,0:T(8,128)(2,1)S(1)}, bf16[1024,512]{1,0:T(8,128)(2,1)}, u32[]{:S(2)}) copy-start(bf16[1024,512]{1,0:T(8,128)(2,1)} %constant.20.clone.refs_2_) | copy-start | bytes 3145732
  32.9 29.7 %copy-start.4 = (f32[16,1,384]{2,1,0:T(1,128)S(1)}, f32[16,1,384]{2,1,0:T(1,128)}, u32[]{:S(2)}) copy-start(f32[16,1,384]{2,1,0:T(1,128)} %constant.22.clone.refs_3_) | copy-start | bytes 73732
  32.9 29.7 %copy-start.5 = (f32[16,1,384]{2,1,0:T(1,128)S(1)}, f32[16,1,384]{2,1,0:T(1,128)}, u32[]{:S(2)}) copy-start(f32[16,1,384]{2,1,0:T(1,128)} %constant.23.clone.refs_4_) | copy-start | bytes 73732
  32.9 29.7 %all-to-all-start.1 = ((bf16[16,32,384]{2,1,0:T(8,128)(2,1)}), bf16[16,32,384]{2,1,0:T(8,128)(2,1)S(1)}, u32[]{:S(2)}, u32[]{:S(2)}) async-start(bf16[16,32,384]{2,1,0:T(8,128)(2,1)} %bitcast.4), calls=%async_computation.1 | async-start | bytes 786432 | tf_op jit(solution)/shard_map/all_to_all | solution.py:354
  38.3 15.0 %collective-permute-start.2 = (bf16[256,128]{1,0:T(8,128)(2,1)S(1)}, bf16[256,128]{1,0:T(8,128)(2,1)S(1)}, u32[]{:S(2)}, u32[]{:S(2)}) collective-permute-start(bf16[256,128]{1,0:T(8,128)(2,1)S(1)} %copy-done.7), channel_id=1, source_target_pairs={{0,16},{2,18},{4,20},{6,22},{8,24},{10,26},{12,28},{14,30},{16,0},... | collective-permute-start | bytes 196616 | tf_op jit(solution)/shard_map/ppermute | solution.py:116
  53.3 7.1 %collective-permute-start.3 = (bf16[2,256,128]{2,1,0:T(8,128)(2,1)S(1)}, bf16[2,256,128]{2,1,0:T(8,128)(2,1)S(1)}, u32[]{:S(2)}, u32[]{:S(2)}) collective-permute-start(bf16[2,256,128]{2,1,0:T(8,128)(2,1)S(1)} %pad_maximum_fusion.2.refs_3_), channel_id=1, source_target_pairs={{0,2},{2,0},{4,6},{6,4},{8,10},{10,8},{12,14},{14,12},{16,18},{18,... | collective-permute-start | bytes 393224 | tf_op jit(solution)/shard_map/ppermute | solution.py:116
  54.9 5.0 %collective-permute-start.4 = (bf16[2,256,128]{2,1,0:T(8,128)(2,1)S(1)}, bf16[2,256,128]{2,1,0:T(8,128)(2,1)S(1)}, u32[]{:S(2)}, u32[]{:S(2)}) collective-permute-start(bf16[2,256,128]{2,1,0:T(8,128)(2,1)S(1)} %pad_maximum_fusion.2.refs_3_), channel_id=1, source_target_pairs={{0,4},{2,6},{4,0},{6,2},{8,12},{10,14},{12,8},{14,10},{16,20},{18,... | collective-permute-start | bytes 393224 | tf_op jit(solution)/shard_map/ppermute | solution.py:116
  56.3 5.3 %collective-permute-start.6 = (bf16[2,256,128]{2,1,0:T(8,128)(2,1)S(1)}, bf16[2,256,128]{2,1,0:T(8,128)(2,1)S(1)}, u32[]{:S(2)}, u32[]{:S(2)}) collective-permute-start(bf16[2,256,128]{2,1,0:T(8,128)(2,1)S(1)} %pad_maximum_fusion.2.refs_3_), channel_id=1, source_target_pairs={{0,8},{2,10},{4,12},{6,14},{8,0},{10,2},{12,4},{14,6},{16,24},{18,... | collective-permute-start | bytes 393224 | tf_op jit(solution)/shard_map/ppermute | solution.py:116
  59.8 10.6 %collective-permute-start.5 = (bf16[2,256,128]{2,1,0:T(8,128)(2,1)S(1)}, bf16[2,256,128]{2,1,0:T(8,128)(2,1)S(1)}, u32[]{:S(2)}, u32[]{:S(2)}) collective-permute-start(bf16[2,256,128]{2,1,0:T(8,128)(2,1)S(1)} %collective-permute-done.4.refs_5_), channel_id=1, source_target_pairs={{0,2},{2,0},{4,6},{6,4},{8,10},{10,8},{12,14},{14,12},{16,18},{18,... | collective-permute-start | bytes 393224 | tf_op jit(solution)/shard_map/ppermute | solution.py:116
  60.4 10.1 %collective-permute-start.7 = (bf16[2,256,128]{2,1,0:T(8,128)(2,1)S(1)}, bf16[2,256,128]{2,1,0:T(8,128)(2,1)S(1)}, u32[]{:S(2)}, u32[]{:S(2)}) collective-permute-start(bf16[2,256,128]{2,1,0:T(8,128)(2,1)S(1)} %collective-permute-done.3.refs_4_), channel_id=1, source_target_pairs={{0,8},{2,10},{4,12},{6,14},{8,0},{10,2},{12,4},{14,6},{16,24},{18,... | collective-permute-start | bytes 393224 | tf_op jit(solution)/shard_map/ppermute | solution.py:116
  61.7 8.8 %collective-permute-start.8 = (bf16[2,256,128]{2,1,0:T(8,128)(2,1)S(1)}, bf16[2,256,128]{2,1,0:T(8,128)(2,1)S(1)}, u32[]{:S(2)}, u32[]{:S(2)}) collective-permute-start(bf16[2,256,128]{2,1,0:T(8,128)(2,1)S(1)} %collective-permute-done.6.refs_7_), channel_id=1, source_target_pairs={{0,4},{2,6},{4,0},{6,2},{8,12},{10,14},{12,8},{14,10},{16,20},{18,... | collective-permute-start | bytes 393224 | tf_op jit(solution)/shard_map/ppermute | solution.py:116
  64.7 14.9 %copy-start.2 = (bf16[512,512]{1,0:T(8,128)(2,1)S(1)}, bf16[512,512]{1,0:T(8,128)(2,1)}, u32[]{:S(2)}) copy-start(bf16[512,512]{1,0:T(8,128)(2,1)} %constant.19.clone.refs_2_) | copy-start | bytes 1572868
  64.7 14.9 %all-to-all-start.2 = ((bf16[16,24,512]{2,1,0:T(8,128)(2,1)}), bf16[16,24,512]{2,1,0:T(8,128)(2,1)S(1)}, u32[]{:S(2)}, u32[]{:S(2)}) async-start(bf16[16,24,512]{2,1,0:T(8,128)(2,1)} %bitcast.6), calls=%async_computation.2 | async-start | bytes 786432 | tf_op jit(solution)/shard_map/all_to_all | solution.py:356
  70.5 9.1 %collective-permute-start.10 = (bf16[8,256,128]{2,1,0:T(8,128)(2,1)}, bf16[8,256,128]{2,1,0:T(8,128)(2,1)S(1)}, u32[]{:S(2)}, u32[]{:S(2)}) collective-permute-start(bf16[8,256,128]{2,1,0:T(8,128)(2,1)} %constant_dynamic-update-slice_fusion), channel_id=1, source_target_pairs={{0,1},{1,0},{2,3},{3,2},{4,5},{5,4},{6,7},{7,6},{8,9},{9,8},{10,11... | collective-permute-start | bytes 1572872 | tf_op jit(solution)/shard_map/ppermute | solution.py:116
  70.5 9.1 %collective-permute-start.11 = (bf16[6,256,128]{2,1,0:T(8,128)(2,1)S(1)}, bf16[6,256,128]{2,1,0:T(8,128)(2,1)S(1)}, u32[]{:S(2)}, u32[]{:S(2)}) collective-permute-start(bf16[6,256,128]{2,1,0:T(8,128)(2,1)S(1)} %pad_maximum_fusion), channel_id=1, source_target_pairs={{0,1},{1,0},{2,3},{3,2},{4,5},{5,4},{6,7},{7,6},{8,9},{9,8},{10,11... | collective-permute-start | bytes 1179656 | tf_op jit(solution)/shard_map/ppermute | solution.py:116
  71.1 7.1 %collective-permute-start.9 = (bf16[2,256,128]{2,1,0:T(8,128)(2,1)S(1)}, bf16[2,256,128]{2,1,0:T(8,128)(2,1)S(1)}, u32[]{:S(2)}, u32[]{:S(2)}) collective-permute-start(bf16[2,256,128]{2,1,0:T(8,128)(2,1)S(1)} %collective-permute-done.8.refs_9_), channel_id=1, source_target_pairs={{0,2},{2,0},{4,6},{6,4},{8,10},{10,8},{12,14},{14,12},{16,18},{18,... | collective-permute-start | bytes 393224 | tf_op jit(solution)/shard_map/ppermute | solution.py:116
  78.2 1.3 %collective-permute-start.12 = (bf16[2,256,128]{2,1,0:T(8,128)(2,1)S(1)}, bf16[2,256,128]{2,1,0:T(8,128)(2,1)S(1)}, u32[]{:S(2)}, u32[]{:S(2)}) collective-permute-start(bf16[2,256,128]{2,1,0:T(8,128)(2,1)S(1)} %collective-permute-done.9.refs_10_), channel_id=1, source_target_pairs={{0,1},{1,0},{2,3},{3,2},{4,5},{5,4},{6,7},{7,6},{8,9},{9,8},{10,11... | collective-permute-start | bytes 393224 | tf_op jit(solution)/shard_map/ppermute | solution.py:116

commit v4 on v2

--- a/solution.py
+++ b/solution.py
@@ -7,6 +7,7 @@
 from jax.experimental import pallas as pl
 from jax.experimental.pallas import tpu as pltpu
 from jax.sharding import PartitionSpec as P
+
 
 GS = 64
 EPS = 1e-06
@@ -151,25 +152,57 @@
     )(tokens, gain.reshape(1, width))
 
 
-def project(me, normed, weight, split, half, into=None):
+def spread_kernel(near, shard_ref, out_ref):
+    for i in range(near):
+        out_ref[i] = shard_ref[...]
+
+
+def spread(shard, near):
+    return pl.pallas_call(
+        lambda *refs: spread_kernel(near, *refs),
+        out_shape=jax.ShapeDtypeStruct((near,) + shard.shape, shard.dtype),
+        in_specs=whole_specs(1),
+        out_specs=pl.BlockSpec(memory_space=pltpu.VMEM),
+        compiler_params=vmem_params(),
+        cost_estimate=cost(shard.size * 400, shard.size * 2 * near),
+        name="spread",
+    )(shard)
+
+
+def project_near(me, normed, own, other):
+    near, depth, columns = own.shape
+    rows = normed.shape[0]
+    span = near * depth
+
+    def kernel(me_ref, normed_ref, own_ref, other_ref, out_ref):
+        piece = normed_ref[:, pl.ds(pl.multiple_of(me_ref[0] // near * span, span), span)]
+        for i, ref in enumerate((own_ref, other_ref)):
+            weight = ref[...].reshape(span, columns)
+            out_ref[:, i * columns : (i + 1) * columns] = jnp.dot(piece, weight, preferred_element_type=F32)
+
+    return pl.pallas_call(
+        kernel,
+        out_shape=jax.ShapeDtypeStruct((rows, 2 * columns), F32),
+        in_specs=[pl.BlockSpec(memory_space=pltpu.SMEM)] + whole_specs(3),
+        out_specs=pl.BlockSpec(memory_space=pltpu.VMEM),
+        compiler_params=vmem_params(),
+        cost_estimate=cost(4 * rows * span * columns, rows * span * 2),
+        name="project_near",
+    )(me, normed, own, other)
+
+
+def project_far(me, normed, weight, split, sofar, half, into=None):
     near, depth, columns = weight.shape
-    depth //= 2
     rows = normed.shape[0]
-
-    def kernel(me_ref, normed_ref, weight_ref, split_ref, *rest):
-        out_ref = rest[-1]
-        upper = me_ref[0] // near
-        total = jnp.zeros((rows, columns), F32)
-        for s in range(near):
-            own = pl.multiple_of((upper * near + s) * depth, depth)
-            far = pl.multiple_of(((1 - upper) * near + s) * depth, depth)
-            piece = jnp.concatenate([normed_ref[:, pl.ds(own, depth)], normed_ref[:, pl.ds(far, depth)]], axis=1)
-            total = total + jnp.dot(piece, weight_ref[s], preferred_element_type=F32)
-        sums = dot(split_ref[...], total.astype(BF), ((1,), (1,)))
-        out_ref[...] = sums.astype(BF)
-
-    args = [me, normed, weight, split] + ([] if into is None else [into])
-    smem = pl.BlockSpec(memory_space=pltpu.SMEM)
+    span = near * depth
+
+    def kernel(me_ref, normed_ref, weight_ref, split_ref, sofar_ref, *rest):
+        piece = normed_ref[:, pl.ds(pl.multiple_of((1 - me_ref[0] // near) * span, span), span)]
+        total = jnp.dot(piece, weight_ref[...].reshape(span, columns), preferred_element_type=F32)
+        total = (total + sofar_ref[...]).astype(BF)
+        rest[-1][...] = dot(split_ref[...], total, ((1,), (1,))).astype(BF)
+
+    args = [me, normed, weight, split, sofar] + ([] if into is None else [into])
     extra = [] if into is None else [pl.BlockSpec(memory_space=pl.ANY)]
     zero = lambda i: (0, 0)
     return pl.pallas_call(
@@ -177,17 +210,18 @@
         out_shape=jax.ShapeDtypeStruct((2 * columns, rows), BF),
         grid=(1,),
         in_specs=[
-            smem,
+            pl.BlockSpec(memory_space=pltpu.SMEM),
             pl.BlockSpec(normed.shape, zero),
             pl.BlockSpec(weight.shape, lambda i: (0, 0, 0)),
             pl.BlockSpec(split.shape, zero),
+            pl.BlockSpec((rows, columns), lambda i: (0, half)),
         ]
         + extra,
         out_specs=pl.BlockSpec((columns, rows), lambda i: (half, 0)),
-        input_output_aliases={} if into is None else {4: 0},
-        compiler_params=vmem_params(),
-        cost_estimate=cost(2 * rows * near * 2 * depth * columns, weight.size * 2),
-        name="project",
+        input_output_aliases={} if into is None else {5: 0},
+        compiler_params=vmem_params(),
+        cost_estimate=cost(2 * rows * span * columns, weight.size * 2),
+        name="project_far",
     )(*args)
 
 
@@ -317,21 +351,22 @@
     def core_swap(value):
         return swap(value, "col", cols, 1)
 
-    in_both = jnp.stack([in_weight, row_swap(in_weight, near)])
-    in_both = in_both.reshape(1, 2 * in_weight.shape[0], in_weight.shape[1])
     groups = [list(range(near)), list(range(near, peers))]
-    in_own = lax.all_to_all(
-        jnp.broadcast_to(in_both, (near,) + in_both.shape[1:]),
-        "row",
-        split_axis=0,
-        concat_axis=0,
-        tiled=True,
-        axis_index_groups=groups,
-    )
+
+    def near_all(copies):
+        return lax.all_to_all(copies, "row", split_axis=0, concat_axis=0, tiled=True, axis_index_groups=groups)
+
+    in_far = row_swap(in_weight, near)
+    copies_a = spread(in_weight, near)
+    in_a = near_all(copies_a)
+    copies_b = spread(in_far, near)
+    in_b = near_all(copies_b)
     normed = norm_rows(tokens, norm_gain)
-    in_other = core_swap(in_own)
-
-    pairs = {0: jnp.stack([out_weight, row_swap(out_weight, near)])}
+    sofar = project_near(me, normed, in_a, core_swap(in_a))
+    other_b = core_swap(in_b)
+
+    out_far = row_swap(out_weight, near)
+    pairs = {0: jnp.stack([out_weight, out_far])}
     for bit in (1, 2, 4):
         pairs[bit] = row_swap(pairs[0], bit)
     pairs[3] = row_swap(pairs[2], 1)
@@ -340,8 +375,8 @@
     pairs[7] = row_swap(pairs[6], 1)
     others = [core_swap(pairs[m]) for m in range(near)]
 
-    sums = project(me, normed, in_own, split_half, 0)
-    sums = project(me, normed, in_other, split_half, 1, sums)
+    sums = project_far(me, normed, in_b, split_half, sofar, 0)
+    sums = project_far(me, normed, other_b, split_half, sofar, 1, sums)
     got = lax.all_to_all(sums.reshape(peers, narrow, rows), "row", split_axis=0, concat_axis=0, tiled=True)
     whole = transform(me, got.reshape(channels, rows), peers, rows)
     back = lax.all_to_all(whole.reshape(peers, inner, channels), "row", split_axis=0, concat_axis=0, tiled=True)

time: 89.4 us -> 92.1 us (1.030)
  blocking collectives: 36.6 us -> 15.8 us
  waiting for transfers between devices: 22.1 us -> 33 us
  starting transfers between devices: 19.7 us -> 30.2 us
  Pallas kernels: 8 us -> 9.73 us
  local copies, waits for them, and re-layouts: 1.53 us -> 2.61 us
    all_to_all x1 -> x0, blocking collectives: 18.4 us -> none  [body_cube(): lax.all_to_all(jnp.broadcast_to(in_both, (near,) + in_both.shape[1:]), 'r...]
    all_to_all x0 -> x2, starting transfers between devices: none -> 11.7 us  [near_all(): lax.all_to_all(copies, 'row', split_axis=0, concat_axis=0, tiled=True, ax...]
    all_to_all x0 -> x2, waiting for transfers between devices: none -> 10.1 us  [near_all(): lax.all_to_all(copies, 'row', split_axis=0, concat_axis=0, tiled=True, ax...]
    all_to_all x1, blocking collectives: 18.2 us -> 15.8 us  [body_cube(): lax.all_to_all(sums.reshape(peers, narrow, rows), 'row', split_axis=0, co...]
    pallas_call x2 -> x5, Pallas kernels: 1.84 us -> 3.58 us  [the longest x2 1.65 us: spread(): pl.pallas_call(lambda *refs: spread_kernel(near, *refs), out_shape=jax.Sh...]
    ppermute x18 -> x19, starting transfers between devices: 16 us -> 14.6 us  [swap(): return lax.ppermute(value, axis, [(i, i ^ bit) for i in range(count)])]
    unnamed x18 -> x22, local copies, waits for them, and re-layouts: 1.45 us -> 2.61 us
    ppermute x18 -> x19, waiting for transfers between devices: 22.1 us -> 22.9 us  [swap(): return lax.ppermute(value, axis, [(i, i ^ bit) for i in range(count)])]
  transfers between devices with their start and end apart: 19 -> 22, of which waited for: 7 -> 9; matrix products, arithmetic and copies ran while one was open for 0% -> 0% of each run, Pallas kernels for 2% -> 3%
where the time goes in v4:
time: 92.1 us; the launch traced here: 91.6 us
  waiting for transfers between devices  33 us (36%)
  starting transfers between devices  30.2 us (33%)
  blocking collectives  15.8 us (17%)
  Pallas kernels  9.73 us (11%)
  local copies, waits for them, and re-layouts  2.61 us (3%)
    ppermute x19, waiting for transfers between devices, swap(): return lax.ppermute(value, axis, [(i, i ^ bit) for i in range(count)])  22.9 us
    all_to_all x1, blocking collectives, body_cube(): lax.all_to_all(sums.reshape(peers, narrow, rows), 'row', split_axis=0, co...  15.8 us
    ppermute x19, starting transfers between devices, swap(): return lax.ppermute(value, axis, [(i, i ^ bit) for i in range(count)])  14.6 us
    all_to_all x2, starting transfers between devices, near_all(): lax.all_to_all(copies, 'row', split_axis=0, concat_axis=0, tiled=True, ax...  11.7 us
    all_to_all x2, waiting for transfers between devices, near_all(): lax.all_to_all(copies, 'row', split_axis=0, concat_axis=0, tiled=True, ax...  10.1 us
    all_to_all x1, starting transfers between devices, body_cube(): lax.all_to_all(whole.reshape(peers, inner, channels), 'row', split_axis=0...  3.92 us
    pallas_call x1, Pallas kernels, output(): pl.pallas_call(kernel, out_shape=jax.ShapeDtypeStruct((rows, width * peer...  2.99 us
    unnamed x22, local copies, waits for them, and re-layouts  2.61 us
  transfers between devices with their start and end apart: 22, of which 9 were waited for; matrix products, arithmetic and copies ran while one was open for 0% of the time, Pallas kernels for 3%

profile of v4, /device:TPU:0, one launch (start us, length us, event | category | flops | bytes accessed | tf_op | source)
XLA Modules:
  0.0 91.6 jit_solution(8651323511750051332)
XLA Ops:
  0.0 0.8 copy-done.4
  0.8 0.8 spread.3
  1.7 6.2 %all-to-all-start.1 = ((bf16[8,128,256]{2,1,0:T(8,128)(2,1)}), bf16[8,128,256]{2,1,0:T(8,128)(2,1)S(1)}, u32[]{:S(2)}, u32[]{:S(2)}) async-start(bf16[8,128,256]{2,1,0:T(8,128)(2,1)} %spread.3), calls=%async_computation.1 | async-start | bytes 1048576 | tf_op jit(solution)/shard_map/all_to_all | solution.py:357
  7.9 2.7 %collective-permute-start = (bf16[128,256]{1,0:T(8,128)(2,1)S(1)}, bf16[128,256]{1,0:T(8,128)(2,1)S(1)}, u32[]{:S(2)}, u32[]{:S(2)}) collective-permute-start(bf16[128,256]{1,0:T(8,128)(2,1)S(1)} %copy-done.5), channel_id=1, source_target_pairs={{0,16},{2,18},{4,20},{6,22},{8,24},{10,26},{12,28},{14,30},{16,0},... | collective-permute-start | bytes 196616 | tf_op jit(solution)/shard_map/ppermute | solution.py:116
  10.5 4.5 %collective-permute-done.refs_0_ = bf16[128,256]{1,0:T(8,128)(2,1)S(1)} collective-permute-done((bf16[128,256]{1,0:T(8,128)(2,1)S(1)}, bf16[128,256]{1,0:T(8,128)(2,1)S(1)}, u32[]{:S(2)}, u32[]{:S(2)}) %collective-permute-start) | collective-permute-done | bytes 65568 | tf_op jit(solution)/shard_map/ppermute | solution.py:116
  15.1 0.8 spread.2
  15.9 2.5 %all-to-all-done.1.own_ref = bf16[8,128,256]{2,1,0:T(8,128)(2,1)S(1)} async-done(((bf16[8,128,256]{2,1,0:T(8,128)(2,1)}), bf16[8,128,256]{2,1,0:T(8,128)(2,1)S(1)}, u32[]{:S(2)}, u32[]{:S(2)}) %all-to-all-start.1) | async-done | bytes 524320 | tf_op jit(solution)/shard_map/all_to_all | solution.py:357
  18.3 5.4 %all-to-all-start = ((bf16[8,128,256]{2,1,0:T(8,128)(2,1)}), bf16[8,128,256]{2,1,0:T(8,128)(2,1)S(1)}, u32[]{:S(2)}, u32[]{:S(2)}) async-start(bf16[8,128,256]{2,1,0:T(8,128)(2,1)} %spread.2), calls=%async_computation | async-start | bytes 1048576 | tf_op jit(solution)/shard_map/all_to_all | solution.py:357
  23.8 7.7 %all-to-all-done.weight_ref = bf16[8,128,256]{2,1,0:T(8,128)(2,1)S(1)} async-done(((bf16[8,128,256]{2,1,0:T(8,128)(2,1)}), bf16[8,128,256]{2,1,0:T(8,128)(2,1)S(1)}, u32[]{:S(2)}, u32[]{:S(2)}) %all-to-all-start) | async-done | bytes 524320 | tf_op jit(solution)/shard_map/all_to_all | solution.py:357
  31.5 1.4 %copy-done.8 = bf16[1,384,2048]{2,1,0:T(8,128)(2,1)S(1)} copy-done((bf16[1,384,2048]{2,1,0:T(8,128)(2,1)S(1)}, bf16[1,384,2048]{2,1,0:T(8,128)(2,1)}, u32[]{:S(2)}) %copy-start.8) | copy-done | bytes 1572888
  32.9 1.0 %norm_rows.1.normed_ref = bf16[384,2048]{1,0:T(8,128)(2,1)S(1)} custom-call(bf16[1,384,2048]{2,1,0:T(8,128)(2,1)S(1)} %copy-done.8, bf16[1,2048]{1,0:T(2,128)(2,1)S(1)} %reshape.16.gain_ref), custom_call_target="tpu_custom_call" | custom-call | flops 1572864000 | bytes 3145728 | tf_op jit(solution)/shard_map/norm_rows/pallas_call | solution.py:140
  34.0 0.6 project_near.1.sofar_ref
  34.8 0.7 project_far.2.rest_0_
  35.6 0.7 project_far.3
  36.3 15.8 %all_to_all.20 = bf16[16,32,384]{2,1,0:T(8,128)(2,1)S(1)} all-to-all(bf16[16,32,384]{2,1,0:T(8,128)(2,1)S(1)} %bitcast.7), channel_id=1, replica_groups=mesh['row'=16,'col'=2] {'row'}, dimensions={0} | all-to-all | bytes 786432 | tf_op jit(solution)/shard_map/all_to_all | solution.py:380
  52.1 2.1 %transform.1 = bf16[384,512]{1,0:T(8,128)(2,1)} custom-call(s32[1]{0:T(128)} %bitcast.me_ref.refs_0_, bf16[512,384]{1,0:T(8,128)(2,1)S(1)} %bitcast.8, bf16[1024,512]{1,0:T(8,128)(2,1)S(1)} %copy-done, f32[16,1,384]{2,1,0:T(1,128)S(1)} %copy-done.6, f32[16,1,384]{2,1,0:T(1,128)S(1)} %copy-done.7, bf16[384,768]{1,0:T(8,128)(2,1)S(1)} %copy-done.1), custom_call_target="tpu_custom_call" | custom-call | flops 402653184 | bytes 1572864 | tf_op jit(solution)/shard_map/transform/pallas_call | solution.py:257
  54.3 3.9 %all-to-all-start.3 = ((bf16[16,24,512]{2,1,0:T(8,128)(2,1)}), bf16[16,24,512]{2,1,0:T(8,128)(2,1)S(1)}, u32[]{:S(2)}, u32[]{:S(2)}) async-start(bf16[16,24,512]{2,1,0:T(8,128)(2,1)} %bitcast.3), calls=%async_computation.3 | async-start | bytes 786432 | tf_op jit(solution)/shard_map/all_to_all | solution.py:382
  58.2 2.9 %collective-permute-start.3 = (bf16[256,128]{1,0:T(8,128)(2,1)S(1)}, bf16[256,128]{1,0:T(8,128)(2,1)S(1)}, u32[]{:S(2)}, u32[]{:S(2)}) collective-permute-start(bf16[256,128]{1,0:T(8,128)(2,1)S(1)} %copy-done.9), channel_id=1, source_target_pairs={{0,16},{2,18},{4,20},{6,22},{8,24},{10,26},{12,28},{14,30},{16,0},... | collective-permute-start | bytes 196616 | tf_op jit(solution)/shard_map/ppermute | solution.py:116
  61.1 11.1 %collective-permute-done.3 = bf16[256,128]{1,0:T(8,128)(2,1)S(1)} collective-permute-done((bf16[256,128]{1,0:T(8,128)(2,1)S(1)}, bf16[256,128]{1,0:T(8,128)(2,1)S(1)}, u32[]{:S(2)}, u32[]{:S(2)}) %collective-permute-start.3) | collective-permute-done | bytes 65568 | tf_op jit(solution)/shard_map/ppermute | solution.py:116
  72.2 1.5 %collective-permute-start.5 = (bf16[2,256,128]{2,1,0:T(8,128)(2,1)S(1)}, bf16[2,256,128]{2,1,0:T(8,128)(2,1)S(1)}, u32[]{:S(2)}, u32[]{:S(2)}) collective-permute-start(bf16[2,256,128]{2,1,0:T(8,128)(2,1)S(1)} %pad_maximum_fusion.refs_3_), channel_id=1, source_target_pairs={{0,4},{2,6},{4,0},{6,2},{8,12},{10,14},{12,8},{14,10},{16,20},{18,... | collective-permute-start | bytes 393224 | tf_op jit(solution)/shard_map/ppermute | solution.py:116
  73.7 1.5 %collective-permute-start.4 = (bf16[2,256,128]{2,1,0:T(8,128)(2,1)S(1)}, bf16[2,256,128]{2,1,0:T(8,128)(2,1)S(1)}, u32[]{:S(2)}, u32[]{:S(2)}) collective-permute-start(bf16[2,256,128]{2,1,0:T(8,128)(2,1)S(1)} %pad_maximum_fusion.refs_3_), channel_id=1, source_target_pairs={{0,2},{2,0},{4,6},{6,4},{8,10},{10,8},{12,14},{14,12},{16,18},{18,... | collective-permute-start | bytes 393224 | tf_op jit(solution)/shard_map/ppermute | solution.py:116
  75.2 2.0 %collective-permute-done.7.refs_7_ = bf16[2,256,128]{2,1,0:T(8,128)(2,1)S(1)} collective-permute-done((bf16[2,256,128]{2,1,0:T(8,128)(2,1)S(1)}, bf16[2,256,128]{2,1,0:T(8,128)(2,1)S(1)}, u32[]{:S(2)}, u32[]{:S(2)}) %collective-permute-start.7) | collective-permute-done | bytes 131104 | tf_op jit(solution)/shard_map/ppermute | solution.py:116
  77.2 1.4 %collective-permute-start.9 = (bf16[2,256,128]{2,1,0:T(8,128)(2,1)S(1)}, bf16[2,256,128]{2,1,0:T(8,128)(2,1)S(1)}, u32[]{:S(2)}, u32[]{:S(2)}) collective-permute-start(bf16[2,256,128]{2,1,0:T(8,128)(2,1)S(1)} %collective-permute-done.7.refs_7_), channel_id=1, source_target_pairs={{0,4},{2,6},{4,0},{6,2},{8,12},{10,14},{12,8},{14,10},{16,20},{18,... | collective-permute-start | bytes 393224 | tf_op jit(solution)/shard_map/ppermute | solution.py:116
  78.6 1.5 %collective-permute-start.6 = (bf16[2,256,128]{2,1,0:T(8,128)(2,1)S(1)}, bf16[2,256,128]{2,1,0:T(8,128)(2,1)S(1)}, u32[]{:S(2)}, u32[]{:S(2)}) collective-permute-start(bf16[2,256,128]{2,1,0:T(8,128)(2,1)S(1)} %collective-permute-done.5.refs_5_), channel_id=1, source_target_pairs={{0,2},{2,0},{4,6},{6,4},{8,10},{10,8},{12,14},{14,12},{16,18},{18,... | collective-permute-start | bytes 393224 | tf_op jit(solution)/shard_map/ppermute | solution.py:116
  80.1 0.6 collective-permute-start.8
  80.7 0.5 collective-permute-start.13
  81.2 0.9 %collective-permute-done.9.refs_9_ = bf16[2,256,128]{2,1,0:T(8,128)(2,1)S(1)} collective-permute-done((bf16[2,256,128]{2,1,0:T(8,128)(2,1)S(1)}, bf16[2,256,128]{2,1,0:T(8,128)(2,1)S(1)}, u32[]{:S(2)}, u32[]{:S(2)}) %collective-permute-start.9) | collective-permute-done | bytes 131104 | tf_op jit(solution)/shard_map/ppermute | solution.py:116
  82.2 1.5 %collective-permute-start.10 = (bf16[2,256,128]{2,1,0:T(8,128)(2,1)S(1)}, bf16[2,256,128]{2,1,0:T(8,128)(2,1)S(1)}, u32[]{:S(2)}, u32[]{:S(2)}) collective-permute-start(bf16[2,256,128]{2,1,0:T(8,128)(2,1)S(1)} %collective-permute-done.9.refs_9_), channel_id=1, source_target_pairs={{0,2},{2,0},{4,6},{6,4},{8,10},{10,8},{12,14},{14,12},{16,18},{18,... | collective-permute-start | bytes 393224 | tf_op jit(solution)/shard_map/ppermute | solution.py:116
  83.6 1.4 %collective-permute-done.8.refs_8_ = bf16[2,256,128]{2,1,0:T(8,128)(2,1)S(1)} collective-permute-done((bf16[2,256,128]{2,1,0:T(8,128)(2,1)S(1)}, bf16[2,256,128]{2,1,0:T(8,128)(2,1)S(1)}, u32[]{:S(2)}, u32[]{:S(2)}) %collective-permute-start.8) | collective-permute-done | bytes 131104 | tf_op jit(solution)/shard_map/ppermute | solution.py:116
  85.6 1.6 %collective-permute-done.10.refs_10_ = bf16[2,256,128]{2,1,0:T(8,128)(2,1)S(1)} collective-permute-done((bf16[2,256,128]{2,1,0:T(8,128)(2,1)S(1)}, bf16[2,256,128]{2,1,0:T(8,128)(2,1)S(1)}, u32[]{:S(2)}, u32[]{:S(2)}) %collective-permute-start.10) | collective-permute-done | bytes 131104 | tf_op jit(solution)/shard_map/ppermute | solution.py:116
  87.3 1.3 %collective-permute-done.18.refs_18_ = bf16[2,256,128]{2,1,0:T(8,128)(2,1)S(1)} collective-permute-done((bf16[2,256,128]{2,1,0:T(8,128)(2,1)S(1)}, bf16[2,256,128]{2,1,0:T(8,128)(2,1)S(1)}, u32[]{:S(2)}, u32[]{:S(2)}) %collective-permute-start.18) | collective-permute-done | bytes 131104 | tf_op jit(solution)/shard_map/ppermute | solution.py:116
  88.6 3.0 %output.1 = bf16[384,2048]{1,0:T(8,128)(2,1)} custom-call(s32[1]{0:T(128)} %bitcast.me_ref.refs_0_, bf16[16,24,512]{2,1,0:T(8,128)(2,1)S(1)} %all-to-all-done.3.refs_1_, bf16[512,512]{1,0:T(8,128)(2,1)S(1)} %copy-done.2, bf16[2,256,128]{2,1,0:T(8,128)(2,1)S(1)} %pad_maximum_fusion.refs_3_, bf16[2,256,128]{2,1,0:T(8,128)(2,1)S(1)} %collective-permute-done.4.refs_4_, ...), custom_call_target="tpu_custom_call" | custom-call | flops 805306368 | bytes 1572864 | tf_op jit(solution)/shard_map/output/pallas_call | solution.py:323
  (45 shorter events, 1.1 us)
Async XLA Ops:
  0.8 7.0 %copy-start.5 = (bf16[128,256]{1,0:T(8,128)(2,1)S(1)}, bf16[128,256]{1,0:T(8,128)(2,1)}, u32[]{:S(2)}) copy-start(bf16[128,256]{1,0:T(8,128)(2,1)} %refs_0_.1) | copy-start | bytes 196612
  0.8 30.6 %copy-start.10 = (bf16[2048]{0:T(1024)(128)(2,1)S(1)}, bf16[2048]{0:T(1024)(128)(2,1)}, u32[]{:S(2)}) copy-start(bf16[2048]{0:T(1024)(128)(2,1)} %param.11) | copy-start | bytes 12292
  1.7 16.7 %all-to-all-start.1 = ((bf16[8,128,256]{2,1,0:T(8,128)(2,1)}), bf16[8,128,256]{2,1,0:T(8,128)(2,1)S(1)}, u32[]{:S(2)}, u32[]{:S(2)}) async-start(bf16[8,128,256]{2,1,0:T(8,128)(2,1)} %spread.3), calls=%async_computation.1 | async-start | bytes 1048576 | tf_op jit(solution)/shard_map/all_to_all | solution.py:357
  7.9 7.2 %collective-permute-start = (bf16[128,256]{1,0:T(8,128)(2,1)S(1)}, bf16[128,256]{1,0:T(8,128)(2,1)S(1)}, u32[]{:S(2)}, u32[]{:S(2)}) collective-permute-start(bf16[128,256]{1,0:T(8,128)(2,1)S(1)} %copy-done.5), channel_id=1, source_target_pairs={{0,16},{2,18},{4,20},{6,22},{8,24},{10,26},{12,28},{14,30},{16,0},... | collective-permute-start | bytes 196616 | tf_op jit(solution)/shard_map/ppermute | solution.py:116
  18.3 13.1 %all-to-all-start = ((bf16[8,128,256]{2,1,0:T(8,128)(2,1)}), bf16[8,128,256]{2,1,0:T(8,128)(2,1)S(1)}, u32[]{:S(2)}, u32[]{:S(2)}) async-start(bf16[8,128,256]{2,1,0:T(8,128)(2,1)} %spread.2), calls=%async_computation | async-start | bytes 1048576 | tf_op jit(solution)/shard_map/all_to_all | solution.py:357
  23.8 10.1 %collective-permute-start.2 = (bf16[8,128,256]{2,1,0:T(8,128)(2,1)S(1)}, bf16[8,128,256]{2,1,0:T(8,128)(2,1)S(1)}, u32[]{:S(2)}, u32[]{:S(2)}) collective-permute-start(bf16[8,128,256]{2,1,0:T(8,128)(2,1)S(1)} %all-to-all-done.1.own_ref), channel_id=1, source_target_pairs={{0,1},{1,0},{2,3},{3,2},{4,5},{5,4},{6,7},{7,6},{8,9},{9,8},{10,11... | collective-permute-start | bytes 1572872 | tf_op jit(solution)/shard_map/ppermute | solution.py:116
  31.5 4.1 %collective-permute-start.1 = (bf16[8,128,256]{2,1,0:T(8,128)(2,1)S(1)}, bf16[8,128,256]{2,1,0:T(8,128)(2,1)S(1)}, u32[]{:S(2)}, u32[]{:S(2)}) collective-permute-start(bf16[8,128,256]{2,1,0:T(8,128)(2,1)S(1)} %all-to-all-done.weight_ref), channel_id=1, source_target_pairs={{0,1},{1,0},{2,3},{3,2},{4,5},{5,4},{6,7},{7,6},{8,9},{9,8},{10,11... | collective-permute-start | bytes 1572872 | tf_op jit(solution)/shard_map/ppermute | solution.py:116
  31.5 1.4 %copy-start.8 = (bf16[1,384,2048]{2,1,0:T(8,128)(2,1)S(1)}, bf16[1,384,2048]{2,1,0:T(8,128)(2,1)}, u32[]{:S(2)}) copy-start(bf16[1,384,2048]{2,1,0:T(8,128)(2,1)} %tokens_ref.1) | copy-start | bytes 4718596
  33.9 0.9 copy-start.3
  35.5 16.6 %copy-start = (bf16[1024,512]{1,0:T(8,128)(2,1)S(1)}, bf16[1024,512]{1,0:T(8,128)(2,1)}, u32[]{:S(2)}) copy-start(bf16[1024,512]{1,0:T(8,128)(2,1)} %constant.20.clone.refs_2_) | copy-start | bytes 3145732
  35.5 16.5 %copy-start.1 = (bf16[384,768]{1,0:T(8,128)(2,1)S(1)}, bf16[384,768]{1,0:T(8,128)(2,1)}, u32[]{:S(2)}) copy-start(bf16[384,768]{1,0:T(8,128)(2,1)} %constant.21.clone.refs_5_) | copy-start | bytes 1769476
  35.6 16.5 %copy-start.6 = (f32[16,1,384]{2,1,0:T(1,128)S(1)}, f32[16,1,384]{2,1,0:T(1,128)}, u32[]{:S(2)}) copy-start(f32[16,1,384]{2,1,0:T(1,128)} %constant.22.clone.refs_3_) | copy-start | bytes 73732
  35.6 16.5 %copy-start.7 = (f32[16,1,384]{2,1,0:T(1,128)S(1)}, f32[16,1,384]{2,1,0:T(1,128)}, u32[]{:S(2)}) copy-start(f32[16,1,384]{2,1,0:T(1,128)} %constant.23.clone.refs_4_) | copy-start | bytes 73732
  52.1 6.1 %copy-start.9 = (bf16[256,128]{1,0:T(8,128)(2,1)S(1)}, bf16[256,128]{1,0:T(8,128)(2,1)}, u32[]{:S(2)}) copy-start(bf16[256,128]{1,0:T(8,128)(2,1)} %param.13) | copy-start | bytes 196612
  52.1 36.5 %copy-start.2 = (bf16[512,512]{1,0:T(8,128)(2,1)S(1)}, bf16[512,512]{1,0:T(8,128)(2,1)}, u32[]{:S(2)}) copy-start(bf16[512,512]{1,0:T(8,128)(2,1)} %constant.19.clone.refs_2_) | copy-start | bytes 1572868
  54.3 34.3 %all-to-all-start.3 = ((bf16[16,24,512]{2,1,0:T(8,128)(2,1)}), bf16[16,24,512]{2,1,0:T(8,128)(2,1)S(1)}, u32[]{:S(2)}, u32[]{:S(2)}) async-start(bf16[16,24,512]{2,1,0:T(8,128)(2,1)} %bitcast.3), calls=%async_computation.3 | async-start | bytes 786432 | tf_op jit(solution)/shard_map/all_to_all | solution.py:382
  58.2 13.9 %collective-permute-start.3 = (bf16[256,128]{1,0:T(8,128)(2,1)S(1)}, bf16[256,128]{1,0:T(8,128)(2,1)S(1)}, u32[]{:S(2)}, u32[]{:S(2)}) collective-permute-start(bf16[256,128]{1,0:T(8,128)(2,1)S(1)} %copy-done.9), channel_id=1, source_target_pairs={{0,16},{2,18},{4,20},{6,22},{8,24},{10,26},{12,28},{14,30},{16,0},... | collective-permute-start | bytes 196616 | tf_op jit(solution)/shard_map/ppermute | solution.py:116
  72.2 5.0 %collective-permute-start.7 = (bf16[2,256,128]{2,1,0:T(8,128)(2,1)S(1)}, bf16[2,256,128]{2,1,0:T(8,128)(2,1)S(1)}, u32[]{:S(2)}, u32[]{:S(2)}) collective-permute-start(bf16[2,256,128]{2,1,0:T(8,128)(2,1)S(1)} %pad_maximum_fusion.refs_3_), channel_id=1, source_target_pairs={{0,8},{2,10},{4,12},{6,14},{8,0},{10,2},{12,4},{14,6},{16,24},{18,... | collective-permute-start | bytes 393224 | tf_op jit(solution)/shard_map/ppermute | solution.py:116
  72.2 6.4 %collective-permute-start.5 = (bf16[2,256,128]{2,1,0:T(8,128)(2,1)S(1)}, bf16[2,256,128]{2,1,0:T(8,128)(2,1)S(1)}, u32[]{:S(2)}, u32[]{:S(2)}) collective-permute-start(bf16[2,256,128]{2,1,0:T(8,128)(2,1)S(1)} %pad_maximum_fusion.refs_3_), channel_id=1, source_target_pairs={{0,4},{2,6},{4,0},{6,2},{8,12},{10,14},{12,8},{14,10},{16,20},{18,... | collective-permute-start | bytes 393224 | tf_op jit(solution)/shard_map/ppermute | solution.py:116
  73.7 6.4 %collective-permute-start.4 = (bf16[2,256,128]{2,1,0:T(8,128)(2,1)S(1)}, bf16[2,256,128]{2,1,0:T(8,128)(2,1)S(1)}, u32[]{:S(2)}, u32[]{:S(2)}) collective-permute-start(bf16[2,256,128]{2,1,0:T(8,128)(2,1)S(1)} %pad_maximum_fusion.refs_3_), channel_id=1, source_target_pairs={{0,2},{2,0},{4,6},{6,4},{8,10},{10,8},{12,14},{14,12},{16,18},{18,... | collective-permute-start | bytes 393224 | tf_op jit(solution)/shard_map/ppermute | solution.py:116
  75.2 5.5 %collective-permute-start.11 = (bf16[2,256,128]{2,1,0:T(8,128)(2,1)S(1)}, bf16[2,256,128]{2,1,0:T(8,128)(2,1)S(1)}, u32[]{:S(2)}, u32[]{:S(2)}) collective-permute-start(bf16[2,256,128]{2,1,0:T(8,128)(2,1)S(1)} %pad_maximum_fusion.refs_3_), channel_id=1, source_target_pairs={{0,1},{1,0},{2,3},{3,2},{4,5},{5,4},{6,7},{7,6},{8,9},{9,8},{10,11... | collective-permute-start | bytes 393224 | tf_op jit(solution)/shard_map/ppermute | solution.py:116
  77.2 5.0 %collective-permute-start.9 = (bf16[2,256,128]{2,1,0:T(8,128)(2,1)S(1)}, bf16[2,256,128]{2,1,0:T(8,128)(2,1)S(1)}, u32[]{:S(2)}, u32[]{:S(2)}) collective-permute-start(bf16[2,256,128]{2,1,0:T(8,128)(2,1)S(1)} %collective-permute-done.7.refs_7_), channel_id=1, source_target_pairs={{0,4},{2,6},{4,0},{6,2},{8,12},{10,14},{12,8},{14,10},{16,20},{18,... | collective-permute-start | bytes 393224 | tf_op jit(solution)/shard_map/ppermute | solution.py:116
  78.6 5.0 %collective-permute-start.6 = (bf16[2,256,128]{2,1,0:T(8,128)(2,1)S(1)}, bf16[2,256,128]{2,1,0:T(8,128)(2,1)S(1)}, u32[]{:S(2)}, u32[]{:S(2)}) collective-permute-start(bf16[2,256,128]{2,1,0:T(8,128)(2,1)S(1)} %collective-permute-done.5.refs_5_), channel_id=1, source_target_pairs={{0,2},{2,0},{4,6},{6,4},{8,10},{10,8},{12,14},{14,12},{16,18},{18,... | collective-permute-start | bytes 393224 | tf_op jit(solution)/shard_map/ppermute | solution.py:116
  80.1 5.0 %collective-permute-start.8 = (bf16[2,256,128]{2,1,0:T(8,128)(2,1)S(1)}, bf16[2,256,128]{2,1,0:T(8,128)(2,1)S(1)}, u32[]{:S(2)}, u32[]{:S(2)}) collective-permute-start(bf16[2,256,128]{2,1,0:T(8,128)(2,1)S(1)} %collective-permute-done.4.refs_4_), channel_id=1, source_target_pairs={{0,8},{2,10},{4,12},{6,14},{8,0},{10,2},{12,4},{14,6},{16,24},{18,... | collective-permute-start | bytes 393224 | tf_op jit(solution)/shard_map/ppermute | solution.py:116
  80.7 4.4 %collective-permute-start.12 = (bf16[2,256,128]{2,1,0:T(8,128)(2,1)S(1)}, bf16[2,256,128]{2,1,0:T(8,128)(2,1)S(1)}, u32[]{:S(2)}, u32[]{:S(2)}) collective-permute-start(bf16[2,256,128]{2,1,0:T(8,128)(2,1)S(1)} %collective-permute-done.4.refs_4_), channel_id=1, source_target_pairs={{0,1},{1,0},{2,3},{3,2},{4,5},{5,4},{6,7},{7,6},{8,9},{9,8},{10,11... | collective-permute-start | bytes 393224 | tf_op jit(solution)/shard_map/ppermute | solution.py:116
  80.7 4.9 %collective-permute-start.13 = (bf16[2,256,128]{2,1,0:T(8,128)(2,1)S(1)}, bf16[2,256,128]{2,1,0:T(8,128)(2,1)S(1)}, u32[]{:S(2)}, u32[]{:S(2)}) collective-permute-start(bf16[2,256,128]{2,1,0:T(8,128)(2,1)S(1)} %collective-permute-done.5.refs_5_), channel_id=1, source_target_pairs={{0,1},{1,0},{2,3},{3,2},{4,5},{5,4},{6,7},{7,6},{8,9},{9,8},{10,11... | collective-permute-start | bytes 393224 | tf_op jit(solution)/shard_map/ppermute | solution.py:116
  82.2 5.1 %collective-permute-start.10 = (bf16[2,256,128]{2,1,0:T(8,128)(2,1)S(1)}, bf16[2,256,128]{2,1,0:T(8,128)(2,1)S(1)}, u32[]{:S(2)}, u32[]{:S(2)}) collective-permute-start(bf16[2,256,128]{2,1,0:T(8,128)(2,1)S(1)} %collective-permute-done.9.refs_9_), channel_id=1, source_target_pairs={{0,2},{2,0},{4,6},{6,4},{8,10},{10,8},{12,14},{14,12},{16,18},{18,... | collective-permute-start | bytes 393224 | tf_op jit(solution)/shard_map/ppermute | solution.py:116
  83.6 3.6 %collective-permute-start.15 = (bf16[2,256,128]{2,1,0:T(8,128)(2,1)S(1)}, bf16[2,256,128]{2,1,0:T(8,128)(2,1)S(1)}, u32[]{:S(2)}, u32[]{:S(2)}) collective-permute-start(bf16[2,256,128]{2,1,0:T(8,128)(2,1)S(1)} %collective-permute-done.7.refs_7_), channel_id=1, source_target_pairs={{0,1},{1,0},{2,3},{3,2},{4,5},{5,4},{6,7},{7,6},{8,9},{9,8},{10,11... | collective-permute-start | bytes 393224 | tf_op jit(solution)/shard_map/ppermute | solution.py:116
  85.1 2.2 %collective-permute-start.17 = (bf16[2,256,128]{2,1,0:T(8,128)(2,1)S(1)}, bf16[2,256,128]{2,1,0:T(8,128)(2,1)S(1)}, u32[]{:S(2)}, u32[]{:S(2)}) collective-permute-start(bf16[2,256,128]{2,1,0:T(8,128)(2,1)S(1)} %collective-permute-done.9.refs_9_), channel_id=1, source_target_pairs={{0,1},{1,0},{2,3},{3,2},{4,5},{5,4},{6,7},{7,6},{8,9},{9,8},{10,11... | collective-permute-start | bytes 393224 | tf_op jit(solution)/shard_map/ppermute | solution.py:116
  85.1 2.2 %collective-permute-start.14 = (bf16[2,256,128]{2,1,0:T(8,128)(2,1)S(1)}, bf16[2,256,128]{2,1,0:T(8,128)(2,1)S(1)}, u32[]{:S(2)}, u32[]{:S(2)}) collective-permute-start(bf16[2,256,128]{2,1,0:T(8,128)(2,1)S(1)} %collective-permute-done.6.refs_6_), channel_id=1, source_target_pairs={{0,1},{1,0},{2,3},{3,2},{4,5},{5,4},{6,7},{7,6},{8,9},{9,8},{10,11... | collective-permute-start | bytes 393224 | tf_op jit(solution)/shard_map/ppermute | solution.py:116
  85.6 1.7 %collective-permute-start.16 = (bf16[2,256,128]{2,1,0:T(8,128)(2,1)S(1)}, bf16[2,256,128]{2,1,0:T(8,128)(2,1)S(1)}, u32[]{:S(2)}, u32[]{:S(2)}) collective-permute-start(bf16[2,256,128]{2,1,0:T(8,128)(2,1)S(1)} %collective-permute-done.8.refs_8_), channel_id=1, source_target_pairs={{0,1},{1,0},{2,3},{3,2},{4,5},{5,4},{6,7},{7,6},{8,9},{9,8},{10,11... | collective-permute-start | bytes 393224 | tf_op jit(solution)/shard_map/ppermute | solution.py:116
  87.2 1.3 %collective-permute-start.18 = (bf16[2,256,128]{2,1,0:T(8,128)(2,1)S(1)}, bf16[2,256,128]{2,1,0:T(8,128)(2,1)S(1)}, u32[]{:S(2)}, u32[]{:S(2)}) collective-permute-start(bf16[2,256,128]{2,1,0:T(8,128)(2,1)S(1)} %collective-permute-done.10.refs_10_), channel_id=1, source_target_pairs={{0,1},{1,0},{2,3},{3,2},{4,5},{5,4},{6,7},{7,6},{8,9},{9,8},{10,11... | collective-permute-start | bytes 393224 | tf_op jit(solution)/shard_map/ppermute | solution.py:116
  (1 other events, 0.8 us)

commit v5 on v4

--- a/solution.py
+++ b/solution.py
@@ -191,78 +191,116 @@
     )(me, normed, own, other)
 
 
-def project_far(me, normed, weight, split, sofar, half, into=None):
+def project_own(me, normed, weight, split, sofar):
     near, depth, columns = weight.shape
     rows = normed.shape[0]
     span = near * depth
 
-    def kernel(me_ref, normed_ref, weight_ref, split_ref, sofar_ref, *rest):
+    def kernel(me_ref, normed_ref, weight_ref, split_ref, sofar_ref, out_ref):
         piece = normed_ref[:, pl.ds(pl.multiple_of((1 - me_ref[0] // near) * span, span), span)]
         total = jnp.dot(piece, weight_ref[...].reshape(span, columns), preferred_element_type=F32)
-        total = (total + sofar_ref[...]).astype(BF)
-        rest[-1][...] = dot(split_ref[...], total, ((1,), (1,))).astype(BF)
-
-    args = [me, normed, weight, split, sofar] + ([] if into is None else [into])
-    extra = [] if into is None else [pl.BlockSpec(memory_space=pl.ANY)]
-    zero = lambda i: (0, 0)
+        total = (total + sofar_ref[:, :columns]).astype(BF)
+        out_ref[...] = dot(split_ref[...], total, ((1,), (1,))).astype(BF)
+
+    return pl.pallas_call(
+        kernel,
+        out_shape=jax.ShapeDtypeStruct((columns, rows), BF),
+        in_specs=[pl.BlockSpec(memory_space=pltpu.SMEM)] + whole_specs(4),
+        out_specs=pl.BlockSpec(memory_space=pltpu.VMEM),
+        compiler_params=vmem_params(),
+        cost_estimate=cost(2 * rows * span * columns, weight.size * 2),
+        name="project_own",
+    )(me, normed, weight, split, sofar)
+
+
+def project_other(me, normed, weight, split, sofar, first):
+    near, depth, columns = weight.shape
+    rows = normed.shape[0]
+    span = near * depth
+
+    def kernel(me_ref, normed_ref, weight_ref, split_ref, sofar_ref, first_ref, out_ref):
+        out_ref[:columns] = first_ref[...]
+        piece = normed_ref[:, pl.ds(pl.multiple_of((1 - me_ref[0] // near) * span, span), span)]
+        total = jnp.dot(piece, weight_ref[...].reshape(span, columns), preferred_element_type=F32)
+        total = (total + sofar_ref[:, columns:]).astype(BF)
+        out_ref[columns:] = dot(split_ref[...], total, ((1,), (1,))).astype(BF)
+
     return pl.pallas_call(
         kernel,
         out_shape=jax.ShapeDtypeStruct((2 * columns, rows), BF),
-        grid=(1,),
-        in_specs=[
-            pl.BlockSpec(memory_space=pltpu.SMEM),
-            pl.BlockSpec(normed.shape, zero),
-            pl.BlockSpec(weight.shape, lambda i: (0, 0, 0)),
-            pl.BlockSpec(split.shape, zero),
-            pl.BlockSpec((rows, columns), lambda i: (0, half)),
-        ]
-        + extra,
-        out_specs=pl.BlockSpec((columns, rows), lambda i: (half, 0)),
-        input_output_aliases={} if into is None else {5: 0},
+        in_specs=[pl.BlockSpec(memory_space=pltpu.SMEM)] + whole_specs(5),
+        out_specs=pl.BlockSpec(memory_space=pltpu.VMEM),
         compiler_params=vmem_params(),
         cost_estimate=cost(2 * rows * span * columns, weight.size * 2),
-        name="project_far",
-    )(*args)
-
-
-def transform_kernel(narrow, me_ref, got_ref, first_ref, cos_ref, sin_ref, second_ref, out_ref):
-    peers, _, rows = cos_ref.shape
-    stage = jnp.dot(first_ref[...], got_ref[...], preferred_element_type=F32)
-    stage = stage.reshape(2, peers, narrow, rows)
-    cos, sin = cos_ref[...], sin_ref[...]
-    real = stage[0] * cos + stage[1] * sin
-    imag = stage[1] * cos - stage[0] * sin
-    which = lax.broadcasted_iota(jnp.int32, (1, narrow, rows), 1) + me_ref[0] * narrow
-    sine = lax.rem(which, GS) > GS // 2
-    lead = jnp.where(sine, -imag, real).reshape(peers * narrow, rows).astype(BF)
-    tail = jnp.where(sine, real, imag).reshape(peers * narrow, rows).astype(BF)
+        name="project_other",
+    )(me, normed, weight, split, sofar, first)
+
+
+def sixteen(lines):
+    wave = [2.0 * math.pi * i / 16 for i in range(16)]
+    total = [lines[r] + lines[r + 8] for r in range(8)]
+    left = [lines[r] - lines[r + 8] for r in range(8)]
+    inner = [total[r] + total[r + 4] for r in range(4)]
+    outer = [total[r] - total[r + 4] for r in range(4)]
+    real, imag = {}, {}
+    even, odd = inner[0] + inner[2], inner[1] + inner[3]
+    real[0], real[8] = even + odd, even - odd
+    imag[0] = imag[8] = jnp.zeros_like(even)
+    real[4], imag[4] = inner[0] - inner[2], inner[3] - inner[1]
+    root = math.sqrt(0.5)
+    less, more = (outer[1] - outer[3]) * root, (outer[1] + outer[3]) * root
+    real[2], real[6] = outer[0] + less, outer[0] - less
+    imag[2], imag[6] = -more - outer[2], outer[2] - more
+    cosine = [left[r] - left[8 - r] for r in range(1, 4)]
+    sine = [left[r] + left[8 - r] for r in range(1, 4)]
+    for k in (1, 3, 5, 7):
+        real[k] = left[0] + sum(cosine[r - 1] * math.cos(wave[r * k % 16]) for r in range(1, 4))
+        middle = left[4] * math.sin(wave[4 * k % 16])
+        imag[k] = -middle - sum(sine[r - 1] * math.sin(wave[r * k % 16]) for r in range(1, 4))
+    return real, imag
+
+
+def transform_kernel(length, me_ref, got_ref, second_ref, out_ref, lead_ref, tail_ref):
+    channels, rows = got_ref.shape
+    peers = length // rows
+    narrow = channels // peers
+    k = lax.broadcasted_iota(jnp.int32, (peers, rows), 0)
+    m = lax.broadcasted_iota(jnp.int32, (peers, rows), 1)
+    radians = lax.rem(k * m, length).astype(F32) * (2.0 * math.pi / length)
+    cos, sin = jnp.cos(radians), jnp.sin(radians)
+    high, wide = 16, 128
+    for c in range(0, narrow, high):
+        which = lax.broadcasted_iota(jnp.int32, (high, wide), 0) + me_ref[0] * narrow + c
+        sums = lax.rem(which, GS) > GS // 2
+        for w in range(0, rows, wide):
+            lines = [got_ref[r * narrow + c : r * narrow + c + high, w : w + wide].astype(F32) for r in range(peers)]
+            real, imag = sixteen(lines)
+            for f in range(peers):
+                a, b = (real[f], imag[f]) if f <= peers // 2 else (real[peers - f], -imag[peers - f])
+                tc, ts = cos[f : f + 1, w : w + wide], sin[f : f + 1, w : w + wide]
+                first, other = a * tc + b * ts, b * tc - a * ts
+                at = f * narrow + c
+                lead_ref[at : at + high, w : w + wide] = jnp.where(sums, -other, first).astype(BF)
+                tail_ref[at : at + high, w : w + wide] = jnp.where(sums, first, other).astype(BF)
     lanes = ((1,), (1,))
-    out = dot(second_ref[:, :rows], lead, lanes) + dot(second_ref[:, rows:], tail, lanes)
+    out = dot(second_ref[:, :rows], lead_ref[...], lanes) + dot(second_ref[:, rows:], tail_ref[...], lanes)
     out_ref[...] = out.astype(BF)
 
 
 def transform(me, got, peers, rows):
     channels = got.shape[0]
-    narrow = channels // peers
-    small_cos, small_sin = angles(np.arange(peers), np.arange(peers), peers)
-    first = jnp.asarray(np.kron(np.concatenate([small_cos, -small_sin]), np.eye(narrow)), BF)
-    turn_cos, turn_sin = angles(np.arange(peers), np.arange(rows), rows * peers)
     long_cos, long_sin = angles(np.arange(rows), np.arange(rows), rows)
     second = jnp.asarray(np.concatenate([long_cos, long_sin], axis=1), BF)
-    turns = [jnp.asarray(t[:, None, :], F32) for t in (turn_cos, turn_sin)]
-
-    def kernel(*refs):
-        transform_kernel(narrow, *refs)
-
-    return pl.pallas_call(
-        kernel,
+    return pl.pallas_call(
+        lambda *refs: transform_kernel(rows * peers, *refs),
         out_shape=jax.ShapeDtypeStruct((rows, channels), BF),
-        in_specs=[pl.BlockSpec(memory_space=pltpu.SMEM)] + whole_specs(5),
+        in_specs=[pl.BlockSpec(memory_space=pltpu.SMEM)] + whole_specs(2),
         out_specs=pl.BlockSpec(memory_space=pltpu.VMEM),
+        scratch_shapes=[pltpu.VMEM((channels, rows), BF), pltpu.VMEM((channels, rows), BF)],
         compiler_params=vmem_params(),
         cost_estimate=cost(4 * rows * channels * channels, 6 * channels * channels),
         name="transform",
-    )(me, got, first, *turns, second)
+    )(me, got, second)
 
 
 def regroup(quads, lane):
@@ -279,57 +317,76 @@
     return out
 
 
-def output_kernel(scale, depth, me_ref, back_ref, join_ref, *refs):
-    own, other, (out_ref, sheet) = refs[:8], refs[8:16], refs[16:]
+BLOCKS = {0: (0, 0), 4: (0, 2), 1: (1, 0), 5: (1, 2), 2: (2, 0), 6: (2, 2), 3: (3, 0), 7: (4, 0)}
+
+
+def join_pattern(width):
+    row = lax.broadcasted_iota(jnp.int32, (width, width), 0)
+    column = lax.broadcasted_iota(jnp.int32, (width, width), 1)
+    r, c = lax.rem(row, GS), lax.rem(column, GS)
+    half = GS // 2
+    cosine = r <= half
+    order = jnp.where(cosine, r, r - half)
+    straight = c == order
+    turned = jnp.logical_and(c == GS - order, order < half)
+    value = jnp.where(straight, jnp.where(cosine, 1.0, -1.0), jnp.where(turned, 1.0, 0.0))
+    return jnp.where(row - r == column - c, value, 0.0).astype(BF)
+
+
+def output_kernel(scale, depth, me_ref, back_ref, *refs):
+    own, other, (out_ref, sheet, made_ref, out_sem) = refs[:5], refs[5:10], refs[10:]
     peers, inner, channels = back_ref.shape
+    near = len(BLOCKS)
+    width = own[0].shape[2]
     lane = lax.broadcasted_iota(jnp.int32, (inner, 128), 1)
     quads = channels // 128
     for a in range(quads):
-        made = []
         for b in range(quads):
             tiles = [back_ref[4 * b + j, :, 128 * a : 128 * a + 128].astype(F32) for j in range(4)]
-            made.append(regroup(tiles, lane))
-        for i in range(4):
-            for b in range(quads):
-                sheet[b, pl.ds(4 * a + i, inner, stride=peers), :] = made[b][i]
-    lines = jnp.concatenate([sheet[b].astype(BF) for b in range(quads)], axis=1)
-    mixed_real = jnp.dot(lines, join_ref[...], preferred_element_type=F32) * scale
-    mixed_real = mixed_real.astype(BF)
-    near = len(own)
+            for i, tile in enumerate(regroup(tiles, lane)):
+                sheet[b, pl.ds(4 * a + i, inner, stride=peers), :] = tile
+    join = join_pattern(128)
+    joined = [jnp.dot(sheet[b].astype(BF), join, preferred_element_type=F32) * scale for b in range(quads)]
+    mixed_real = jnp.concatenate([part.astype(BF) for part in joined], axis=1)
     upper = me_ref[0] // near
     place = lax.rem(me_ref[0], near)
-    width = own[0].shape[2]
-    for m in range(near):
-        left = jnp.concatenate([own[m][0], own[m][1]], axis=1)
-        right = jnp.concatenate([other[m][0], other[m][1]], axis=1)
+    stores = []
+    for m, (source, start) in BLOCKS.items():
+        left, right = [
+            jnp.concatenate([arrays[source][start], arrays[source][start + 1]], axis=1) for arrays in (own, other)
+        ]
         part = jnp.dot(mixed_real[:, :depth], left, preferred_element_type=F32)
         part = part + jnp.dot(mixed_real[:, depth:], right, preferred_element_type=F32)
-        part = part.astype(BF)
+        made_ref[m] = part.astype(BF)
         at = lax.bitwise_xor(place, m)
-        here = pl.multiple_of((upper * near + at) * width, width)
-        there = pl.multiple_of(((1 - upper) * near + at) * width, width)
-        out_ref[:, pl.ds(here, width)] = part[:, :width]
-        out_ref[:, pl.ds(there, width)] = part[:, width:]
-
-
-def output(me, back, join, own, other, scale):
+        for t, half in enumerate((upper, 1 - upper)):
+            into = out_ref.at[:, pl.ds(pl.multiple_of((half * near + at) * width, width), width)]
+            store = pltpu.make_async_copy(made_ref.at[m, :, t * width : t * width + width], into, out_sem.at[m, t])
+            store.start()
+            stores.append(store)
+    for store in stores:
+        store.wait()
+
+
+def output(me, back, own, other, scale):
     peers, inner, channels = back.shape
     depth, width = own[0].shape[1:]
     rows = peers * inner
-
-    def kernel(*refs):
-        output_kernel(scale, depth, *refs)
-
-    return pl.pallas_call(
-        kernel,
+    near = len(BLOCKS)
+    return pl.pallas_call(
+        lambda *refs: output_kernel(scale, depth, *refs),
         out_shape=jax.ShapeDtypeStruct((rows, width * peers), BF),
-        in_specs=[pl.BlockSpec(memory_space=pltpu.SMEM)] + whole_specs(2 + len(own) + len(other)),
-        out_specs=pl.BlockSpec(memory_space=pltpu.VMEM),
-        scratch_shapes=[pltpu.VMEM((channels // 128, rows, 128), F32)],
+        in_specs=[pl.BlockSpec(memory_space=pltpu.SMEM)] + whole_specs(1 + len(own) + len(other)),
+        out_specs=pl.BlockSpec(memory_space=pltpu.HBM),
+        scratch_shapes=[
+            pltpu.VMEM((channels // 128, rows, 128), F32),
+            pltpu.VMEM((near, rows, 2 * width), BF),
+            pltpu.SemaphoreType.DMA((near, 2)),
+        ],
         compiler_params=vmem_params(),
         cost_estimate=cost(2 * rows * channels * width * peers, rows * width * peers * 2),
         name="output",
-    )(me, back, join, *own, *other)
+    )(me, back, *own, *other)
 
 
 def body_cube(tokens, norm_gain, in_weight, out_weight):
@@ -341,9 +398,8 @@
     narrow = channels // peers
     inner = rows // peers
     me = lax.axis_index("row").astype(jnp.int32).reshape(1)
-    split, join = group_tables()
+    split, _ = group_tables()
     split_half = jnp.asarray(np.kron(np.eye(channels // cols // GS), split.T), BF)
-    join_all = jnp.asarray(np.kron(np.eye(channels // GS), join), BF)
 
     def row_swap(value, bit):
         return swap(value, "row", peers, bit)
@@ -366,22 +422,22 @@
     other_b = core_swap(in_b)
 
     out_far = row_swap(out_weight, near)
-    pairs = {0: jnp.stack([out_weight, out_far])}
-    for bit in (1, 2, 4):
-        pairs[bit] = row_swap(pairs[0], bit)
-    pairs[3] = row_swap(pairs[2], 1)
-    pairs[6] = row_swap(pairs[4], 2)
-    pairs[5] = row_swap(pairs[1], 4)
-    pairs[7] = row_swap(pairs[6], 1)
-    others = [core_swap(pairs[m]) for m in range(near)]
-
-    sums = project_far(me, normed, in_b, split_half, sofar, 0)
-    sums = project_far(me, normed, other_b, split_half, sofar, 1, sums)
+    pair = jnp.stack([out_weight, out_far])
+    beside = row_swap(pair, 4)
+    quad = jnp.concatenate([pair, beside])
+    over_x = row_swap(quad, 1)
+    over_y = row_swap(quad, 2)
+    over_xy = [row_swap(over_y[:2], 1), row_swap(over_x[2:], 2)]
+    ours = [quad, over_x, over_y, *over_xy]
+    others = [core_swap(value) for value in ours]
+
+    sums = project_own(me, normed, in_b, split_half, sofar)
+    sums = project_other(me, normed, other_b, split_half, sofar, sums)
     got = lax.all_to_all(sums.reshape(peers, narrow, rows), "row", split_axis=0, concat_axis=0, tiled=True)
     whole = transform(me, got.reshape(channels, rows), peers, rows)
     back = lax.all_to_all(whole.reshape(peers, inner, channels), "row", split_axis=0, concat_axis=0, tiled=True)
     scale = 1.0 / math.sqrt(rows * peers * GS)
-    result = output(me, back, join_all, [pairs[m] for m in range(near)], others, scale)
+    result = output(me, back, ours, others, scale)
     return result[None]
 
 

time: 92.1 us -> 85.7 us (0.931)
  blocking collectives: 15.8 us -> 0 us
  waiting for transfers between devices: 33 us -> 39.7 us
  starting transfers between devices: 30.2 us -> 32.9 us
    all_to_all x1 -> x0, blocking collectives: 15.8 us -> none  [body_cube(): lax.all_to_all(sums.reshape(peers, narrow, rows), 'row', split_axis=0, co...]
    ppermute x19 -> x14, waiting for transfers between devices: 22.9 us -> 29.6 us  [swap(): return lax.ppermute(value, axis, [(i, i ^ bit) for i in range(count)])]
    all_to_all x0 -> x1, starting transfers between devices: none -> 3.55 us  [body_cube(): lax.all_to_all(sums.reshape(peers, narrow, rows), 'row', split_axis=0, co...]
    ppermute x19 -> x14, starting transfers between devices: 14.6 us -> 12.5 us  [swap(): return lax.ppermute(value, axis, [(i, i ^ bit) for i in range(count)])]
    all_to_all x1, starting transfers between devices: 3.92 us -> 5.19 us  [body_cube(): lax.all_to_all(whole.reshape(peers, inner, channels), 'row', split_axis=0...]
    unnamed x22 -> x14, local copies, waits for them, and re-layouts: 2.61 us -> 2.58 us
  transfers between devices with their start and end apart: 22 -> 18, of which waited for: 9 -> 8; matrix products, arithmetic and copies ran while one was open for 0% -> 0% of each run, Pallas kernels for 3% -> 6%
where the time goes in v5:
time: 85.7 us; the launch traced here: 85.1 us
  waiting for transfers between devices  39.7 us (46%)
  starting transfers between devices  32.9 us (38%)
  Pallas kernels  9.68 us (11%)
  local copies, waits for them, and re-layouts  2.61 us (3%)
    ppermute x14, waiting for transfers between devices, swap(): return lax.ppermute(value, axis, [(i, i ^ bit) for i in range(count)])  29.6 us
    ppermute x14, starting transfers between devices, swap(): return lax.ppermute(value, axis, [(i, i ^ bit) for i in range(count)])  12.5 us
    all_to_all x2, starting transfers between devices, near_all(): lax.all_to_all(copies, 'row', split_axis=0, concat_axis=0, tiled=True, ax...  11.7 us
    all_to_all x2, waiting for transfers between devices, near_all(): lax.all_to_all(copies, 'row', split_axis=0, concat_axis=0, tiled=True, ax...  10.1 us
    all_to_all x1, starting transfers between devices, body_cube(): lax.all_to_all(whole.reshape(peers, inner, channels), 'row', split_axis=0...  5.19 us
    all_to_all x1, starting transfers between devices, body_cube(): lax.all_to_all(sums.reshape(peers, narrow, rows), 'row', split_axis=0, co...  3.55 us
    unnamed x14, local copies, waits for them, and re-layouts  2.58 us
    pallas_call x1, Pallas kernels, output(): pl.pallas_call(lambda *refs: output_kernel(scale, depth, *refs), out_shap...  2.4 us
  transfers between devices with their start and end apart: 18, of which 8 were waited for; matrix products, arithmetic and copies ran while one was open for 0% of the time, Pallas kernels for 6%

profile of v5, /device:TPU:0, one launch (start us, length us, event | category | flops | bytes accessed | tf_op | source)
XLA Modules:
  0.0 85.1 jit_solution(15358739381489388432)
XLA Ops:
  0.0 0.8 copy-done.1
  0.8 0.8 spread.3
  1.7 6.2 %all-to-all-start.1 = ((bf16[8,128,256]{2,1,0:T(8,128)(2,1)}), bf16[8,128,256]{2,1,0:T(8,128)(2,1)S(1)}, u32[]{:S(2)}, u32[]{:S(2)}) async-start(bf16[8,128,256]{2,1,0:T(8,128)(2,1)} %spread.3), calls=%async_computation.1 | async-start | bytes 1048576 | tf_op jit(solution)/shard_map/all_to_all | solution.py:413
  7.9 2.7 %collective-permute-start = (bf16[128,256]{1,0:T(8,128)(2,1)S(1)}, bf16[128,256]{1,0:T(8,128)(2,1)S(1)}, u32[]{:S(2)}, u32[]{:S(2)}) collective-permute-start(bf16[128,256]{1,0:T(8,128)(2,1)S(1)} %copy-done.2), channel_id=1, source_target_pairs={{0,16},{2,18},{4,20},{6,22},{8,24},{10,26},{12,28},{14,30},{16,0},... | collective-permute-start | bytes 196616 | tf_op jit(solution)/shard_map/ppermute | solution.py:116
  10.6 4.5 %collective-permute-done.refs_0_ = bf16[128,256]{1,0:T(8,128)(2,1)S(1)} collective-permute-done((bf16[128,256]{1,0:T(8,128)(2,1)S(1)}, bf16[128,256]{1,0:T(8,128)(2,1)S(1)}, u32[]{:S(2)}, u32[]{:S(2)}) %collective-permute-start) | collective-permute-done | bytes 65568 | tf_op jit(solution)/shard_map/ppermute | solution.py:116
  15.1 0.8 spread.2
  15.9 2.5 %all-to-all-done.1.own_ref = bf16[8,128,256]{2,1,0:T(8,128)(2,1)S(1)} async-done(((bf16[8,128,256]{2,1,0:T(8,128)(2,1)}), bf16[8,128,256]{2,1,0:T(8,128)(2,1)S(1)}, u32[]{:S(2)}, u32[]{:S(2)}) %all-to-all-start.1) | async-done | bytes 524320 | tf_op jit(solution)/shard_map/all_to_all | solution.py:413
  18.4 5.4 %all-to-all-start = ((bf16[8,128,256]{2,1,0:T(8,128)(2,1)}), bf16[8,128,256]{2,1,0:T(8,128)(2,1)S(1)}, u32[]{:S(2)}, u32[]{:S(2)}) async-start(bf16[8,128,256]{2,1,0:T(8,128)(2,1)} %spread.2), calls=%async_computation | async-start | bytes 1048576 | tf_op jit(solution)/shard_map/all_to_all | solution.py:413
  23.8 7.7 %all-to-all-done.weight_ref = bf16[8,128,256]{2,1,0:T(8,128)(2,1)S(1)} async-done(((bf16[8,128,256]{2,1,0:T(8,128)(2,1)}), bf16[8,128,256]{2,1,0:T(8,128)(2,1)S(1)}, u32[]{:S(2)}, u32[]{:S(2)}) %all-to-all-start) | async-done | bytes 524320 | tf_op jit(solution)/shard_map/all_to_all | solution.py:413
  31.5 1.4 %copy-done.3 = bf16[1,384,2048]{2,1,0:T(8,128)(2,1)S(1)} copy-done((bf16[1,384,2048]{2,1,0:T(8,128)(2,1)S(1)}, bf16[1,384,2048]{2,1,0:T(8,128)(2,1)}, u32[]{:S(2)}) %copy-start.3) | copy-done | bytes 1572888
  32.9 1.0 %norm_rows.1.normed_ref = bf16[384,2048]{1,0:T(8,128)(2,1)S(1)} custom-call(bf16[1,384,2048]{2,1,0:T(8,128)(2,1)S(1)} %copy-done.3, bf16[1,2048]{1,0:T(2,128)(2,1)S(1)} %reshape.16.gain_ref), custom_call_target="tpu_custom_call" | custom-call | flops 1572864000 | bytes 3145728 | tf_op jit(solution)/shard_map/norm_rows/pallas_call | solution.py:140
  34.0 0.0 copy-start
  34.0 0.6 project_near.1.sofar_ref
  34.6 0.3 copy-done
  34.9 0.7 project_own.1.first_ref
  35.6 1.4 %project_other.1 = bf16[512,384]{1,0:T(8,128)(2,1)} custom-call(s32[1]{0:T(128)} %bitcast.me_ref.refs_0_, bf16[384,2048]{1,0:T(8,128)(2,1)S(1)} %norm_rows.1.normed_ref, bf16[8,128,256]{2,1,0:T(8,128)(2,1)S(1)} %collective-permute-done.1.weight_ref, bf16[256,256]{1,0:T(8,128)(2,1)S(1)} %copy-done, f32[384,512]{1,0:T(8,128)S(1)} %project_near.1.sofar_ref, ...), custom_call_target="tpu_custom_call" | custom-call | flops 201326592 | bytes 524288 | tf_op jit(solution)/shard_map/project_other/pallas_call | solution.py:228
  37.0 3.6 %all-to-all-start.2 = ((bf16[16,32,384]{2,1,0:T(8,128)(2,1)}), bf16[16,32,384]{2,1,0:T(8,128)(2,1)S(1)}, u32[]{:S(2)}, u32[]{:S(2)}) async-start(bf16[16,32,384]{2,1,0:T(8,128)(2,1)} %bitcast.1), calls=%async_computation.2 | async-start | bytes 786432 | tf_op jit(solution)/shard_map/all_to_all | solution.py:436
  40.6 2.8 %collective-permute-start.3 = (bf16[256,128]{1,0:T(8,128)(2,1)S(1)}, bf16[256,128]{1,0:T(8,128)(2,1)S(1)}, u32[]{:S(2)}, u32[]{:S(2)}) collective-permute-start(bf16[256,128]{1,0:T(8,128)(2,1)S(1)} %copy-done.5), channel_id=1, source_target_pairs={{0,16},{2,18},{4,20},{6,22},{8,24},{10,26},{12,28},{14,30},{16,0},... | collective-permute-start | bytes 196616 | tf_op jit(solution)/shard_map/ppermute | solution.py:116
  43.4 12.4 %collective-permute-done.3 = bf16[256,128]{1,0:T(8,128)(2,1)S(1)} collective-permute-done((bf16[256,128]{1,0:T(8,128)(2,1)S(1)}, bf16[256,128]{1,0:T(8,128)(2,1)S(1)}, u32[]{:S(2)}, u32[]{:S(2)}) %collective-permute-start.3) | collective-permute-done | bytes 65568 | tf_op jit(solution)/shard_map/ppermute | solution.py:116
  55.9 0.1 collective-permute-start.4
  56.0 1.9 %transform.1 = bf16[384,512]{1,0:T(8,128)(2,1)} custom-call(s32[1]{0:T(128)} %bitcast.me_ref.refs_0_, bf16[512,384]{1,0:T(8,128)(2,1)S(1)} %bitcast.7, bf16[384,768]{1,0:T(8,128)(2,1)S(1)} %copy-done.4), custom_call_target="tpu_custom_call" | custom-call | flops 402653184 | bytes 1572864 | tf_op jit(solution)/shard_map/transform/pallas_call | solution.py:294
  57.9 5.2 %all-to-all-start.3 = ((bf16[16,24,512]{2,1,0:T(8,128)(2,1)}), bf16[16,24,512]{2,1,0:T(8,128)(2,1)S(1)}, u32[]{:S(2)}, u32[]{:S(2)}) async-start(bf16[16,24,512]{2,1,0:T(8,128)(2,1)} %bitcast.3), calls=%async_computation.3 | async-start | bytes 786432 | tf_op jit(solution)/shard_map/all_to_all | solution.py:438
  63.1 2.0 %collective-permute-start.6 = (bf16[4,256,128]{2,1,0:T(8,128)(2,1)S(1)}, bf16[4,256,128]{2,1,0:T(8,128)(2,1)S(1)}, u32[]{:S(2)}, u32[]{:S(2)}) collective-permute-start(bf16[4,256,128]{2,1,0:T(8,128)(2,1)S(1)} %pad_maximum_fusion.refs_2_), channel_id=1, source_target_pairs={{0,4},{2,6},{4,0},{6,2},{8,12},{10,14},{12,8},{14,10},{16,20},{18,... | collective-permute-start | bytes 786440 | tf_op jit(solution)/shard_map/ppermute | solution.py:116
  65.1 1.5 %collective-permute-start.5 = (bf16[4,256,128]{2,1,0:T(8,128)(2,1)S(1)}, bf16[4,256,128]{2,1,0:T(8,128)(2,1)S(1)}, u32[]{:S(2)}, u32[]{:S(2)}) collective-permute-start(bf16[4,256,128]{2,1,0:T(8,128)(2,1)S(1)} %pad_maximum_fusion.refs_2_), channel_id=1, source_target_pairs={{0,2},{2,0},{4,6},{6,4},{8,10},{10,8},{12,14},{14,12},{16,18},{18,... | collective-permute-start | bytes 786440 | tf_op jit(solution)/shard_map/ppermute | solution.py:116
  66.6 8.0 %collective-permute-done.6.refs_4_ = bf16[4,256,128]{2,1,0:T(8,128)(2,1)S(1)} collective-permute-done((bf16[4,256,128]{2,1,0:T(8,128)(2,1)S(1)}, bf16[4,256,128]{2,1,0:T(8,128)(2,1)S(1)}, u32[]{:S(2)}, u32[]{:S(2)}) %collective-permute-start.6) | collective-permute-done | bytes 262176 | tf_op jit(solution)/shard_map/ppermute | solution.py:116
  74.5 1.8 %collective-permute-start.7 = (bf16[2,256,128]{2,1,0:T(8,128)(2,1)S(1)}, bf16[2,256,128]{2,1,0:T(8,128)(2,1)S(1)}, u32[]{:S(2)}, u32[]{:S(2)}) collective-permute-start(bf16[2,256,128]{2,1,0:T(8,128)(2,1)S(1)} %slice.8), channel_id=1, source_target_pairs={{0,2},{2,0},{4,6},{6,4},{8,10},{10,8},{12,14},{14,12},{16,18},{18,... | collective-permute-start | bytes 393224 | tf_op jit(solution)/shard_map/ppermute | solution.py:116
  76.3 1.2 %collective-permute-start.8 = (bf16[2,256,128]{2,1,0:T(8,128)(2,1)S(1)}, bf16[2,256,128]{2,1,0:T(8,128)(2,1)S(1)}, u32[]{:S(2)}, u32[]{:S(2)}) collective-permute-start(bf16[2,256,128]{2,1,0:T(8,128)(2,1)S(1)} %slice.9), channel_id=1, source_target_pairs={{0,4},{2,6},{4,0},{6,2},{8,12},{10,14},{12,8},{14,10},{16,20},{18,... | collective-permute-start | bytes 393224 | tf_op jit(solution)/shard_map/ppermute | solution.py:116
  77.5 0.5 collective-permute-start.11
  78.0 1.5 %collective-permute-done.7.refs_5_ = bf16[2,256,128]{2,1,0:T(8,128)(2,1)S(1)} collective-permute-done((bf16[2,256,128]{2,1,0:T(8,128)(2,1)S(1)}, bf16[2,256,128]{2,1,0:T(8,128)(2,1)S(1)}, u32[]{:S(2)}, u32[]{:S(2)}) %collective-permute-start.7) | collective-permute-done | bytes 131104 | tf_op jit(solution)/shard_map/ppermute | solution.py:116
  79.6 1.8 %collective-permute-done.8.refs_6_ = bf16[2,256,128]{2,1,0:T(8,128)(2,1)S(1)} collective-permute-done((bf16[2,256,128]{2,1,0:T(8,128)(2,1)S(1)}, bf16[2,256,128]{2,1,0:T(8,128)(2,1)S(1)}, u32[]{:S(2)}, u32[]{:S(2)}) %collective-permute-start.8) | collective-permute-done | bytes 131104 | tf_op jit(solution)/shard_map/ppermute | solution.py:116
  81.4 1.3 %collective-permute-done.13.refs_11_ = bf16[2,256,128]{2,1,0:T(8,128)(2,1)S(1)} collective-permute-done((bf16[2,256,128]{2,1,0:T(8,128)(2,1)S(1)}, bf16[2,256,128]{2,1,0:T(8,128)(2,1)S(1)}, u32[]{:S(2)}, u32[]{:S(2)}) %collective-permute-start.13) | collective-permute-done | bytes 131104 | tf_op jit(solution)/shard_map/ppermute | solution.py:116
  82.7 2.4 %output.1 = bf16[384,2048]{1,0:T(8,128)(2,1)} custom-call(s32[1]{0:T(128)} %bitcast.me_ref.refs_0_, bf16[16,24,512]{2,1,0:T(8,128)(2,1)S(1)} %all-to-all-done.3.refs_1_, bf16[4,256,128]{2,1,0:T(8,128)(2,1)S(1)} %pad_maximum_fusion.refs_2_, bf16[4,256,128]{2,1,0:T(8,128)(2,1)S(1)} %collective-permute-done.5.refs_3_, ...), custom_call_target="tpu_custom_call" | custom-call | flops 805306368 | bytes 1572864 | tf_op jit(solution)/shard_map/output/pallas_call | solution.py:376
  (31 shorter events, 0.1 us)
Async XLA Ops:
  0.0 0.8 copy-start.1
  0.8 7.1 %copy-start.2 = (bf16[128,256]{1,0:T(8,128)(2,1)S(1)}, bf16[128,256]{1,0:T(8,128)(2,1)}, u32[]{:S(2)}) copy-start(bf16[128,256]{1,0:T(8,128)(2,1)} %refs_0_.1) | copy-start | bytes 196612
  0.8 30.7 %copy-start.6 = (bf16[2048]{0:T(1024)(128)(2,1)S(1)}, bf16[2048]{0:T(1024)(128)(2,1)}, u32[]{:S(2)}) copy-start(bf16[2048]{0:T(1024)(128)(2,1)} %param.7) | copy-start | bytes 12292
  1.7 16.7 %all-to-all-start.1 = ((bf16[8,128,256]{2,1,0:T(8,128)(2,1)}), bf16[8,128,256]{2,1,0:T(8,128)(2,1)S(1)}, u32[]{:S(2)}, u32[]{:S(2)}) async-start(bf16[8,128,256]{2,1,0:T(8,128)(2,1)} %spread.3), calls=%async_computation.1 | async-start | bytes 1048576 | tf_op jit(solution)/shard_map/all_to_all | solution.py:413
  7.9 7.2 %collective-permute-start = (bf16[128,256]{1,0:T(8,128)(2,1)S(1)}, bf16[128,256]{1,0:T(8,128)(2,1)S(1)}, u32[]{:S(2)}, u32[]{:S(2)}) collective-permute-start(bf16[128,256]{1,0:T(8,128)(2,1)S(1)} %copy-done.2), channel_id=1, source_target_pairs={{0,16},{2,18},{4,20},{6,22},{8,24},{10,26},{12,28},{14,30},{16,0},... | collective-permute-start | bytes 196616 | tf_op jit(solution)/shard_map/ppermute | solution.py:116
  18.4 13.1 %all-to-all-start = ((bf16[8,128,256]{2,1,0:T(8,128)(2,1)}), bf16[8,128,256]{2,1,0:T(8,128)(2,1)S(1)}, u32[]{:S(2)}, u32[]{:S(2)}) async-start(bf16[8,128,256]{2,1,0:T(8,128)(2,1)} %spread.2), calls=%async_computation | async-start | bytes 1048576 | tf_op jit(solution)/shard_map/all_to_all | solution.py:413
  23.8 10.1 %collective-permute-start.2 = (bf16[8,128,256]{2,1,0:T(8,128)(2,1)S(1)}, bf16[8,128,256]{2,1,0:T(8,128)(2,1)S(1)}, u32[]{:S(2)}, u32[]{:S(2)}) collective-permute-start(bf16[8,128,256]{2,1,0:T(8,128)(2,1)S(1)} %all-to-all-done.1.own_ref), channel_id=1, source_target_pairs={{0,1},{1,0},{2,3},{3,2},{4,5},{5,4},{6,7},{7,6},{8,9},{9,8},{10,11... | collective-permute-start | bytes 1572872 | tf_op jit(solution)/shard_map/ppermute | solution.py:116
  31.5 4.1 %collective-permute-start.1 = (bf16[8,128,256]{2,1,0:T(8,128)(2,1)S(1)}, bf16[8,128,256]{2,1,0:T(8,128)(2,1)S(1)}, u32[]{:S(2)}, u32[]{:S(2)}) collective-permute-start(bf16[8,128,256]{2,1,0:T(8,128)(2,1)S(1)} %all-to-all-done.weight_ref), channel_id=1, source_target_pairs={{0,1},{1,0},{2,3},{3,2},{4,5},{5,4},{6,7},{7,6},{8,9},{9,8},{10,11... | collective-permute-start | bytes 1572872 | tf_op jit(solution)/shard_map/ppermute | solution.py:116
  31.5 1.4 %copy-start.3 = (bf16[1,384,2048]{2,1,0:T(8,128)(2,1)S(1)}, bf16[1,384,2048]{2,1,0:T(8,128)(2,1)}, u32[]{:S(2)}) copy-start(bf16[1,384,2048]{2,1,0:T(8,128)(2,1)} %tokens_ref.1) | copy-start | bytes 4718596
  34.0 0.9 %copy-start = (bf16[256,256]{1,0:T(8,128)(2,1)S(1)}, bf16[256,256]{1,0:T(8,128)(2,1)}, u32[]{:S(2)}) copy-start(bf16[256,256]{1,0:T(8,128)(2,1)} %constant.10.clone.split_ref) | copy-start | bytes 393220
  35.6 5.0 %copy-start.5 = (bf16[256,128]{1,0:T(8,128)(2,1)S(1)}, bf16[256,128]{1,0:T(8,128)(2,1)}, u32[]{:S(2)}) copy-start(bf16[256,128]{1,0:T(8,128)(2,1)} %param.9) | copy-start | bytes 196612
  35.6 20.4 %copy-start.4 = (bf16[384,768]{1,0:T(8,128)(2,1)S(1)}, bf16[384,768]{1,0:T(8,128)(2,1)}, u32[]{:S(2)}) copy-start(bf16[384,768]{1,0:T(8,128)(2,1)} %constant.11.clone.refs_2_) | copy-start | bytes 1769476
  37.0 18.9 %all-to-all-start.2 = ((bf16[16,32,384]{2,1,0:T(8,128)(2,1)}), bf16[16,32,384]{2,1,0:T(8,128)(2,1)S(1)}, u32[]{:S(2)}, u32[]{:S(2)}) async-start(bf16[16,32,384]{2,1,0:T(8,128)(2,1)} %bitcast.1), calls=%async_computation.2 | async-start | bytes 786432 | tf_op jit(solution)/shard_map/all_to_all | solution.py:436
  40.6 15.3 %collective-permute-start.3 = (bf16[256,128]{1,0:T(8,128)(2,1)S(1)}, bf16[256,128]{1,0:T(8,128)(2,1)S(1)}, u32[]{:S(2)}, u32[]{:S(2)}) collective-permute-start(bf16[256,128]{1,0:T(8,128)(2,1)S(1)} %copy-done.5), channel_id=1, source_target_pairs={{0,16},{2,18},{4,20},{6,22},{8,24},{10,26},{12,28},{14,30},{16,0},... | collective-permute-start | bytes 196616 | tf_op jit(solution)/shard_map/ppermute | solution.py:116
  55.9 7.2 %collective-permute-start.4 = (bf16[2,256,128]{2,1,0:T(8,128)(2,1)S(1)}, bf16[2,256,128]{2,1,0:T(8,128)(2,1)S(1)}, u32[]{:S(2)}, u32[]{:S(2)}) collective-permute-start(bf16[2,256,128]{2,1,0:T(8,128)(2,1)S(1)} %pad_maximum_fusion.1), channel_id=1, source_target_pairs={{0,8},{2,10},{4,12},{6,14},{8,0},{10,2},{12,4},{14,6},{16,24},{18,... | collective-permute-start | bytes 393224 | tf_op jit(solution)/shard_map/ppermute | solution.py:116
  57.9 24.9 %all-to-all-start.3 = ((bf16[16,24,512]{2,1,0:T(8,128)(2,1)}), bf16[16,24,512]{2,1,0:T(8,128)(2,1)S(1)}, u32[]{:S(2)}, u32[]{:S(2)}) async-start(bf16[16,24,512]{2,1,0:T(8,128)(2,1)} %bitcast.3), calls=%async_computation.3 | async-start | bytes 786432 | tf_op jit(solution)/shard_map/all_to_all | solution.py:438
  63.1 11.4 %collective-permute-start.6 = (bf16[4,256,128]{2,1,0:T(8,128)(2,1)S(1)}, bf16[4,256,128]{2,1,0:T(8,128)(2,1)S(1)}, u32[]{:S(2)}, u32[]{:S(2)}) collective-permute-start(bf16[4,256,128]{2,1,0:T(8,128)(2,1)S(1)} %pad_maximum_fusion.refs_2_), channel_id=1, source_target_pairs={{0,4},{2,6},{4,0},{6,2},{8,12},{10,14},{12,8},{14,10},{16,20},{18,... | collective-permute-start | bytes 786440 | tf_op jit(solution)/shard_map/ppermute | solution.py:116
  65.1 11.2 %collective-permute-start.5 = (bf16[4,256,128]{2,1,0:T(8,128)(2,1)S(1)}, bf16[4,256,128]{2,1,0:T(8,128)(2,1)S(1)}, u32[]{:S(2)}, u32[]{:S(2)}) collective-permute-start(bf16[4,256,128]{2,1,0:T(8,128)(2,1)S(1)} %pad_maximum_fusion.refs_2_), channel_id=1, source_target_pairs={{0,2},{2,0},{4,6},{6,4},{8,10},{10,8},{12,14},{14,12},{16,18},{18,... | collective-permute-start | bytes 786440 | tf_op jit(solution)/shard_map/ppermute | solution.py:116
  66.6 14.8 %collective-permute-start.9 = (bf16[4,256,128]{2,1,0:T(8,128)(2,1)S(1)}, bf16[4,256,128]{2,1,0:T(8,128)(2,1)S(1)}, u32[]{:S(2)}, u32[]{:S(2)}) collective-permute-start(bf16[4,256,128]{2,1,0:T(8,128)(2,1)S(1)} %pad_maximum_fusion.refs_2_), channel_id=1, source_target_pairs={{0,1},{1,0},{2,3},{3,2},{4,5},{5,4},{6,7},{7,6},{8,9},{9,8},{10,11... | collective-permute-start | bytes 786440 | tf_op jit(solution)/shard_map/ppermute | solution.py:116
  74.5 5.0 %collective-permute-start.7 = (bf16[2,256,128]{2,1,0:T(8,128)(2,1)S(1)}, bf16[2,256,128]{2,1,0:T(8,128)(2,1)S(1)}, u32[]{:S(2)}, u32[]{:S(2)}) collective-permute-start(bf16[2,256,128]{2,1,0:T(8,128)(2,1)S(1)} %slice.8), channel_id=1, source_target_pairs={{0,2},{2,0},{4,6},{6,4},{8,10},{10,8},{12,14},{14,12},{16,18},{18,... | collective-permute-start | bytes 393224 | tf_op jit(solution)/shard_map/ppermute | solution.py:116
  76.3 5.0 %collective-permute-start.8 = (bf16[2,256,128]{2,1,0:T(8,128)(2,1)S(1)}, bf16[2,256,128]{2,1,0:T(8,128)(2,1)S(1)}, u32[]{:S(2)}, u32[]{:S(2)}) collective-permute-start(bf16[2,256,128]{2,1,0:T(8,128)(2,1)S(1)} %slice.9), channel_id=1, source_target_pairs={{0,4},{2,6},{4,0},{6,2},{8,12},{10,14},{12,8},{14,10},{16,20},{18,... | collective-permute-start | bytes 393224 | tf_op jit(solution)/shard_map/ppermute | solution.py:116
  77.5 5.2 %collective-permute-start.10 = (bf16[4,256,128]{2,1,0:T(8,128)(2,1)S(1)}, bf16[4,256,128]{2,1,0:T(8,128)(2,1)S(1)}, u32[]{:S(2)}, u32[]{:S(2)}) collective-permute-start(bf16[4,256,128]{2,1,0:T(8,128)(2,1)S(1)} %collective-permute-done.5.refs_3_), channel_id=1, source_target_pairs={{0,1},{1,0},{2,3},{3,2},{4,5},{5,4},{6,7},{7,6},{8,9},{9,8},{10,11... | collective-permute-start | bytes 786440 | tf_op jit(solution)/shard_map/ppermute | solution.py:116
  77.5 5.2 %collective-permute-start.11 = (bf16[4,256,128]{2,1,0:T(8,128)(2,1)S(1)}, bf16[4,256,128]{2,1,0:T(8,128)(2,1)S(1)}, u32[]{:S(2)}, u32[]{:S(2)}) collective-permute-start(bf16[4,256,128]{2,1,0:T(8,128)(2,1)S(1)} %collective-permute-done.6.refs_4_), channel_id=1, source_target_pairs={{0,1},{1,0},{2,3},{3,2},{4,5},{5,4},{6,7},{7,6},{8,9},{9,8},{10,11... | collective-permute-start | bytes 786440 | tf_op jit(solution)/shard_map/ppermute | solution.py:116
  79.6 1.8 %collective-permute-start.12 = (bf16[2,256,128]{2,1,0:T(8,128)(2,1)S(1)}, bf16[2,256,128]{2,1,0:T(8,128)(2,1)S(1)}, u32[]{:S(2)}, u32[]{:S(2)}) collective-permute-start(bf16[2,256,128]{2,1,0:T(8,128)(2,1)S(1)} %collective-permute-done.7.refs_5_), channel_id=1, source_target_pairs={{0,1},{1,0},{2,3},{3,2},{4,5},{5,4},{6,7},{7,6},{8,9},{9,8},{10,11... | collective-permute-start | bytes 393224 | tf_op jit(solution)/shard_map/ppermute | solution.py:116
  81.4 1.3 %collective-permute-start.13 = (bf16[2,256,128]{2,1,0:T(8,128)(2,1)S(1)}, bf16[2,256,128]{2,1,0:T(8,128)(2,1)S(1)}, u32[]{:S(2)}, u32[]{:S(2)}) collective-permute-start(bf16[2,256,128]{2,1,0:T(8,128)(2,1)S(1)} %collective-permute-done.8.refs_6_), channel_id=1, source_target_pairs={{0,1},{1,0},{2,3},{3,2},{4,5},{5,4},{6,7},{7,6},{8,9},{9,8},{10,11... | collective-permute-start | bytes 393224 | tf_op jit(solution)/shard_map/ppermute | solution.py:116
